TPU v7x, 512 devices: a whole 4x8x8 slice. The times are simulated.
512 devices in a mesh: sp: 32 (over z, x), tp: 16 (over y, core).
Axes of the slice: x: 4, y: 8, z: 8, core: 2. Of those that a mesh axis runs over, the one named last changes fastest.
Arguments:
- stream_in: bfloat16 [4096, 2048], P('sp'), may hold values from -8 to 8
- out_cot: bfloat16 [4096, 2048], P('sp'), may hold values from -6 to 6
- route_experts: int32 [4096, 2], P('sp'), may hold values from 0 to 31, all different within a row; in each aligned block of 128 rows (0 to 127, 128 to 255, ...) at most 16 rows name the same one
- route_weights: float32 [4096, 2], P('sp'), may hold values from 0.1 to 1
- w_gate: bfloat16 [32, 2048, 2048], P('sp', None, 'tp'), may hold values from -0.125 to 0.125
- w_up: bfloat16 [32, 2048, 2048], P('sp', None, 'tp'), may hold values from -0.125 to 0.125
- w_down: bfloat16 [32, 2048, 2048], P('sp', 'tp'), may hold values from -0.125 to 0.125
- w_proj: bfloat16 [2048, 1024], P(None, 'tp'), may hold values from -0.1875 to 0.1875
- conv_value: bfloat16 [1024, 4096], P('tp', 'sp'), may hold values from -6 to 6
- conv_gate: bfloat16 [1024, 4096], P('tp', 'sp'), may hold values from -8 to 8
- conv_taps: float32 [31, 1024], P(None, 'tp'), may hold values from -1 to 1
- conv_result: bfloat16 [1024, 4096], P('tp', 'sp'), may hold values from -100 to 100
- channel_norm_gain: float32 [1024], P('tp'), may hold values from 0.1 to 1.9
Outputs:
- grad_gate: bfloat16 [32, 2048, 2048], P('sp', None, 'tp')
- grad_up: bfloat16 [32, 2048, 2048], P('sp', None, 'tp')
- grad_down: bfloat16 [32, 2048, 2048], P('sp', 'tp')
- grad_stream: bfloat16 [4096, 2048], P('sp')
- grad_proj: float32 [2048, 1024], P('sp', 'tp')
- grad_value: bfloat16 [1024, 4096], P('tp', 'sp')
- grad_gate_in: bfloat16 [1024, 4096], P('tp', 'sp')
Inputs may be any that keep to these rules, and one draw needn't show every extreme that they name: `route_experts`: each row names 2 different experts; within each aligned block of 128 rows no expert is named by more than 16 rows, and at least one block reaches that bound for some expert.
All inputs are finite; a program needn't handle non-finite values.
Results may differ from a plain program's by a relative error of at most 0.025.
Values may be sent and summed in bfloat16 or wider, within the bound.
No kernel may reach another device: no remote copies, remote signals or barrier semaphores. Data moves between devices by JAX's collectives and lax.ppermute only.
A program may use at most 64 MiB of HBM per device.

v0:
```python
import functools

import jax
import jax.numpy as jnp
from jax import lax
from jax.experimental import pallas as pl
from jax.experimental.pallas import tpu as pltpu
from jax.sharding import Mesh
from jax.sharding import PartitionSpec as P


norm_eps = 1e-05
clamp_limit = 7.0
alpha_gate = 1.702
bf16 = jnp.bfloat16
f32 = jnp.float32
LANES = 128


TP = ("chip", "core")
VMEM = pl.BlockSpec(memory_space=pltpu.VMEM)
SMEM = pl.BlockSpec(memory_space=pltpu.SMEM)


def dot(a, b, dims):
    return lax.dot_general(a, b, (dims, ((), ())), preferred_element_type=f32)


NN = ((1,), (0,))
NT = ((1,), (1,))
TN = ((0,), (0,))


def local_kernel(body, outs, *args, specs=None, flops=10**9):
    size = sum(a.size * a.dtype.itemsize for a in args)
    return pl.pallas_call(
        body,
        out_shape=outs,
        in_specs=[VMEM] * len(args) if specs is None else specs,
        out_specs=jax.tree.map(lambda _: VMEM, outs),
        cost_estimate=pl.CostEstimate(flops=flops, bytes_accessed=size, transcendentals=0),
        compiler_params=pltpu.CompilerParams(vmem_limit_bytes=40 * 2**20),
    )(*args)


def shaped(shape, dtype):
    return jax.ShapeDtypeStruct(shape, dtype)


def swap_cores(value):
    return lax.ppermute(value, "core", [(0, 1), (1, 0)])


def swap_chips(value):
    count = lax.axis_size("chip")
    return lax.ppermute(value, "chip", [(k, k ^ 1) for k in range(count)])


def prepare(experts, capacity, share, chips, ids, routes, weights, stream, cot, out, slots):
    top, count = routes.shape
    core, part = ids[0], ids[1]
    before = (
        lax.broadcasted_iota(jnp.int32, (count, count), 0)
        < lax.broadcasted_iota(jnp.int32, (count, count), 1)
    ).astype(bf16)
    named = lax.broadcasted_iota(jnp.int32, (experts, count), 0)
    row = lax.broadcasted_iota(jnp.int32, (experts * share, count), 0)
    base = jnp.zeros((experts, 1), f32)
    picked = jnp.zeros((experts * share, count), jnp.bool_)
    weight = jnp.zeros((experts * share, count), f32)
    for k in range(top):
        route = routes[k : k + 1, :]
        hot = named == route
        ones = jnp.where(hot, 1.0, 0.0)
        ahead = dot(ones.astype(bf16), before, NN) + base
        base = base + jnp.sum(ones, axis=1, keepdims=True)
        rank = jnp.sum(jnp.where(hot, ahead, 0.0), axis=0, keepdims=True).astype(jnp.int32)
        slots[k : k + 1, :] = route * capacity + rank
        local = rank - part * share
        held = (local >= 0) & (local < share)
        mine = row == jnp.where(held, route * share + local, -1)
        picked = picked | mine
        weight = weight + jnp.where(mine, weights[k : k + 1, :], 0.0)
    choice = jnp.where(picked, 1.0, 0.0).astype(bf16)
    scale = jnp.sum(weight, axis=1, keepdims=True)
    half = chips * LANES
    for i in range(chips):
        at = pl.ds(pl.multiple_of((2 * i + core) * LANES, LANES), LANES)
        out[:, i * LANES : (i + 1) * LANES] = dot(choice, stream[:, at], NN).astype(bf16)
        got = dot(choice, cot[:, at], NN)
        out[:, half + i * LANES : half + (i + 1) * LANES] = (scale * got).astype(bf16)


def experts_step(mine, other, own, far, own_acts, far_acts, back_mine, back_other):
    half = mine.shape[1] // 2
    for w, acts in ((own, own_acts), (far, far_acts)):

        def product(n, at):
            return dot(mine[:, at : at + half], w[n, :half], NN) + dot(
                other[:, at : at + half], w[n, half:], NN
            )

        pre_gate, pre_up, grad_act = product(0, 0), product(1, 0), product(2, half)
        glu = jnp.minimum(pre_gate, clamp_limit)
        lin = jnp.clip(pre_up, -clamp_limit, clamp_limit)
        sig = jax.nn.sigmoid(alpha_gate * glu)
        slope = sig + alpha_gate * glu * sig * (1.0 - sig)
        acts[2] = (glu * sig * (lin + 1.0)).astype(bf16)
        acts[0] = jnp.where(
            pre_gate < clamp_limit, grad_act * (lin + 1.0) * slope, 0.0
        ).astype(bf16)
        acts[1] = jnp.where(
            jnp.abs(pre_up) < clamp_limit, grad_act * glu * sig, 0.0
        ).astype(bf16)

    def back(at):
        total = 0.0
        for w, acts in ((own, own_acts), (far, far_acts)):
            total = total + dot(acts[0], w[0, at : at + half], NT)
            total = total + dot(acts[1], w[1, at : at + half], NT)
        return total

    back_other[...] = back(half).astype(bf16)
    back_mine[...] = back(0)


def weight_grads(chips, ids, mine, other, far, far_other, own_acts, far_acts, gate, up, down):
    core = ids[0]
    half = chips * LANES
    for turn, (near_rows, far_rows) in enumerate(((mine, far), (other, far_other))):
        which = core if turn == 0 else 1 - core
        for i in range(chips):
            at = pl.ds(pl.multiple_of((2 * i + which) * LANES, LANES), LANES)
            here = slice(i * LANES, (i + 1) * LANES)
            there = slice(half + i * LANES, half + (i + 1) * LANES)
            near, away = near_rows[:, here], far_rows[:, here]
            for n, out in enumerate((gate, up)):
                total = dot(near, own_acts[n], TN) + dot(away, far_acts[n], TN)
                out[at, :] = total.astype(bf16)
            total = dot(own_acts[2], near_rows[:, there], TN)
            total = total + dot(far_acts[2], far_rows[:, there], TN)
            down[:, at] = total.astype(bf16)


def finish(capacity, share, chips, data, slots, cot, lean_one, lean_two, out):
    rows, count = data.shape[0], slots.shape[1]
    row = lax.broadcasted_iota(jnp.int32, (rows, count), 0)
    expert = row // (chips * share)
    chip = (row // share) % chips
    key = expert * capacity + (chip % 2) * share + row % share
    hit = (key == slots[0:1, :]) | (key == slots[1:2, :])
    total = dot(jnp.where(hit, 1.0, 0.0).astype(bf16), data[...], TN)
    stream = (cot[...].astype(f32) + total).astype(bf16)
    out[0:count, :] = stream
    wide = stream.astype(f32)
    one = jnp.sum((wide * lean_one[...]).T, axis=0, keepdims=True)
    two = jnp.sum((wide * lean_two[...]).T, axis=0, keepdims=True)
    at = lax.broadcasted_iota(jnp.int32, (16, count), 0)
    both = jnp.where((at // 2) % 2 == 0, one, two)
    high = both.astype(bf16)
    low = (both - high.astype(f32)).astype(bf16)
    out[count : count + 16, :] = jnp.where(at % 2 == 0, high.astype(f32), low.astype(f32)).astype(bf16)


def tail(total_channels, got, proj_t, hid_t, steep, centred, inverse, conv, stream, packed):
    pieces, count = got.shape[0], stream.shape[0]
    channels = proj_t.shape[0]
    lane = lax.broadcasted_iota(jnp.int32, (32, 2 * channels), 1)
    hidden_grad = jnp.zeros((channels, count), f32)
    sums = jnp.zeros((16, count), f32)
    for j in range(pieces):
        part = got[j, :count, :]
        stream[:, j * LANES : (j + 1) * LANES] = part
        hidden_grad = hidden_grad + dot(proj_t[:, j * LANES : (j + 1) * LANES], part, NT)
        sums = sums + got[j, count : count + 16, :].astype(f32)
        outer = dot(part, hid_t[...], TN)
        for u in range(2):
            first = outer[64 * u : 64 * u + 32]
            second = outer[64 * u + 32 : 64 * u + 64]
            packed[2 * j + u] = jnp.where(lane < channels, first, second).astype(bf16)
    mean_one = (sums[0:1] + sums[1:2]) / total_channels
    mean_two = (sums[2:3] + sums[3:4]) / total_channels
    xhat = hidden_grad * steep[...]
    conv[...] = inverse[...] * (xhat - mean_one - centred[...] * mean_two)


def convolve(conv, rim, taps, gate, value, grad_value, grad_gate_in):
    count = conv.shape[1]
    lane = lax.broadcasted_iota(jnp.int32, conv.shape, 1)
    near, after = conv[...], rim[...]
    total = taps[:, 0:1] * near
    for tap in range(1, taps.shape[1]):
        shifted = jnp.where(
            lane < count - tap,
            pltpu.roll(near, count - tap, 1),
            pltpu.roll(after, count - tap, 1),
        )
        total = total + taps[:, tap : tap + 1] * shifted
    sig = jax.nn.sigmoid(gate[...].astype(f32))
    grad_value[...] = (total * sig).astype(bf16)
    grad_gate_in[...] = (total * value[...].astype(f32) * sig * (1.0 - sig)).astype(bf16)


def split_three(x):
    high = lax.reduce_precision(x, 8, 7)
    middle = lax.reduce_precision(x - high, 8, 7)
    return jnp.stack([high, middle, x - high - middle]).astype(bf16)


def norm_terms(conv, gain, mean, inverse):
    centred = (conv.astype(f32) - mean) * inverse
    normed = centred * gain
    sig = jax.nn.sigmoid(normed)
    steep = sig * (1.0 + normed * (1.0 - sig)) * gain
    return centred, normed * sig, steep


def body(
    stream_in,
    out_cot,
    route_experts,
    route_weights,
    w_gate,
    w_up,
    w_down,
    w_proj,
    conv_value,
    conv_gate,
    conv_taps,
    conv_result,
    channel_norm_gain,
):
    sp_count = lax.axis_size("sp")
    chips = lax.axis_size("chip")
    core = lax.axis_index("core")
    chip = lax.axis_index("chip")
    tp = 2 * chip + core
    tp_count = 2 * chips
    experts = w_gate.shape[0] * sp_count
    tokens, width = stream_in.shape
    top = route_experts.shape[1]
    capacity = 2 * top * tokens // experts
    share = capacity // 2
    rows = sp_count * share
    half = width // 2
    cols = width // tp_count
    hid = w_gate.shape[2]

    def halves(x, axis):
        shape = x.shape[:axis] + (chips, 2, cols) + x.shape[axis + 1 :]
        x = x.reshape(shape)
        mine = lax.dynamic_index_in_dim(x, core, axis + 1, keepdims=False)
        other = lax.dynamic_index_in_dim(x, 1 - core, axis + 1, keepdims=False)
        flat = shape[:axis] + (half,) + shape[axis + 3 :]
        return mine.reshape(flat), other.reshape(flat)

    channels = conv_result.shape[0]
    channel_total = channels * tp_count
    positions = conv_result.shape[1]
    proj_t = w_proj.T
    proj_out = proj_t.reshape(channels, tp_count, cols).transpose(1, 0, 2)
    proj_in = lax.all_to_all(proj_out, TP, 0, 0, tiled=True)

    w_own = jnp.stack([w_gate[0], w_up[0], w_down[0].T])
    w_own = jnp.concatenate(halves(w_own, 1), axis=1)
    w_far = swap_chips(w_own)

    ids = jnp.stack([core, chip % 2]).astype(jnp.int32)
    sent, slots = local_kernel(
        functools.partial(prepare, experts, capacity, share, chips),
        (shaped((experts * share, width), bf16), shaped((top, tokens), jnp.int32)),
        ids,
        route_experts.T,
        route_weights.T,
        stream_in,
        out_cot,
        specs=[SMEM, VMEM, VMEM, VMEM, VMEM],
    )
    sent, proj_in, w_own = lax.optimization_barrier((sent, proj_in, w_own))
    mine = lax.all_to_all(sent.reshape(experts, share, width), "sp", 0, 0, tiled=True)
    mine = mine.reshape(rows, width)
    other = swap_cores(mine)

    far_rows = swap_chips(mine)

    own_acts, far_acts, back_mine, back_other = local_kernel(
        experts_step,
        (
            shaped((3, rows, hid), bf16),
            shaped((3, rows, hid), bf16),
            shaped((rows, half), f32),
            shaped((rows, half), bf16),
        ),
        mine,
        other,
        w_own,
        w_far,
    )
    from_core = swap_cores(back_other)
    back = (back_mine + from_core.astype(f32)).astype(bf16)
    back = back.reshape(sp_count, share, chips, cols).transpose(0, 2, 1, 3)
    back = back.reshape(sp_count * chips, share, cols)
    gains = jnp.pad(split_three(channel_norm_gain), ((0, 5), (0, positions - channels)))
    conv_out = jnp.concatenate([conv_result, gains])
    back, own_acts, far_acts, conv_out = lax.optimization_barrier(
        (back, own_acts, far_acts, conv_out)
    )
    returned = lax.all_to_all(back, ("sp", "chip"), 0, 0, tiled=True)

    far_acts = swap_chips(far_acts)
    far_other = swap_cores(far_rows)
    gate, up, down = local_kernel(
        functools.partial(weight_grads, chips),
        (shaped((width, hid), bf16), shaped((width, hid), bf16), shaped((hid, width), bf16)),
        ids,
        mine,
        other,
        far_rows,
        far_other,
        own_acts,
        far_acts,
        specs=[SMEM] + [VMEM] * 6,
    )
    grad_gate, grad_up, grad_down = gate[None], up[None], down[None]

    every = lax.all_gather(conv_out, TP)
    all_conv = every[:, :channels].reshape(channel_total, positions).astype(f32)
    all_gain = jnp.sum(every[:, channels : channels + 3, :channels].astype(f32), axis=1)
    all_gain = all_gain.reshape(channel_total, 1)
    mean = jnp.sum(all_conv, axis=0) / channel_total
    variance = jnp.sum(all_conv * all_conv, axis=0) / channel_total - mean * mean
    inverse = lax.rsqrt(variance + norm_eps)
    all_centred, _, all_steep = norm_terms(all_conv, all_gain, mean, inverse)
    centred, hidden, steep = norm_terms(
        conv_result, channel_norm_gain[:, None], mean, inverse
    )
    hidden = hidden.astype(bf16)

    proj_in = proj_in.reshape(channel_total, cols)
    lean_one = dot(all_steep.astype(bf16), proj_in, TN)
    lean_two = dot((all_steep * all_centred).astype(bf16), proj_in, TN)

    cot_cols = lax.dynamic_slice_in_dim(out_cot, tp * cols, cols, 1)
    payload = local_kernel(
        functools.partial(finish, capacity, share, chips),
        shaped((tokens + 16, cols), bf16),
        returned.reshape(experts * chips * share, cols),
        slots,
        cot_cols,
        lean_one,
        lean_two,
    )
    got = lax.all_gather(payload, TP)

    grad_conv, grad_stream, packed = local_kernel(
        functools.partial(tail, channel_total),
        (
            shaped((channels, positions), f32),
            shaped((tokens, width), bf16),
            shaped((sp_count, 32, 2 * channels), bf16),
        ),
        got,
        proj_t,
        jnp.concatenate([hidden, hidden]).T,
        steep,
        centred,
        inverse[None],
    )

    packed = lax.all_to_all(packed, "sp", 0, 0, tiled=True)
    total = jnp.sum(packed.astype(f32), axis=0)
    grad_proj = jnp.concatenate([total[:, :channels], total[:, channels:]], axis=0)

    rim = lax.ppermute(grad_conv, "sp", [(k, k - 1) for k in range(1, sp_count)])
    grad_value, grad_gate_in = local_kernel(
        convolve,
        (shaped((channels, positions), bf16), shaped((channels, positions), bf16)),
        grad_conv,
        rim,
        conv_taps.T,
        conv_gate,
        conv_value,
    )
    return (grad_gate, grad_up, grad_down, grad_stream, grad_proj, grad_value, grad_gate_in)


def solution(mesh):
    sp_count = mesh.shape["sp"]
    devices = mesh.devices.reshape(sp_count, -1, 2)
    return jax.shard_map(
        body,
        mesh=Mesh(devices, ("sp", "chip", "core")),
        in_specs=(
            P("sp", None),
            P("sp", None),
            P("sp", None),
            P("sp", None),
            P("sp", None, TP),
            P("sp", None, TP),
            P("sp", TP, None),
            P(None, TP),
            P(TP, "sp"),
            P(TP, "sp"),
            P(None, TP),
            P(TP, "sp"),
            P(TP),
        ),
        out_specs=(
            P("sp", None, TP),
            P("sp", None, TP),
            P("sp", TP, None),
            P("sp", None),
            P("sp", TP),
            P(TP, "sp"),
            P(TP, "sp"),
        ),
        check_vma=False,
    )
```

profile of v0, /device:TPU:1, one launch (start us, length us, event | category | flops | bytes accessed | tf_op | source)
XLA Modules:
  0.0 191.2 jit_solution(6866859318517877707)
XLA Ops:
  0.7 1.8 bitcast_bitcast_fusion
  2.5 10.8 %all-to-all-start = ((bf16[16,64,128]{2,1,0:T(8,128)(2,1)}), bf16[16,64,128]{2,1,0:T(8,128)(2,1)}, u32[]{:S(2)}, u32[]{:S(2)}) async-start(bf16[16,64,128]{2,1,0:T(8,128)(2,1)} %bitcast_bitcast_fusion), calls=%async_computation | async-start | bytes 524288 | tf_op jit(solution)/shard_map/all_to_all | solution.py:262
  13.2 1.4 stack.40
  15.4 0.9 copy-done.2
  16.5 1.2 shard_map.180
  17.8 0.9 copy-done
  18.8 6.3 %all-to-all-done = bf16[16,64,128]{2,1,0:T(8,128)(2,1)} async-done(((bf16[16,64,128]{2,1,0:T(8,128)(2,1)}), bf16[16,64,128]{2,1,0:T(8,128)(2,1)}, u32[]{:S(2)}, u32[]{:S(2)}) %all-to-all-start) | async-done | bytes 262176 | tf_op jit(solution)/shard_map/all_to_all | solution.py:262
  25.1 10.6 %all-to-all-start.1 = ((bf16[32,8,2048]{2,1,0:T(8,128)(2,1)}), bf16[32,8,2048]{2,1,0:T(8,128)(2,1)S(1)}, u32[]{:S(2)}, u32[]{:S(2)}) async-start(bf16[32,8,2048]{2,1,0:T(8,128)(2,1)} %bitcast.55), calls=%async_computation.1 | async-start | bytes 2097152 | tf_op jit(solution)/shard_map/all_to_all | solution.py:280
  35.7 1.9 %collective-permute-start.3 = (bf16[3,2048,128]{2,1,0:T(8,128)(2,1)S(1)}, bf16[3,2048,128]{2,1,0:T(8,128)(2,1)}, u32[]{:S(2)}, u32[]{:S(2)}) collective-permute-start(bf16[3,2048,128]{2,1,0:T(8,128)(2,1)S(1)} %pad_maximum_fusion.1.own), channel_id=1, source_target_pairs={{0,2},{2,0},{4,6},{6,4},{8,10},{10,8},{12,14},{14,12},{1,3},{3,1},... | collective-permute-start | bytes 4718600 | tf_op jit(solution)/shard_map/ppermute | solution.py:56
  37.6 25.3 %all-to-all-done.1 = bf16[32,8,2048]{2,1,0:T(8,128)(2,1)S(1)} async-done(((bf16[32,8,2048]{2,1,0:T(8,128)(2,1)}), bf16[32,8,2048]{2,1,0:T(8,128)(2,1)S(1)}, u32[]{:S(2)}, u32[]{:S(2)}) %all-to-all-start.1) | async-done | bytes 1048608 | tf_op jit(solution)/shard_map/all_to_all | solution.py:280
  62.9 3.7 %collective-permute-start = (bf16[256,2048]{1,0:T(8,128)(2,1)S(1)}, bf16[256,2048]{1,0:T(8,128)(2,1)}, u32[]{:S(2)}, u32[]{:S(2)}) collective-permute-start(bf16[256,2048]{1,0:T(8,128)(2,1)S(1)} %bitcast.51), channel_id=1, source_target_pairs={{0,1},{1,0},{2,3},{3,2},{4,5},{5,4},{6,7},{7,6},{8,9},{9,8},{10,11... | collective-permute-start | bytes 3145736 | tf_op jit(solution)/shard_map/ppermute | solution.py:51
  66.6 1.9 %collective-permute-start.1 = (bf16[256,2048]{1,0:T(8,128)(2,1)S(1)}, bf16[256,2048]{1,0:T(8,128)(2,1)}, u32[]{:S(2)}, u32[]{:S(2)}) collective-permute-start(bf16[256,2048]{1,0:T(8,128)(2,1)S(1)} %bitcast.52), channel_id=1, source_target_pairs={{0,2},{2,0},{4,6},{6,4},{8,10},{10,8},{12,14},{14,12},{1,3},{3,1},... | collective-permute-start | bytes 3145736 | tf_op jit(solution)/shard_map/ppermute | solution.py:56
  68.5 5.1 %collective-permute-done.3.far = bf16[3,2048,128]{2,1,0:T(8,128)(2,1)} collective-permute-done((bf16[3,2048,128]{2,1,0:T(8,128)(2,1)S(1)}, bf16[3,2048,128]{2,1,0:T(8,128)(2,1)}, u32[]{:S(2)}, u32[]{:S(2)}) %collective-permute-start.3) | collective-permute-done | bytes 1572896 | tf_op jit(solution)/shard_map/ppermute | solution.py:56
  73.7 4.7 %shard_map.181 = (bf16[3,256,128]{2,1,0:T(8,128)(2,1)S(1)}, bf16[3,256,128]{2,1,0:T(8,128)(2,1)S(1)}, f32[256,1024]{1,0:T(8,128)S(1)}, bf16[256,1024]{1,0:T(8,128)(2,1)S(1)}) custom-call(bf16[256,2048]{1,0:T(8,128)(2,1)S(1)} %bitcast.53, bf16[256,2048]{1,0:T(8,128)(2,1)} %collective-permute-done.other, bf16[3,2048,128]{2,1,0:T(8,128)(2,1)S(1)} %pad_maximum_fusion.1.own, ...), custom_call_target="tpu_custom_call" | custom-call | flops 1000000000 | bytes 5242880 | tf_op jit(solution)/shard_map/pallas_call | solution.py:36
  78.4 3.1 %collective-permute-start.4 = (bf16[256,1024]{1,0:T(8,128)(2,1)S(1)}, bf16[256,1024]{1,0:T(8,128)(2,1)S(1)}, u32[]{:S(2)}, u32[]{:S(2)}) collective-permute-start(bf16[256,1024]{1,0:T(8,128)(2,1)S(1)} %get-tuple-element.32), channel_id=1, source_target_pairs={{0,1},{1,0},{2,3},{3,2},{4,5},{5,4},{6,7},{7,6},{8,9},{9,8},{10,11... | collective-permute-start | bytes 1572872 | tf_op jit(solution)/shard_map/ppermute | solution.py:51
  81.6 14.6 %collective-permute-done.1.far = bf16[256,2048]{1,0:T(8,128)(2,1)} collective-permute-done((bf16[256,2048]{1,0:T(8,128)(2,1)S(1)}, bf16[256,2048]{1,0:T(8,128)(2,1)}, u32[]{:S(2)}, u32[]{:S(2)}) %collective-permute-start.1) | collective-permute-done | bytes 1048608 | tf_op jit(solution)/shard_map/ppermute | solution.py:56
  96.1 2.7 %collective-permute-start.2 = (bf16[256,2048]{1,0:T(8,128)(2,1)}, bf16[256,2048]{1,0:T(8,128)(2,1)S(1)}, u32[]{:S(2)}, u32[]{:S(2)}) collective-permute-start(bf16[256,2048]{1,0:T(8,128)(2,1)} %collective-permute-done.1.far), channel_id=1, source_target_pairs={{0,1},{1,0},{2,3},{3,2},{4,5},{5,4},{6,7},{7,6},{8,9},{9,8},{10,11... | collective-permute-start | bytes 3145736 | tf_op jit(solution)/shard_map/ppermute | solution.py:51
  98.8 0.9 add_convert_fusion
  99.8 15.2 %all-gather = bf16[1152,128]{1,0:T(8,128)(2,1)S(1)} all-gather(bf16[72,128]{1,0:T(8,128)(2,1)S(1)} %pad_maximum_fusion.3), channel_id=2, replica_groups=mesh['sp'=32,'chip'=8,'core'=2] {'chip','core'}, dimensions={0}, use_global_device_ids=true | all-gather | bytes 313344 | tf_op jit(solution)/shard_map/all_gather | solution.py:326
  115.2 16.2 %all-to-all-start.2 = ((bf16[256,8,128]{2,1,0:T(8,128)(2,1)}), bf16[256,8,128]{2,1,0:T(8,128)(2,1)S(1)}, u32[]{:S(2)}, u32[]{:S(2)}) async-start(bf16[256,8,128]{2,1,0:T(8,128)(2,1)} %bitcast.16), calls=%async_computation.2 | async-start | bytes 1048576 | tf_op jit(solution)/shard_map/all_to_all | solution.py:308
  131.5 1.4 convolution_bitcast_fusion.1.lean_one
  133.2 1.5 convolution_bitcast_fusion.lean_two
  134.6 16.9 %all-to-all-done.2 = bf16[256,8,128]{2,1,0:T(8,128)(2,1)S(1)} async-done(((bf16[256,8,128]{2,1,0:T(8,128)(2,1)}), bf16[256,8,128]{2,1,0:T(8,128)(2,1)S(1)}, u32[]{:S(2)}, u32[]{:S(2)}) %all-to-all-start.2) | async-done | bytes 524320 | tf_op jit(solution)/shard_map/all_to_all | solution.py:308
  151.5 0.9 shard_map.183
  152.4 18.4 %all-gather.1 = bf16[2304,128]{1,0:T(8,128)(2,1)S(1)} all-gather(bf16[144,128]{1,0:T(8,128)(2,1)S(1)} %shard_map.183), channel_id=3, replica_groups=mesh['sp'=32,'chip'=8,'core'=2] {'chip','core'}, dimensions={0}, use_global_device_ids=true | all-gather | bytes 626688 | tf_op jit(solution)/shard_map/all_gather | solution.py:353
  170.8 1.4 shard_map.184
  172.2 4.0 %all-to-all-start.3 = ((bf16[32,32,128]{2,1,0:T(8,128)(2,1)}), bf16[32,32,128]{2,1,0:T(8,128)(2,1)S(1)}, u32[]{:S(2)}, u32[]{:S(2)}) async-start(bf16[32,32,128]{2,1,0:T(8,128)(2,1)} %get-tuple-element.45), calls=%async_computation.3 | async-start | bytes 524288 | tf_op jit(solution)/shard_map/all_to_all | solution.py:370
  176.3 3.0 %collective-permute-start.5 = (bf16[3,256,128]{2,1,0:T(8,128)(2,1)S(1)}, bf16[3,256,128]{2,1,0:T(8,128)(2,1)S(1)}, u32[]{:S(2)}, u32[]{:S(2)}) collective-permute-start(bf16[3,256,128]{2,1,0:T(8,128)(2,1)S(1)} %copy-done.5), channel_id=1, source_target_pairs={{0,2},{2,0},{4,6},{6,4},{8,10},{10,8},{12,14},{14,12},{1,3},{3,1},... | collective-permute-start | bytes 589832 | tf_op jit(solution)/shard_map/ppermute | solution.py:56
  179.4 1.4 collective-permute-start.6
  180.8 3.3 %collective-permute-done.5.far_acts = bf16[3,256,128]{2,1,0:T(8,128)(2,1)S(1)} collective-permute-done((bf16[3,256,128]{2,1,0:T(8,128)(2,1)S(1)}, bf16[3,256,128]{2,1,0:T(8,128)(2,1)S(1)}, u32[]{:S(2)}, u32[]{:S(2)}) %collective-permute-start.5) | collective-permute-done | bytes 196640 | tf_op jit(solution)/shard_map/ppermute | solution.py:56
  184.2 4.7 %shard_map.182 = (bf16[2048,128]{1,0:T(8,128)(2,1)}, bf16[2048,128]{1,0:T(8,128)(2,1)}, bf16[128,2048]{1,0:T(8,128)(2,1)}) custom-call(s32[2]{0:T(128)S(1)} %pad_add_fusion.ids, bf16[256,2048]{1,0:T(8,128)(2,1)S(1)} %bitcast.54, bf16[256,2048]{1,0:T(8,128)(2,1)} %collective-permute-done.other, bf16[256,2048]{1,0:T(8,128)(2,1)} %collective-permute-done.1.far, ...), custom_call_target="tpu_custom_call" | custom-call | flops 1000000000 | bytes 4587528 | tf_op jit(solution)/shard_map/pallas_call | solution.py:36
  188.9 1.6 shard_map.185
  (52 shorter events, 2.5 us)
Async XLA Ops:
  0.6 14.6 %copy-start.10 = (bf16[1,2048,128]{2,1,0:T(8,128)(2,1)S(1)}, bf16[1,2048,128]{2,1,0:T(8,128)(2,1)}, u32[]{:S(2)}) copy-start(bf16[1,2048,128]{2,1,0:T(8,128)(2,1)} %param.17) | copy-start | bytes 1572868
  0.6 14.6 %copy-start.11 = (bf16[1,2048,128]{2,1,0:T(8,128)(2,1)S(1)}, bf16[1,2048,128]{2,1,0:T(8,128)(2,1)}, u32[]{:S(2)}) copy-start(bf16[1,2048,128]{2,1,0:T(8,128)(2,1)} %param.18) | copy-start | bytes 1572868
  2.5 22.6 %all-to-all-start = ((bf16[16,64,128]{2,1,0:T(8,128)(2,1)}), bf16[16,64,128]{2,1,0:T(8,128)(2,1)}, u32[]{:S(2)}, u32[]{:S(2)}) async-start(bf16[16,64,128]{2,1,0:T(8,128)(2,1)} %bitcast_bitcast_fusion), calls=%async_computation | async-start | bytes 524288 | tf_op jit(solution)/shard_map/all_to_all | solution.py:262
  15.3 1.0 copy-start.2
  15.3 1.2 copy-start.3
  15.3 1.2 copy-start.8
  15.3 1.2 copy-start.9
  17.7 1.0 copy-start
  25.1 37.8 %all-to-all-start.1 = ((bf16[32,8,2048]{2,1,0:T(8,128)(2,1)}), bf16[32,8,2048]{2,1,0:T(8,128)(2,1)S(1)}, u32[]{:S(2)}, u32[]{:S(2)}) async-start(bf16[32,8,2048]{2,1,0:T(8,128)(2,1)} %bitcast.55), calls=%async_computation.1 | async-start | bytes 2097152 | tf_op jit(solution)/shard_map/all_to_all | solution.py:280
  35.7 38.0 %collective-permute-start.3 = (bf16[3,2048,128]{2,1,0:T(8,128)(2,1)S(1)}, bf16[3,2048,128]{2,1,0:T(8,128)(2,1)}, u32[]{:S(2)}, u32[]{:S(2)}) collective-permute-start(bf16[3,2048,128]{2,1,0:T(8,128)(2,1)S(1)} %pad_maximum_fusion.1.own), channel_id=1, source_target_pairs={{0,2},{2,0},{4,6},{6,4},{8,10},{10,8},{12,14},{14,12},{1,3},{3,1},... | collective-permute-start | bytes 4718600 | tf_op jit(solution)/shard_map/ppermute | solution.py:56
  62.9 10.8 %collective-permute-start = (bf16[256,2048]{1,0:T(8,128)(2,1)S(1)}, bf16[256,2048]{1,0:T(8,128)(2,1)}, u32[]{:S(2)}, u32[]{:S(2)}) collective-permute-start(bf16[256,2048]{1,0:T(8,128)(2,1)S(1)} %bitcast.51), channel_id=1, source_target_pairs={{0,1},{1,0},{2,3},{3,2},{4,5},{5,4},{6,7},{7,6},{8,9},{9,8},{10,11... | collective-permute-start | bytes 3145736 | tf_op jit(solution)/shard_map/ppermute | solution.py:51
  66.6 29.6 %collective-permute-start.1 = (bf16[256,2048]{1,0:T(8,128)(2,1)S(1)}, bf16[256,2048]{1,0:T(8,128)(2,1)}, u32[]{:S(2)}, u32[]{:S(2)}) collective-permute-start(bf16[256,2048]{1,0:T(8,128)(2,1)S(1)} %bitcast.52), channel_id=1, source_target_pairs={{0,2},{2,0},{4,6},{6,4},{8,10},{10,8},{12,14},{14,12},{1,3},{3,1},... | collective-permute-start | bytes 3145736 | tf_op jit(solution)/shard_map/ppermute | solution.py:56
  68.5 13.0 %copy-start.14 = (f32[64]{0:T(128)S(1)}, f32[64]{0:T(128)}, u32[]{:S(2)}) copy-start(f32[64]{0:T(128)} %param.25) | copy-start | bytes 772
  68.5 13.0 %copy-start.12 = (bf16[64,128]{1,0:T(8,128)(2,1)S(1)}, bf16[64,128]{1,0:T(8,128)(2,1)}, u32[]{:S(2)}) copy-start(bf16[64,128]{1,0:T(8,128)(2,1)} %param.24) | copy-start | bytes 49156
  78.4 21.4 %copy-start.4 = (bf16[3,256,128]{2,1,0:T(8,128)(2,1)}, bf16[3,256,128]{2,1,0:T(8,128)(2,1)S(1)}, u32[]{:S(2)}) copy-start(bf16[3,256,128]{2,1,0:T(8,128)(2,1)S(1)} %get-tuple-element.36) | copy-start | bytes 589828
  78.4 20.5 %collective-permute-start.4 = (bf16[256,1024]{1,0:T(8,128)(2,1)S(1)}, bf16[256,1024]{1,0:T(8,128)(2,1)S(1)}, u32[]{:S(2)}, u32[]{:S(2)}) collective-permute-start(bf16[256,1024]{1,0:T(8,128)(2,1)S(1)} %get-tuple-element.32), channel_id=1, source_target_pairs={{0,1},{1,0},{2,3},{3,2},{4,5},{5,4},{6,7},{7,6},{8,9},{9,8},{10,11... | collective-permute-start | bytes 1572872 | tf_op jit(solution)/shard_map/ppermute | solution.py:51
  96.1 88.0 %collective-permute-start.2 = (bf16[256,2048]{1,0:T(8,128)(2,1)}, bf16[256,2048]{1,0:T(8,128)(2,1)S(1)}, u32[]{:S(2)}, u32[]{:S(2)}) collective-permute-start(bf16[256,2048]{1,0:T(8,128)(2,1)} %collective-permute-done.1.far), channel_id=1, source_target_pairs={{0,1},{1,0},{2,3},{3,2},{4,5},{5,4},{6,7},{7,6},{8,9},{9,8},{10,11... | collective-permute-start | bytes 3145736 | tf_op jit(solution)/shard_map/ppermute | solution.py:51
  115.2 36.3 %all-to-all-start.2 = ((bf16[256,8,128]{2,1,0:T(8,128)(2,1)}), bf16[256,8,128]{2,1,0:T(8,128)(2,1)S(1)}, u32[]{:S(2)}, u32[]{:S(2)}) async-start(bf16[256,8,128]{2,1,0:T(8,128)(2,1)} %bitcast.16), calls=%async_computation.2 | async-start | bytes 1048576 | tf_op jit(solution)/shard_map/all_to_all | solution.py:308
  151.5 19.3 %copy-start.1 = (bf16[2048,64]{0,1:T(8,128)(2,1)S(1)}, bf16[2048,64]{0,1:T(8,128)(2,1)}, u32[]{:S(2)}) copy-start(bf16[2048,64]{0,1:T(8,128)(2,1)} %param.20) | copy-start | bytes 786436
  170.8 5.4 %copy-start.5 = (bf16[3,256,128]{2,1,0:T(8,128)(2,1)S(1)}, bf16[3,256,128]{2,1,0:T(8,128)(2,1)}, u32[]{:S(2)}) copy-start(bf16[3,256,128]{2,1,0:T(8,128)(2,1)} %copy-done.4) | copy-start | bytes 589828
  170.8 8.4 %copy-start.13 = (f32[31,64]{1,0:T(8,128)S(1)}, f32[31,64]{1,0:T(8,128)}, u32[]{:S(2)}) copy-start(f32[31,64]{1,0:T(8,128)} %param.23) | copy-start | bytes 23812
  172.2 18.3 %all-to-all-start.3 = ((bf16[32,32,128]{2,1,0:T(8,128)(2,1)}), bf16[32,32,128]{2,1,0:T(8,128)(2,1)S(1)}, u32[]{:S(2)}, u32[]{:S(2)}) async-start(bf16[32,32,128]{2,1,0:T(8,128)(2,1)} %get-tuple-element.45), calls=%async_computation.3 | async-start | bytes 524288 | tf_op jit(solution)/shard_map/all_to_all | solution.py:370
  176.3 7.9 %collective-permute-start.5 = (bf16[3,256,128]{2,1,0:T(8,128)(2,1)S(1)}, bf16[3,256,128]{2,1,0:T(8,128)(2,1)S(1)}, u32[]{:S(2)}, u32[]{:S(2)}) collective-permute-start(bf16[3,256,128]{2,1,0:T(8,128)(2,1)S(1)} %copy-done.5), channel_id=1, source_target_pairs={{0,2},{2,0},{4,6},{6,4},{8,10},{10,8},{12,14},{14,12},{1,3},{3,1},... | collective-permute-start | bytes 589832 | tf_op jit(solution)/shard_map/ppermute | solution.py:56
  179.4 9.5 %copy-start.6 = (bf16[64,128]{1,0:T(8,128)(2,1)S(1)}, bf16[64,128]{1,0:T(8,128)(2,1)}, u32[]{:S(2)}) copy-start(bf16[64,128]{1,0:T(8,128)(2,1)} %gate.1) | copy-start | bytes 49156
  179.4 9.5 %copy-start.7 = (bf16[64,128]{1,0:T(8,128)(2,1)S(1)}, bf16[64,128]{1,0:T(8,128)(2,1)}, u32[]{:S(2)}) copy-start(bf16[64,128]{1,0:T(8,128)(2,1)} %value.1) | copy-start | bytes 49156
  179.4 9.5 %collective-permute-start.6 = (f32[64,128]{1,0:T(8,128)S(1)}, f32[64,128]{1,0:T(8,128)S(1)}, u32[]{:S(2)}, u32[]{:S(2)}) collective-permute-start(f32[64,128]{1,0:T(8,128)S(1)} %get-tuple-element.46.conv), channel_id=1, source_target_pairs={{16,0},{32,16},{48,32},{64,48},{80,64},{96,80},{112,96},{128,112},... | collective-permute-start | bytes 98312 | tf_op jit(solution)/shard_map/ppermute | solution.py:374
where the time goes:
time: 192 us; the launch traced here: 191 us
  waiting for transfers between devices  71.5 us (37%)
  starting transfers between devices  59.3 us (31%)
  blocking collectives  33.7 us (18%)
  Pallas kernels  14.5 us (8%)
  local copies, waits for them, and re-layouts  6.16 us (3%)
  matrix products  2.9 us (2%)
  other arithmetic  2.22 us (1%)
    all_to_all x1, waiting for transfers between devices, body(): lax.all_to_all(sent.reshape(experts, share, width), 'sp', 0, 0, tiled=True)  25.3 us
    ppermute x3, waiting for transfers between devices, swap_chips(): return lax.ppermute(value, 'chip', [(k, k ^ 1) for k in range(count)])  23.1 us
    all_gather x1, blocking collectives, body(): got = lax.all_gather(payload, TP)  18.4 us
    all_to_all x1, waiting for transfers between devices, body(): returned = lax.all_to_all(back, ('sp', 'chip'), 0, 0, tiled=True)  16.9 us
    all_to_all x1, starting transfers between devices, body(): returned = lax.all_to_all(back, ('sp', 'chip'), 0, 0, tiled=True)  16.2 us
    all_gather x1, blocking collectives, body(): every = lax.all_gather(conv_out, TP)  15.2 us
    pallas_call x6, Pallas kernels, local_kernel(): pl.pallas_call(body, out_shape=outs, in_specs=[VMEM] * len(args) if specs...  14.5 us
    all_to_all x1, starting transfers between devices, body(): proj_in = lax.all_to_all(proj_out, TP, 0, 0, tiled=True)  10.8 us
  transfers between devices with their start and end apart: 11, of which 6 were waited for; matrix products, arithmetic and copies ran while one was open for 4% of the time, Pallas kernels for 8%

commit v1 on v0

--- a/solution.py
+++ b/solution.py
@@ -258,8 +258,15 @@
     channel_total = channels * tp_count
     positions = conv_result.shape[1]
     proj_t = w_proj.T
-    proj_out = proj_t.reshape(channels, tp_count, cols).transpose(1, 0, 2)
-    proj_in = lax.all_to_all(proj_out, TP, 0, 0, tiled=True)
+    gains = jnp.pad(split_three(channel_norm_gain), ((0, 5), (0, positions - channels)))
+    shared = jnp.concatenate([conv_result, gains])
+    proj_out = jnp.concatenate(
+        [
+            proj_t.reshape(channels, tp_count, cols).transpose(1, 0, 2),
+            jnp.broadcast_to(shared, (tp_count, *shared.shape)),
+        ],
+        axis=1,
+    )
 
     w_own = jnp.stack([w_gate[0], w_up[0], w_down[0].T])
     w_own = jnp.concatenate(halves(w_own, 1), axis=1)
@@ -276,10 +283,11 @@
         out_cot,
         specs=[SMEM, VMEM, VMEM, VMEM, VMEM],
     )
-    sent, proj_in, w_own = lax.optimization_barrier((sent, proj_in, w_own))
     mine = lax.all_to_all(sent.reshape(experts, share, width), "sp", 0, 0, tiled=True)
     mine = mine.reshape(rows, width)
     other = swap_cores(mine)
+    proj_out, _ = lax.optimization_barrier((proj_out, mine))
+    every = lax.all_to_all(proj_out, TP, 0, 0, tiled=True)
 
     far_rows = swap_chips(mine)
 
@@ -300,14 +308,41 @@
     back = (back_mine + from_core.astype(f32)).astype(bf16)
     back = back.reshape(sp_count, share, chips, cols).transpose(0, 2, 1, 3)
     back = back.reshape(sp_count * chips, share, cols)
-    gains = jnp.pad(split_three(channel_norm_gain), ((0, 5), (0, positions - channels)))
-    conv_out = jnp.concatenate([conv_result, gains])
-    back, own_acts, far_acts, conv_out = lax.optimization_barrier(
-        (back, own_acts, far_acts, conv_out)
+    back, own_acts, far_acts, every = lax.optimization_barrier(
+        (back, own_acts, far_acts, every)
     )
     returned = lax.all_to_all(back, ("sp", "chip"), 0, 0, tiled=True)
 
     far_acts = swap_chips(far_acts)
+    proj_in = every[:, :channels].reshape(channel_total, cols)
+    every = every[:, channels:]
+    all_conv = every[:, :channels].reshape(channel_total, positions).astype(f32)
+    all_gain = jnp.sum(every[:, channels : channels + 3, :channels].astype(f32), axis=1)
+    all_gain = all_gain.reshape(channel_total, 1)
+    mean = jnp.sum(all_conv, axis=0) / channel_total
+    variance = jnp.sum(all_conv * all_conv, axis=0) / channel_total - mean * mean
+    inverse = lax.rsqrt(variance + norm_eps)
+    all_centred, _, all_steep = norm_terms(all_conv, all_gain, mean, inverse)
+    centred, hidden, steep = norm_terms(
+        conv_result, channel_norm_gain[:, None], mean, inverse
+    )
+    hidden = hidden.astype(bf16)
+
+    lean_one = dot(all_steep.astype(bf16), proj_in, TN)
+    lean_two = dot((all_steep * all_centred).astype(bf16), proj_in, TN)
+
+    cot_cols = lax.dynamic_slice_in_dim(out_cot, tp * cols, cols, 1)
+    payload = local_kernel(
+        functools.partial(finish, capacity, share, chips),
+        shaped((tokens + 16, cols), bf16),
+        returned.reshape(experts * chips * share, cols),
+        slots,
+        cot_cols,
+        lean_one,
+        lean_two,
+    )
+    got = lax.all_gather(payload, TP)
+    far_rows, _ = lax.optimization_barrier((far_rows, got))
     far_other = swap_cores(far_rows)
     gate, up, down = local_kernel(
         functools.partial(weight_grads, chips),
@@ -323,34 +358,6 @@
     )
     grad_gate, grad_up, grad_down = gate[None], up[None], down[None]
 
-    every = lax.all_gather(conv_out, TP)
-    all_conv = every[:, :channels].reshape(channel_total, positions).astype(f32)
-    all_gain = jnp.sum(every[:, channels : channels + 3, :channels].astype(f32), axis=1)
-    all_gain = all_gain.reshape(channel_total, 1)
-    mean = jnp.sum(all_conv, axis=0) / channel_total
-    variance = jnp.sum(all_conv * all_conv, axis=0) / channel_total - mean * mean
-    inverse = lax.rsqrt(variance + norm_eps)
-    all_centred, _, all_steep = norm_terms(all_conv, all_gain, mean, inverse)
-    centred, hidden, steep = norm_terms(
-        conv_result, channel_norm_gain[:, None], mean, inverse
-    )
-    hidden = hidden.astype(bf16)
-
-    proj_in = proj_in.reshape(channel_total, cols)
-    lean_one = dot(all_steep.astype(bf16), proj_in, TN)
-    lean_two = dot((all_steep * all_centred).astype(bf16), proj_in, TN)
-
-    cot_cols = lax.dynamic_slice_in_dim(out_cot, tp * cols, cols, 1)
-    payload = local_kernel(
-        functools.partial(finish, capacity, share, chips),
-        shaped((tokens + 16, cols), bf16),
-        returned.reshape(experts * chips * share, cols),
-        slots,
-        cot_cols,
-        lean_one,
-        lean_two,
-    )
-    got = lax.all_gather(payload, TP)
 
     grad_conv, grad_stream, packed = local_kernel(
         functools.partial(tail, channel_total),

time: 192 us -> 171 us (0.89)
  waiting for transfers between devices: 71.5 us -> 45.7 us
  blocking collectives: 33.7 us -> 19 us
  starting transfers between devices: 59.3 us -> 67.4 us
  local copies, waits for them, and re-layouts: 6.16 us -> 11.1 us
  other arithmetic: 2.22 us -> 7.14 us
    ppermute x3, waiting for transfers between devices: 23.1 us -> 0.01 us  [swap_chips(): return lax.ppermute(value, 'chip', [(k, k ^ 1) for k in range(count)])]
    all_gather x1 -> x0, blocking collectives: 15.2 us -> none  [body(): every = lax.all_gather(conv_out, TP)]
    unnamed x31 -> x35, local copies, waits for them, and re-layouts: 2.07 us -> 9 us
    all_to_all x1, starting transfers between devices: 16.2 us -> 21.7 us  [body(): returned = lax.all_to_all(back, ('sp', 'chip'), 0, 0, tiled=True)]
    all_to_all x1, waiting for transfers between devices: 6.28 us -> 1.48 us  [body(): every = lax.all_to_all(proj_out, TP, 0, 0, tiled=True)]
    all_to_all x1, waiting for transfers between devices: 25.3 us -> 21.3 us  [body(): lax.all_to_all(sent.reshape(experts, share, width), 'sp', 0, 0, tiled=True)]
    all_to_all x1, waiting for transfers between devices: 0.01 us -> 3.56 us  [body(): packed = lax.all_to_all(packed, 'sp', 0, 0, tiled=True)]
    all_to_all x1, starting transfers between devices: 10.8 us -> 7.23 us  [body(): every = lax.all_to_all(proj_out, TP, 0, 0, tiled=True)]
  transfers between devices with their start and end apart: 11 -> 11, of which waited for: 6 -> 5; matrix products, arithmetic and copies ran while one was open for 4% -> 8% of each run, Pallas kernels for 8% -> 5%
where the time goes in v1:
time: 171 us; the launch traced here: 169 us
  starting transfers between devices  67.4 us (39%)
  waiting for transfers between devices  45.7 us (27%)
  blocking collectives  19 us (11%)
  Pallas kernels  15.1 us (9%)
  local copies, waits for them, and re-layouts  11.1 us (6%)
  other arithmetic  7.14 us (4%)
  matrix products  3.06 us (2%)
    all_to_all x1, starting transfers between devices, body(): returned = lax.all_to_all(back, ('sp', 'chip'), 0, 0, tiled=True)  21.7 us
    all_to_all x1, waiting for transfers between devices, body(): lax.all_to_all(sent.reshape(experts, share, width), 'sp', 0, 0, tiled=True)  21.3 us
    all_gather x1, blocking collectives, body(): got = lax.all_gather(payload, TP)  19 us
    all_to_all x1, waiting for transfers between devices, body(): returned = lax.all_to_all(back, ('sp', 'chip'), 0, 0, tiled=True)  18.4 us
    pallas_call x6, Pallas kernels, local_kernel(): pl.pallas_call(body, out_shape=outs, in_specs=[VMEM] * len(args) if specs...  15.1 us
    all_to_all x1, starting transfers between devices, body(): lax.all_to_all(sent.reshape(experts, share, width), 'sp', 0, 0, tiled=True)  13.8 us
    ppermute x3, starting transfers between devices, swap_cores(): return lax.ppermute(value, 'core', [(0, 1), (1, 0)])  10.1 us
    unnamed x35, local copies, waits for them, and re-layouts  9 us
  transfers between devices with their start and end apart: 11, of which 5 were waited for; matrix products, arithmetic and copies ran while one was open for 8% of the time, Pallas kernels for 5%

profile of v1, /device:TPU:1, one launch (start us, length us, event | category | flops | bytes accessed | tf_op | source)
XLA Modules:
  0.0 169.5 jit_solution(15160296189142475522)
XLA Ops:
  0.7 1.0 copy-done.5
  1.8 1.0 copy-done.6
  4.2 2.2 %shard_map.180 = (bf16[256,2048]{1,0:T(8,128)(2,1)}, s32[2,128]{1,0:T(2,128)S(1)}) custom-call(s32[2]{0:T(128)S(1)} %pad_add_fusion.ids, s32[2,128]{1,0:T(2,128)S(1)} %bitcast.56, f32[2,128]{1,0:T(2,128)S(1)} %bitcast.57, bf16[128,2048]{1,0:T(8,128)(2,1)S(1)} %copy-done.6, bf16[128,2048]{1,0:T(8,128)(2,1)S(1)} %copy-done.5), custom_call_target="tpu_custom_call" | custom-call | flops 1000000000 | bytes 1050632 | tf_op jit(solution)/shard_map/pallas_call | solution.py:36
  6.3 13.8 %all-to-all-start = ((bf16[32,8,2048]{2,1,0:T(8,128)(2,1)}), bf16[32,8,2048]{2,1,0:T(8,128)(2,1)S(1)}, u32[]{:S(2)}, u32[]{:S(2)}) async-start(bf16[32,8,2048]{2,1,0:T(8,128)(2,1)} %bitcast.4), calls=%async_computation | async-start | bytes 2097152 | tf_op jit(solution)/shard_map/all_to_all | solution.py:286
  21.8 3.2 %collective-permute-start.2 = (bf16[3,2048,128]{2,1,0:T(8,128)(2,1)S(1)}, bf16[3,2048,128]{2,1,0:T(8,128)(2,1)}, u32[]{:S(2)}, u32[]{:S(2)}) collective-permute-start(bf16[3,2048,128]{2,1,0:T(8,128)(2,1)S(1)} %pad_maximum_fusion.1.own), channel_id=1, source_target_pairs={{0,2},{2,0},{4,6},{6,4},{8,10},{10,8},{12,14},{14,12},{1,3},{3,1},... | collective-permute-start | bytes 4718600 | tf_op jit(solution)/shard_map/ppermute | solution.py:56
  25.0 21.3 %all-to-all-done = bf16[32,8,2048]{2,1,0:T(8,128)(2,1)S(1)} async-done(((bf16[32,8,2048]{2,1,0:T(8,128)(2,1)}), bf16[32,8,2048]{2,1,0:T(8,128)(2,1)S(1)}, u32[]{:S(2)}, u32[]{:S(2)}) %all-to-all-start) | async-done | bytes 1048608 | tf_op jit(solution)/shard_map/all_to_all | solution.py:286
  46.4 4.7 %collective-permute-start = (bf16[256,2048]{1,0:T(8,128)(2,1)S(1)}, bf16[256,2048]{1,0:T(8,128)(2,1)}, u32[]{:S(2)}, u32[]{:S(2)}) collective-permute-start(bf16[256,2048]{1,0:T(8,128)(2,1)S(1)} %bitcast.48), channel_id=1, source_target_pairs={{0,1},{1,0},{2,3},{3,2},{4,5},{5,4},{6,7},{7,6},{8,9},{9,8},{10,11... | collective-permute-start | bytes 3145736 | tf_op jit(solution)/shard_map/ppermute | solution.py:51
  51.3 0.8 pad_maximum_fusion.2
  52.1 7.2 %all-to-all-start.1 = ((bf16[16,136,128]{2,1,0:T(8,128)(2,1)}), bf16[16,136,128]{2,1,0:T(8,128)(2,1)}, u32[]{:S(2)}, u32[]{:S(2)}) async-start(bf16[16,136,128]{2,1,0:T(8,128)(2,1)} %pad_maximum_fusion.2), calls=%async_computation.1 | async-start | bytes 1114112 | tf_op jit(solution)/shard_map/all_to_all | solution.py:290
  59.4 4.7 %shard_map.181 = (bf16[3,256,128]{2,1,0:T(8,128)(2,1)S(1)}, bf16[3,256,128]{2,1,0:T(8,128)(2,1)S(1)}, f32[256,1024]{1,0:T(8,128)S(1)}, bf16[256,1024]{1,0:T(8,128)(2,1)S(1)}) custom-call(bf16[256,2048]{1,0:T(8,128)(2,1)S(1)} %bitcast.49, bf16[256,2048]{1,0:T(8,128)(2,1)} %collective-permute-done.other, bf16[3,2048,128]{2,1,0:T(8,128)(2,1)S(1)} %pad_maximum_fusion.1.own, ...), custom_call_target="tpu_custom_call" | custom-call | flops 1000000000 | bytes 5242880 | tf_op jit(solution)/shard_map/pallas_call | solution.py:36
  64.0 1.0 copy-done
  66.4 3.2 %collective-permute-start.3 = (bf16[256,1024]{1,0:T(8,128)(2,1)S(1)}, bf16[256,1024]{1,0:T(8,128)(2,1)}, u32[]{:S(2)}, u32[]{:S(2)}) collective-permute-start(bf16[256,1024]{1,0:T(8,128)(2,1)S(1)} %get-tuple-element.29), channel_id=1, source_target_pairs={{0,1},{1,0},{2,3},{3,2},{4,5},{5,4},{6,7},{7,6},{8,9},{9,8},{10,11... | collective-permute-start | bytes 1572872 | tf_op jit(solution)/shard_map/ppermute | solution.py:51
  70.3 3.2 %collective-permute-start.1 = (bf16[256,2048]{1,0:T(8,128)(2,1)S(1)}, bf16[256,2048]{1,0:T(8,128)(2,1)S(1)}, u32[]{:S(2)}, u32[]{:S(2)}) collective-permute-start(bf16[256,2048]{1,0:T(8,128)(2,1)S(1)} %bitcast.50), channel_id=1, source_target_pairs={{0,2},{2,0},{4,6},{6,4},{8,10},{10,8},{12,14},{14,12},{1,3},{3,1},... | collective-permute-start | bytes 3145736 | tf_op jit(solution)/shard_map/ppermute | solution.py:56
  73.5 2.3 %add_convert_fusion = bf16[256,1024]{1,0:T(8,128)(2,1)} fusion(f32[256,1024]{1,0:T(8,128)} %copy-done, bf16[256,1024]{1,0:T(8,128)(2,1)} %collective-permute-done.3), kind=kLoop, calls=%fused_computation.4 | loop fusion | flops 786432 | bytes 2097152 | tf_op jit(solution)/shard_map/convert_element_type | solution.py:308
  75.8 1.5 all-to-all-done.1
  77.3 1.1 convert_reduce_fusion
  78.4 21.7 %all-to-all-start.2 = ((bf16[256,8,128]{2,1,0:T(8,128)(2,1)}), bf16[256,8,128]{2,1,0:T(8,128)(2,1)S(1)}, u32[]{:S(2)}, u32[]{:S(2)}) async-start(bf16[256,8,128]{2,1,0:T(8,128)(2,1)} %bitcast.14), calls=%async_computation.2 | async-start | bytes 1048576 | tf_op jit(solution)/shard_map/all_to_all | solution.py:314
  101.2 1.5 convolution_bitcast_fusion.1.lean_one
  102.8 1.5 convolution_bitcast_fusion.lean_two
  104.3 18.4 %all-to-all-done.2 = bf16[256,8,128]{2,1,0:T(8,128)(2,1)S(1)} async-done(((bf16[256,8,128]{2,1,0:T(8,128)(2,1)}), bf16[256,8,128]{2,1,0:T(8,128)(2,1)S(1)}, u32[]{:S(2)}, u32[]{:S(2)}) %all-to-all-start.2) | async-done | bytes 524320 | tf_op jit(solution)/shard_map/all_to_all | solution.py:314
  122.7 0.9 shard_map.182
  123.6 19.0 %all-gather = bf16[2304,128]{1,0:T(8,128)(2,1)S(1)} all-gather(bf16[144,128]{1,0:T(8,128)(2,1)S(1)} %shard_map.182), channel_id=2, replica_groups=mesh['sp'=32,'chip'=8,'core'=2] {'chip','core'}, dimensions={0}, use_global_device_ids=true | all-gather | bytes 626688 | tf_op jit(solution)/shard_map/all_gather | solution.py:344
  142.6 2.2 %collective-permute-start.4 = (bf16[256,2048]{1,0:T(8,128)(2,1)S(1)}, bf16[256,2048]{1,0:T(8,128)(2,1)S(1)}, u32[]{:S(2)}, u32[]{:S(2)}) collective-permute-start(bf16[256,2048]{1,0:T(8,128)(2,1)S(1)} %collective-permute-done.1.far), channel_id=1, source_target_pairs={{0,1},{1,0},{2,3},{3,2},{4,5},{5,4},{6,7},{7,6},{8,9},{9,8},{10,11... | collective-permute-start | bytes 3145736 | tf_op jit(solution)/shard_map/ppermute | solution.py:51
  144.9 1.3 shard_map.184
  146.9 4.6 %all-to-all-start.3 = ((bf16[32,32,128]{2,1,0:T(8,128)(2,1)}), bf16[32,32,128]{2,1,0:T(8,128)(2,1)}, u32[]{:S(2)}, u32[]{:S(2)}) async-start(bf16[32,32,128]{2,1,0:T(8,128)(2,1)} %copy-done.2), calls=%async_computation.3 | async-start | bytes 524288 | tf_op jit(solution)/shard_map/all_to_all | solution.py:377
  151.5 1.3 collective-permute-start.6
  153.6 2.2 %collective-permute-start.5 = (bf16[3,256,128]{2,1,0:T(8,128)(2,1)}, bf16[3,256,128]{2,1,0:T(8,128)(2,1)}, u32[]{:S(2)}, u32[]{:S(2)}) collective-permute-start(bf16[3,256,128]{2,1,0:T(8,128)(2,1)} %copy-done.7), channel_id=1, source_target_pairs={{0,2},{2,0},{4,6},{6,4},{8,10},{10,8},{12,14},{14,12},{1,3},{3,1},... | collective-permute-start | bytes 589832 | tf_op jit(solution)/shard_map/ppermute | solution.py:56
  155.8 0.9 collective-permute-done.6.rim
  158.2 1.6 shard_map.185
  159.7 3.6 %all-to-all-done.3 = bf16[32,32,128]{2,1,0:T(8,128)(2,1)} async-done(((bf16[32,32,128]{2,1,0:T(8,128)(2,1)}), bf16[32,32,128]{2,1,0:T(8,128)(2,1)}, u32[]{:S(2)}, u32[]{:S(2)}) %all-to-all-start.3) | async-done | bytes 262176 | tf_op jit(solution)/shard_map/all_to_all | solution.py:377
  163.3 1.0 convert_reduce_fusion.1
  165.0 4.5 %shard_map.183 = (bf16[2048,128]{1,0:T(8,128)(2,1)}, bf16[2048,128]{1,0:T(8,128)(2,1)}, bf16[128,2048]{1,0:T(8,128)(2,1)}) custom-call(s32[2]{0:T(128)S(1)} %pad_add_fusion.ids, bf16[256,2048]{1,0:T(8,128)(2,1)S(1)} %bitcast.51, bf16[256,2048]{1,0:T(8,128)(2,1)} %collective-permute-done.other, bf16[256,2048]{1,0:T(8,128)(2,1)S(1)} %collective-permute-done.1.far, ...), custom_call_target="tpu_custom_call" | custom-call | flops 1000000000 | bytes 4587528 | tf_op jit(solution)/shard_map/pallas_call | solution.py:36
  (57 shorter events, 9.9 us)
Async XLA Ops:
  0.7 1.0 copy-start.5
  1.8 1.0 copy-start.6
  2.8 0.7 copy-start.10
  3.5 0.7 copy-start.11
  6.3 13.9 %copy-start.12 = (bf16[1,128,2048]{2,1,0:T(8,128)(2,1)S(1)}, bf16[1,128,2048]{2,1,0:T(8,128)(2,1)}, u32[]{:S(2)}) copy-start(bf16[1,128,2048]{2,1,0:T(8,128)(2,1)} %param.19) | copy-start | bytes 1572868
  6.3 40.0 %all-to-all-start = ((bf16[32,8,2048]{2,1,0:T(8,128)(2,1)}), bf16[32,8,2048]{2,1,0:T(8,128)(2,1)S(1)}, u32[]{:S(2)}, u32[]{:S(2)}) async-start(bf16[32,8,2048]{2,1,0:T(8,128)(2,1)} %bitcast.4), calls=%async_computation | async-start | bytes 2097152 | tf_op jit(solution)/shard_map/all_to_all | solution.py:286
  20.2 1.0 copy-start.13
  20.2 1.2 copy-start.14
  21.7 29.4 %copy-start.16 = (f32[64]{0:T(128)S(1)}, f32[64]{0:T(128)}, u32[]{:S(2)}) copy-start(f32[64]{0:T(128)} %param.25) | copy-start | bytes 772
  21.7 29.4 %copy-start.15 = (bf16[64,128]{1,0:T(8,128)(2,1)S(1)}, bf16[64,128]{1,0:T(8,128)(2,1)}, u32[]{:S(2)}) copy-start(bf16[64,128]{1,0:T(8,128)(2,1)} %param.24) | copy-start | bytes 49156
  21.7 29.5 %copy-start.1 = (bf16[2048,64]{0,1:T(8,128)(2,1)S(1)}, bf16[2048,64]{0,1:T(8,128)(2,1)}, u32[]{:S(2)}) copy-start(bf16[2048,64]{0,1:T(8,128)(2,1)} %param.20) | copy-start | bytes 786436
  21.8 37.5 %collective-permute-start.2 = (bf16[3,2048,128]{2,1,0:T(8,128)(2,1)S(1)}, bf16[3,2048,128]{2,1,0:T(8,128)(2,1)}, u32[]{:S(2)}, u32[]{:S(2)}) collective-permute-start(bf16[3,2048,128]{2,1,0:T(8,128)(2,1)S(1)} %pad_maximum_fusion.1.own), channel_id=1, source_target_pairs={{0,2},{2,0},{4,6},{6,4},{8,10},{10,8},{12,14},{14,12},{1,3},{3,1},... | collective-permute-start | bytes 4718600 | tf_op jit(solution)/shard_map/ppermute | solution.py:56
  46.4 13.0 %collective-permute-start = (bf16[256,2048]{1,0:T(8,128)(2,1)S(1)}, bf16[256,2048]{1,0:T(8,128)(2,1)}, u32[]{:S(2)}, u32[]{:S(2)}) collective-permute-start(bf16[256,2048]{1,0:T(8,128)(2,1)S(1)} %bitcast.48), channel_id=1, source_target_pairs={{0,1},{1,0},{2,3},{3,2},{4,5},{5,4},{6,7},{7,6},{8,9},{9,8},{10,11... | collective-permute-start | bytes 3145736 | tf_op jit(solution)/shard_map/ppermute | solution.py:51
  52.1 25.2 %all-to-all-start.1 = ((bf16[16,136,128]{2,1,0:T(8,128)(2,1)}), bf16[16,136,128]{2,1,0:T(8,128)(2,1)}, u32[]{:S(2)}, u32[]{:S(2)}) async-start(bf16[16,136,128]{2,1,0:T(8,128)(2,1)} %pad_maximum_fusion.2), calls=%async_computation.1 | async-start | bytes 1114112 | tf_op jit(solution)/shard_map/all_to_all | solution.py:290
  64.0 1.0 copy-start
  65.0 0.7 copy-start.3
  65.7 0.7 copy-start.7
  66.4 7.2 %collective-permute-start.3 = (bf16[256,1024]{1,0:T(8,128)(2,1)S(1)}, bf16[256,1024]{1,0:T(8,128)(2,1)}, u32[]{:S(2)}, u32[]{:S(2)}) collective-permute-start(bf16[256,1024]{1,0:T(8,128)(2,1)S(1)} %get-tuple-element.29), channel_id=1, source_target_pairs={{0,1},{1,0},{2,3},{3,2},{4,5},{5,4},{6,7},{7,6},{8,9},{9,8},{10,11... | collective-permute-start | bytes 1572872 | tf_op jit(solution)/shard_map/ppermute | solution.py:51
  70.3 72.3 %collective-permute-start.1 = (bf16[256,2048]{1,0:T(8,128)(2,1)S(1)}, bf16[256,2048]{1,0:T(8,128)(2,1)S(1)}, u32[]{:S(2)}, u32[]{:S(2)}) collective-permute-start(bf16[256,2048]{1,0:T(8,128)(2,1)S(1)} %bitcast.50), channel_id=1, source_target_pairs={{0,2},{2,0},{4,6},{6,4},{8,10},{10,8},{12,14},{14,12},{1,3},{3,1},... | collective-permute-start | bytes 3145736 | tf_op jit(solution)/shard_map/ppermute | solution.py:56
  78.4 44.2 %all-to-all-start.2 = ((bf16[256,8,128]{2,1,0:T(8,128)(2,1)}), bf16[256,8,128]{2,1,0:T(8,128)(2,1)S(1)}, u32[]{:S(2)}, u32[]{:S(2)}) async-start(bf16[256,8,128]{2,1,0:T(8,128)(2,1)} %bitcast.14), calls=%async_computation.2 | async-start | bytes 1048576 | tf_op jit(solution)/shard_map/all_to_all | solution.py:314
  142.6 22.4 %collective-permute-start.4 = (bf16[256,2048]{1,0:T(8,128)(2,1)S(1)}, bf16[256,2048]{1,0:T(8,128)(2,1)S(1)}, u32[]{:S(2)}, u32[]{:S(2)}) collective-permute-start(bf16[256,2048]{1,0:T(8,128)(2,1)S(1)} %collective-permute-done.1.far), channel_id=1, source_target_pairs={{0,1},{1,0},{2,3},{3,2},{4,5},{5,4},{6,7},{7,6},{8,9},{9,8},{10,11... | collective-permute-start | bytes 3145736 | tf_op jit(solution)/shard_map/ppermute | solution.py:51
  146.2 0.7 copy-start.2
  146.9 16.4 %all-to-all-start.3 = ((bf16[32,32,128]{2,1,0:T(8,128)(2,1)}), bf16[32,32,128]{2,1,0:T(8,128)(2,1)}, u32[]{:S(2)}, u32[]{:S(2)}) async-start(bf16[32,32,128]{2,1,0:T(8,128)(2,1)} %copy-done.2), calls=%async_computation.3 | async-start | bytes 524288 | tf_op jit(solution)/shard_map/all_to_all | solution.py:377
  151.5 5.2 %collective-permute-start.6 = (f32[64,128]{1,0:T(8,128)S(1)}, f32[64,128]{1,0:T(8,128)S(1)}, u32[]{:S(2)}, u32[]{:S(2)}) collective-permute-start(f32[64,128]{1,0:T(8,128)S(1)} %get-tuple-element.44.conv), channel_id=1, source_target_pairs={{16,0},{32,16},{48,32},{64,48},{80,64},{96,80},{112,96},{128,112},... | collective-permute-start | bytes 98312 | tf_op jit(solution)/shard_map/ppermute | solution.py:381
  153.6 11.4 %collective-permute-start.5 = (bf16[3,256,128]{2,1,0:T(8,128)(2,1)}, bf16[3,256,128]{2,1,0:T(8,128)(2,1)}, u32[]{:S(2)}, u32[]{:S(2)}) collective-permute-start(bf16[3,256,128]{2,1,0:T(8,128)(2,1)} %copy-done.7), channel_id=1, source_target_pairs={{0,2},{2,0},{4,6},{6,4},{8,10},{10,8},{12,14},{14,12},{1,3},{3,1},... | collective-permute-start | bytes 589832 | tf_op jit(solution)/shard_map/ppermute | solution.py:56
  156.7 0.7 copy-start.8
  157.4 0.7 copy-start.9
  158.2 6.8 %copy-start.4 = (bf16[3,256,128]{2,1,0:T(8,128)(2,1)S(1)}, bf16[3,256,128]{2,1,0:T(8,128)(2,1)}, u32[]{:S(2)}) copy-start(bf16[3,256,128]{2,1,0:T(8,128)(2,1)} %copy-done.3) | copy-start | bytes 589828

commit v2 on v0

--- a/solution.py
+++ b/solution.py
@@ -54,6 +54,18 @@
 def swap_chips(value):
     count = lax.axis_size("chip")
     return lax.ppermute(value, "chip", [(k, k ^ 1) for k in range(count)])
+
+
+def pack_weights(chips, ids, gate, up, down, out):
+    half = chips * LANES
+    for turn in range(2):
+        which = ids[0] if turn == 0 else 1 - ids[0]
+        for i in range(chips):
+            at = pl.ds(pl.multiple_of((2 * i + which) * LANES, LANES), LANES)
+            here = slice(turn * half + i * LANES, turn * half + (i + 1) * LANES)
+            out[0, here, :] = gate[at, :]
+            out[1, here, :] = up[at, :]
+            out[2, here, :] = down[:, at]
 
 
 def prepare(experts, capacity, share, chips, ids, routes, weights, stream, cot, out, slots):
@@ -100,7 +112,13 @@
                 other[:, at : at + half], w[n, half:], NN
             )
 
-        pre_gate, pre_up, grad_act = product(0, 0), product(1, 0), product(2, half)
+        pre_gate, pre_up = product(0, 0), product(1, 0)
+        grad_act = 0.0
+        for i in range(half // LANES):
+            here, there = i * LANES, half + i * LANES
+            block = slice(there, there + LANES)
+            grad_act = grad_act + dot(mine[:, block], w[2, here : here + LANES], NT)
+            grad_act = grad_act + dot(other[:, block], w[2, there : there + LANES], NT)
         glu = jnp.minimum(pre_gate, clamp_limit)
         lin = jnp.clip(pre_up, -clamp_limit, clamp_limit)
         sig = jax.nn.sigmoid(alpha_gate * glu)
@@ -142,7 +160,13 @@
             down[:, at] = total.astype(bf16)
 
 
-def finish(capacity, share, chips, data, slots, cot, lean_one, lean_two, out):
+def in_parts(x):
+    high = x.astype(bf16).astype(f32)
+    middle = (x - high).astype(bf16).astype(f32)
+    return high, middle, x - high - middle
+
+
+def finish(capacity, share, chips, data, slots, cot, conv, out):
     rows, count = data.shape[0], slots.shape[1]
     row = lax.broadcasted_iota(jnp.int32, (rows, count), 0)
     expert = row // (chips * share)
@@ -150,38 +174,59 @@
     key = expert * capacity + (chip % 2) * share + row % share
     hit = (key == slots[0:1, :]) | (key == slots[1:2, :])
     total = dot(jnp.where(hit, 1.0, 0.0).astype(bf16), data[...], TN)
-    stream = (cot[...].astype(f32) + total).astype(bf16)
-    out[0:count, :] = stream
-    wide = stream.astype(f32)
-    one = jnp.sum((wide * lean_one[...]).T, axis=0, keepdims=True)
-    two = jnp.sum((wide * lean_two[...]).T, axis=0, keepdims=True)
+    out[0:count, :] = (cot[...].astype(f32) + total).astype(bf16)
+    wide = conv[...].astype(f32)
     at = lax.broadcasted_iota(jnp.int32, (16, count), 0)
-    both = jnp.where((at // 2) % 2 == 0, one, two)
-    high = both.astype(bf16)
-    low = (both - high.astype(f32)).astype(bf16)
-    out[count : count + 16, :] = jnp.where(at % 2 == 0, high.astype(f32), low.astype(f32)).astype(bf16)
-
-
-def tail(total_channels, got, proj_t, hid_t, steep, centred, inverse, conv, stream, packed):
+    block = jnp.zeros((16, count), f32)
+    sums = jnp.sum(wide, axis=0, keepdims=True), jnp.sum(wide * wide, axis=0, keepdims=True)
+    for n, x in enumerate(in_parts(sums[0]) + in_parts(sums[1])):
+        block = jnp.where(at == n, x, block)
+    out[count : count + 16, :] = block.astype(bf16)
+
+
+def tail(total_channels, got, proj_t, conv, gain, xhat, centred, inverse, sums, stream, packed):
     pieces, count = got.shape[0], stream.shape[0]
     channels = proj_t.shape[0]
     lane = lax.broadcasted_iota(jnp.int32, (32, 2 * channels), 1)
+    parts = jnp.zeros((16, count), f32)
+    for j in range(pieces):
+        parts = parts + got[j, count : count + 16, :].astype(f32)
+    mean = (parts[0:1] + parts[1:2] + parts[2:3]) / total_channels
+    square = (parts[3:4] + parts[4:5] + parts[5:6]) / total_channels
+    scale = lax.rsqrt(square - mean * mean + norm_eps)
+    removed = (conv[...].astype(f32) - mean) * scale
+    normed = removed * gain[...]
+    sig = jax.nn.sigmoid(normed)
+    hidden = normed * sig
+    hid_t = jnp.concatenate([hidden, hidden]).T.astype(bf16)
     hidden_grad = jnp.zeros((channels, count), f32)
-    sums = jnp.zeros((16, count), f32)
     for j in range(pieces):
         part = got[j, :count, :]
         stream[:, j * LANES : (j + 1) * LANES] = part
         hidden_grad = hidden_grad + dot(proj_t[:, j * LANES : (j + 1) * LANES], part, NT)
-        sums = sums + got[j, count : count + 16, :].astype(f32)
-        outer = dot(part, hid_t[...], TN)
+        outer = dot(part, hid_t, TN)
         for u in range(2):
             first = outer[64 * u : 64 * u + 32]
             second = outer[64 * u + 32 : 64 * u + 64]
             packed[2 * j + u] = jnp.where(lane < channels, first, second).astype(bf16)
-    mean_one = (sums[0:1] + sums[1:2]) / total_channels
-    mean_two = (sums[2:3] + sums[3:4]) / total_channels
-    xhat = hidden_grad * steep[...]
-    conv[...] = inverse[...] * (xhat - mean_one - centred[...] * mean_two)
+    grown = hidden_grad * sig * (1.0 + normed * (1.0 - sig)) * gain[...]
+    xhat[...] = grown
+    centred[...] = removed
+    inverse[...] = scale
+    at = lax.broadcasted_iota(jnp.int32, (8, count), 0)
+    one = jnp.sum(grown, axis=0, keepdims=True)
+    two = jnp.sum(grown * removed, axis=0, keepdims=True)
+    block = jnp.where(at == 0, one, jnp.where(at == 1, two, 0.0))
+    for j in range(pieces):
+        sums[j] = block
+
+
+def normalise(total_channels, sums, xhat, centred, inverse, conv):
+    block = jnp.zeros(sums.shape[1:], f32)
+    for j in range(sums.shape[0]):
+        block = block + sums[j]
+    block = block / total_channels
+    conv[...] = inverse[...] * (xhat[...] - block[0:1] - centred[...] * block[1:2])
 
 
 def convolve(conv, rim, taps, gate, value, grad_value, grad_gate_in):
@@ -199,20 +244,6 @@
     sig = jax.nn.sigmoid(gate[...].astype(f32))
     grad_value[...] = (total * sig).astype(bf16)
     grad_gate_in[...] = (total * value[...].astype(f32) * sig * (1.0 - sig)).astype(bf16)
-
-
-def split_three(x):
-    high = lax.reduce_precision(x, 8, 7)
-    middle = lax.reduce_precision(x - high, 8, 7)
-    return jnp.stack([high, middle, x - high - middle]).astype(bf16)
-
-
-def norm_terms(conv, gain, mean, inverse):
-    centred = (conv.astype(f32) - mean) * inverse
-    normed = centred * gain
-    sig = jax.nn.sigmoid(normed)
-    steep = sig * (1.0 + normed * (1.0 - sig)) * gain
-    return centred, normed * sig, steep
 
 
 def body(
@@ -246,26 +277,22 @@
     cols = width // tp_count
     hid = w_gate.shape[2]
 
-    def halves(x, axis):
-        shape = x.shape[:axis] + (chips, 2, cols) + x.shape[axis + 1 :]
-        x = x.reshape(shape)
-        mine = lax.dynamic_index_in_dim(x, core, axis + 1, keepdims=False)
-        other = lax.dynamic_index_in_dim(x, 1 - core, axis + 1, keepdims=False)
-        flat = shape[:axis] + (half,) + shape[axis + 3 :]
-        return mine.reshape(flat), other.reshape(flat)
-
     channels = conv_result.shape[0]
     channel_total = channels * tp_count
     positions = conv_result.shape[1]
-    proj_t = w_proj.T
-    proj_out = proj_t.reshape(channels, tp_count, cols).transpose(1, 0, 2)
-    proj_in = lax.all_to_all(proj_out, TP, 0, 0, tiled=True)
-
-    w_own = jnp.stack([w_gate[0], w_up[0], w_down[0].T])
-    w_own = jnp.concatenate(halves(w_own, 1), axis=1)
+
+    ids = jnp.stack([core, chip % 2]).astype(jnp.int32)
+    w_own = local_kernel(
+        functools.partial(pack_weights, chips),
+        shaped((3, width, hid), bf16),
+        ids,
+        w_gate[0],
+        w_up[0],
+        w_down[0],
+        specs=[SMEM, VMEM, VMEM, VMEM],
+    )
     w_far = swap_chips(w_own)
 
-    ids = jnp.stack([core, chip % 2]).astype(jnp.int32)
     sent, slots = local_kernel(
         functools.partial(prepare, experts, capacity, share, chips),
         (shaped((experts * share, width), bf16), shaped((top, tokens), jnp.int32)),
@@ -276,7 +303,6 @@
         out_cot,
         specs=[SMEM, VMEM, VMEM, VMEM, VMEM],
     )
-    sent, proj_in, w_own = lax.optimization_barrier((sent, proj_in, w_own))
     mine = lax.all_to_all(sent.reshape(experts, share, width), "sp", 0, 0, tiled=True)
     mine = mine.reshape(rows, width)
     other = swap_cores(mine)
@@ -300,11 +326,7 @@
     back = (back_mine + from_core.astype(f32)).astype(bf16)
     back = back.reshape(sp_count, share, chips, cols).transpose(0, 2, 1, 3)
     back = back.reshape(sp_count * chips, share, cols)
-    gains = jnp.pad(split_three(channel_norm_gain), ((0, 5), (0, positions - channels)))
-    conv_out = jnp.concatenate([conv_result, gains])
-    back, own_acts, far_acts, conv_out = lax.optimization_barrier(
-        (back, own_acts, far_acts, conv_out)
-    )
+    back, own_acts, far_acts = lax.optimization_barrier((back, own_acts, far_acts))
     returned = lax.all_to_all(back, ("sp", "chip"), 0, 0, tiled=True)
 
     far_acts = swap_chips(far_acts)
@@ -323,23 +345,6 @@
     )
     grad_gate, grad_up, grad_down = gate[None], up[None], down[None]
 
-    every = lax.all_gather(conv_out, TP)
-    all_conv = every[:, :channels].reshape(channel_total, positions).astype(f32)
-    all_gain = jnp.sum(every[:, channels : channels + 3, :channels].astype(f32), axis=1)
-    all_gain = all_gain.reshape(channel_total, 1)
-    mean = jnp.sum(all_conv, axis=0) / channel_total
-    variance = jnp.sum(all_conv * all_conv, axis=0) / channel_total - mean * mean
-    inverse = lax.rsqrt(variance + norm_eps)
-    all_centred, _, all_steep = norm_terms(all_conv, all_gain, mean, inverse)
-    centred, hidden, steep = norm_terms(
-        conv_result, channel_norm_gain[:, None], mean, inverse
-    )
-    hidden = hidden.astype(bf16)
-
-    proj_in = proj_in.reshape(channel_total, cols)
-    lean_one = dot(all_steep.astype(bf16), proj_in, TN)
-    lean_two = dot((all_steep * all_centred).astype(bf16), proj_in, TN)
-
     cot_cols = lax.dynamic_slice_in_dim(out_cot, tp * cols, cols, 1)
     payload = local_kernel(
         functools.partial(finish, capacity, share, chips),
@@ -347,24 +352,33 @@
         returned.reshape(experts * chips * share, cols),
         slots,
         cot_cols,
-        lean_one,
-        lean_two,
+        conv_result,
     )
     got = lax.all_gather(payload, TP)
 
-    grad_conv, grad_stream, packed = local_kernel(
+    xhat, centred, inverse, sums, grad_stream, packed = local_kernel(
         functools.partial(tail, channel_total),
         (
             shaped((channels, positions), f32),
+            shaped((channels, positions), f32),
+            shaped((1, positions), f32),
+            shaped((tp_count, 8, positions), f32),
             shaped((tokens, width), bf16),
             shaped((sp_count, 32, 2 * channels), bf16),
         ),
         got,
-        proj_t,
-        jnp.concatenate([hidden, hidden]).T,
-        steep,
+        w_proj.T,
+        conv_result,
+        channel_norm_gain[:, None],
+    )
+    sums = lax.all_to_all(sums, TP, 0, 0, tiled=True)
+    grad_conv = local_kernel(
+        functools.partial(normalise, channel_total),
+        shaped((channels, positions), f32),
+        sums,
+        xhat,
         centred,
-        inverse[None],
+        inverse,
     )
 
     packed = lax.all_to_all(packed, "sp", 0, 0, tiled=True)

time: 192 us -> 173 us (0.901)
  waiting for transfers between devices: 71.5 us -> 50.5 us
  Pallas kernels: 14.5 us -> 18.5 us
  matrix products: 2.9 us -> 0 us
  blocking collectives: 33.7 us -> 31.2 us
  local copies, waits for them, and re-layouts: 6.16 us -> 8.18 us
    all_gather x1 -> x0, blocking collectives: 15.2 us -> none  [body(): every = lax.all_gather(conv_out, TP)]
    all_to_all x0 -> x1, blocking collectives: none -> 12.3 us  [body(): sums = lax.all_to_all(sums, TP, 0, 0, tiled=True)]
    all_to_all x1 -> x0, starting transfers between devices: 10.8 us -> none  [body(): proj_in = lax.all_to_all(proj_out, TP, 0, 0, tiled=True)]
    ppermute x3, waiting for transfers between devices: 23.1 us -> 15.6 us  [swap_chips(): return lax.ppermute(value, 'chip', [(k, k ^ 1) for k in range(count)])]
    all_to_all x1 -> x0, waiting for transfers between devices: 6.28 us -> none  [body(): proj_in = lax.all_to_all(proj_out, TP, 0, 0, tiled=True)]
    unnamed x31 -> x39, local copies, waits for them, and re-layouts: 2.07 us -> 7.25 us
    all_to_all x1, waiting for transfers between devices: 25.3 us -> 21.1 us  [body(): lax.all_to_all(sent.reshape(experts, share, width), 'sp', 0, 0, tiled=True)]
    pallas_call x6 -> x8, Pallas kernels: 14.5 us -> 18.5 us  [local_kernel(): pl.pallas_call(body, out_shape=outs, in_specs=[VMEM] * len(args) if specs...]
  transfers between devices with their start and end apart: 11 -> 10, of which waited for: 6 -> 5; matrix products, arithmetic and copies ran while one was open for 4% -> 2% of each run, Pallas kernels for 8% -> 7%
where the time goes in v2:
time: 173 us; the launch traced here: 171 us
  starting transfers between devices  59 us (34%)
  waiting for transfers between devices  50.5 us (29%)
  blocking collectives  31.2 us (18%)
  Pallas kernels  18.5 us (11%)
  local copies, waits for them, and re-layouts  8.18 us (5%)
  other arithmetic  2.65 us (2%)
    all_to_all x1, waiting for transfers between devices, body(): lax.all_to_all(sent.reshape(experts, share, width), 'sp', 0, 0, tiled=True)  21.1 us
    all_to_all x1, starting transfers between devices, body(): returned = lax.all_to_all(back, ('sp', 'chip'), 0, 0, tiled=True)  18.9 us
    all_gather x1, blocking collectives, body(): got = lax.all_gather(payload, TP)  18.9 us
    pallas_call x8, Pallas kernels, local_kernel(): pl.pallas_call(body, out_shape=outs, in_specs=[VMEM] * len(args) if specs...  18.5 us
    ppermute x3, waiting for transfers between devices, swap_chips(): return lax.ppermute(value, 'chip', [(k, k ^ 1) for k in range(count)])  15.6 us
    all_to_all x1, starting transfers between devices, body(): lax.all_to_all(sent.reshape(experts, share, width), 'sp', 0, 0, tiled=True)  13.8 us
    all_to_all x1, waiting for transfers between devices, body(): returned = lax.all_to_all(back, ('sp', 'chip'), 0, 0, tiled=True)  13.8 us
    all_to_all x1, blocking collectives, body(): sums = lax.all_to_all(sums, TP, 0, 0, tiled=True)  12.3 us
  transfers between devices with their start and end apart: 10, of which 5 were waited for; matrix products, arithmetic and copies ran while one was open for 2% of the time, Pallas kernels for 7%

profile of v2, /device:TPU:1, one launch (start us, length us, event | category | flops | bytes accessed | tf_op | source)
XLA Modules:
  0.0 170.8 jit_solution(9411631824913871532)
XLA Ops:
  0.7 1.0 copy-done.2
  1.8 1.0 copy-done.3
  4.2 2.2 %shard_map.180 = (bf16[256,2048]{1,0:T(8,128)(2,1)}, s32[2,128]{1,0:T(2,128)S(1)}) custom-call(s32[2]{0:T(128)S(1)} %pad_add_fusion.ids, s32[2,128]{1,0:T(2,128)S(1)} %bitcast.32, f32[2,128]{1,0:T(2,128)S(1)} %bitcast.33, bf16[128,2048]{1,0:T(8,128)(2,1)S(1)} %copy-done.3, bf16[128,2048]{1,0:T(8,128)(2,1)S(1)} %copy-done.2), custom_call_target="tpu_custom_call" | custom-call | flops 1000000000 | bytes 1050632 | tf_op jit(solution)/shard_map/pallas_call | solution.py:36
  6.3 13.8 %all-to-all-start = ((bf16[32,8,2048]{2,1,0:T(8,128)(2,1)}), bf16[32,8,2048]{2,1,0:T(8,128)(2,1)S(1)}, u32[]{:S(2)}, u32[]{:S(2)}) async-start(bf16[32,8,2048]{2,1,0:T(8,128)(2,1)} %bitcast.4), calls=%async_computation | async-start | bytes 2097152 | tf_op jit(solution)/shard_map/all_to_all | solution.py:306
  20.2 1.9 %shard_map.181.own = bf16[3,2048,128]{2,1,0:T(8,128)(2,1)} custom-call(s32[2]{0:T(128)S(1)} %pad_add_fusion.ids, bf16[2048,128]{1,0:T(8,128)(2,1)S(1)} %bitcast.28, bf16[2048,128]{1,0:T(8,128)(2,1)S(1)} %bitcast.29, bf16[128,2048]{1,0:T(8,128)(2,1)S(1)} %bitcast.30), custom_call_target="tpu_custom_call" | custom-call | flops 1000000000 | bytes 1572872 | tf_op jit(solution)/shard_map/pallas_call | solution.py:36
  22.1 3.2 %collective-permute-start.3 = (bf16[3,2048,128]{2,1,0:T(8,128)(2,1)}, bf16[3,2048,128]{2,1,0:T(8,128)(2,1)}, u32[]{:S(2)}, u32[]{:S(2)}) collective-permute-start(bf16[3,2048,128]{2,1,0:T(8,128)(2,1)} %shard_map.181.own), channel_id=1, source_target_pairs={{0,2},{2,0},{4,6},{6,4},{8,10},{10,8},{12,14},{14,12},{1,3},{3,1},... | collective-permute-start | bytes 4718600 | tf_op jit(solution)/shard_map/ppermute | solution.py:56
  25.3 21.1 %all-to-all-done = bf16[32,8,2048]{2,1,0:T(8,128)(2,1)S(1)} async-done(((bf16[32,8,2048]{2,1,0:T(8,128)(2,1)}), bf16[32,8,2048]{2,1,0:T(8,128)(2,1)S(1)}, u32[]{:S(2)}, u32[]{:S(2)}) %all-to-all-start) | async-done | bytes 1048608 | tf_op jit(solution)/shard_map/all_to_all | solution.py:306
  46.4 4.7 %collective-permute-start = (bf16[256,2048]{1,0:T(8,128)(2,1)S(1)}, bf16[256,2048]{1,0:T(8,128)(2,1)S(1)}, u32[]{:S(2)}, u32[]{:S(2)}) collective-permute-start(bf16[256,2048]{1,0:T(8,128)(2,1)S(1)} %bitcast.22), channel_id=1, source_target_pairs={{0,1},{1,0},{2,3},{3,2},{4,5},{5,4},{6,7},{7,6},{8,9},{9,8},{10,11... | collective-permute-start | bytes 3145736 | tf_op jit(solution)/shard_map/ppermute | solution.py:51
  51.1 8.2 %collective-permute-done.3.far = bf16[3,2048,128]{2,1,0:T(8,128)(2,1)} collective-permute-done((bf16[3,2048,128]{2,1,0:T(8,128)(2,1)}, bf16[3,2048,128]{2,1,0:T(8,128)(2,1)}, u32[]{:S(2)}, u32[]{:S(2)}) %collective-permute-start.3) | collective-permute-done | bytes 1572896 | tf_op jit(solution)/shard_map/ppermute | solution.py:56
  59.3 4.9 %shard_map.182 = (bf16[3,256,128]{2,1,0:T(8,128)(2,1)S(1)}, bf16[3,256,128]{2,1,0:T(8,128)(2,1)S(1)}, f32[256,1024]{1,0:T(8,128)S(1)}, bf16[256,1024]{1,0:T(8,128)(2,1)S(1)}) custom-call(bf16[256,2048]{1,0:T(8,128)(2,1)S(1)} %bitcast.23, bf16[256,2048]{1,0:T(8,128)(2,1)S(1)} %collective-permute-done.other, bf16[3,2048,128]{2,1,0:T(8,128)(2,1)} %shard_map.181.own, ...), custom_call_target="tpu_custom_call" | custom-call | flops 1000000000 | bytes 5242880 | tf_op jit(solution)/shard_map/pallas_call | solution.py:36
  64.3 3.7 %collective-permute-start.4 = (bf16[256,1024]{1,0:T(8,128)(2,1)S(1)}, bf16[256,1024]{1,0:T(8,128)(2,1)S(1)}, u32[]{:S(2)}, u32[]{:S(2)}) collective-permute-start(bf16[256,1024]{1,0:T(8,128)(2,1)S(1)} %get-tuple-element.29), channel_id=1, source_target_pairs={{0,1},{1,0},{2,3},{3,2},{4,5},{5,4},{6,7},{7,6},{8,9},{9,8},{10,11... | collective-permute-start | bytes 1572872 | tf_op jit(solution)/shard_map/ppermute | solution.py:51
  68.0 3.2 %collective-permute-start.1 = (bf16[256,2048]{1,0:T(8,128)(2,1)S(1)}, bf16[256,2048]{1,0:T(8,128)(2,1)S(1)}, u32[]{:S(2)}, u32[]{:S(2)}) collective-permute-start(bf16[256,2048]{1,0:T(8,128)(2,1)S(1)} %bitcast.24), channel_id=1, source_target_pairs={{0,2},{2,0},{4,6},{6,4},{8,10},{10,8},{12,14},{14,12},{1,3},{3,1},... | collective-permute-start | bytes 3145736 | tf_op jit(solution)/shard_map/ppermute | solution.py:56
  71.2 0.9 add_convert_fusion
  72.2 18.9 %all-to-all-start.1 = ((bf16[256,8,128]{2,1,0:T(8,128)(2,1)}), bf16[256,8,128]{2,1,0:T(8,128)(2,1)}, u32[]{:S(2)}, u32[]{:S(2)}) async-start(bf16[256,8,128]{2,1,0:T(8,128)(2,1)} %bitcast.34), calls=%async_computation.1 | async-start | bytes 1048576 | tf_op jit(solution)/shard_map/all_to_all | solution.py:330
  91.1 6.4 %collective-permute-done.1.far = bf16[256,2048]{1,0:T(8,128)(2,1)S(1)} collective-permute-done((bf16[256,2048]{1,0:T(8,128)(2,1)S(1)}, bf16[256,2048]{1,0:T(8,128)(2,1)S(1)}, u32[]{:S(2)}, u32[]{:S(2)}) %collective-permute-start.1) | collective-permute-done | bytes 1048608 | tf_op jit(solution)/shard_map/ppermute | solution.py:56
  97.5 3.1 %collective-permute-start.2 = (bf16[256,2048]{1,0:T(8,128)(2,1)S(1)}, bf16[256,2048]{1,0:T(8,128)(2,1)}, u32[]{:S(2)}, u32[]{:S(2)}) collective-permute-start(bf16[256,2048]{1,0:T(8,128)(2,1)S(1)} %collective-permute-done.1.far), channel_id=1, source_target_pairs={{0,1},{1,0},{2,3},{3,2},{4,5},{5,4},{6,7},{7,6},{8,9},{9,8},{10,11... | collective-permute-start | bytes 3145736 | tf_op jit(solution)/shard_map/ppermute | solution.py:51
  100.8 0.8 constant_dynamic-slice_fusion.cot
  101.5 13.8 %all-to-all-done.1 = bf16[256,8,128]{2,1,0:T(8,128)(2,1)} async-done(((bf16[256,8,128]{2,1,0:T(8,128)(2,1)}), bf16[256,8,128]{2,1,0:T(8,128)(2,1)}, u32[]{:S(2)}, u32[]{:S(2)}) %all-to-all-start.1) | async-done | bytes 524320 | tf_op jit(solution)/shard_map/all_to_all | solution.py:330
  115.3 1.9 %shard_map.184 = bf16[144,128]{1,0:T(8,128)(2,1)S(1)} custom-call(bf16[2048,128]{1,0:T(8,128)(2,1)} %bitcast.15.data, s32[2,128]{1,0:T(2,128)S(1)} %get-tuple-element.38.slots, bf16[128,128]{1,0:T(8,128)(2,1)S(1)} %constant_dynamic-slice_fusion.cot, bf16[64,128]{1,0:T(8,128)(2,1)S(1)} %copy-done.9), custom_call_target="tpu_custom_call" | custom-call | flops 1000000000 | bytes 574464 | tf_op jit(solution)/shard_map/pallas_call | solution.py:36
  117.3 18.9 %all-gather = bf16[2304,128]{1,0:T(8,128)(2,1)S(1)} all-gather(bf16[144,128]{1,0:T(8,128)(2,1)S(1)} %shard_map.184), channel_id=2, replica_groups=mesh['sp'=32,'chip'=8,'core'=2] {'chip','core'}, dimensions={0}, use_global_device_ids=true | all-gather | bytes 626688 | tf_op jit(solution)/shard_map/all_gather | solution.py:357
  136.1 1.5 shard_map.185
  137.6 12.3 %all_to_all.20.sums = f32[16,8,128]{2,1,0:T(8,128)} all-to-all(f32[16,8,128]{2,1,0:T(8,128)S(1)} %get-tuple-element.41), channel_id=1, replica_groups=mesh['sp'=32,'chip'=8,'core'=2] {'chip','core'}, dimensions={0} | all-to-all | bytes 131072 | tf_op jit(solution)/shard_map/all_to_all | solution.py:374
  149.9 4.6 %all-to-all-start.2 = ((bf16[32,32,128]{2,1,0:T(8,128)(2,1)}), bf16[32,32,128]{2,1,0:T(8,128)(2,1)}, u32[]{:S(2)}, u32[]{:S(2)}) async-start(bf16[32,32,128]{2,1,0:T(8,128)(2,1)} %get-tuple-element.40), calls=%async_computation.2 | async-start | bytes 524288 | tf_op jit(solution)/shard_map/all_to_all | solution.py:384
  154.5 2.1 %collective-permute-start.5 = (bf16[3,256,128]{2,1,0:T(8,128)(2,1)}, bf16[3,256,128]{2,1,0:T(8,128)(2,1)S(1)}, u32[]{:S(2)}, u32[]{:S(2)}) collective-permute-start(bf16[3,256,128]{2,1,0:T(8,128)(2,1)} %copy-done.8), channel_id=1, source_target_pairs={{0,2},{2,0},{4,6},{6,4},{8,10},{10,8},{12,14},{14,12},{1,3},{3,1},... | collective-permute-start | bytes 589832 | tf_op jit(solution)/shard_map/ppermute | solution.py:56
  156.6 1.4 copy.21
  158.0 0.8 copy-done
  158.9 0.8 copy-done.15
  160.5 1.6 collective-permute-start.6
  162.1 1.0 collective-permute-done.5.far_acts
  163.1 4.5 %shard_map.183 = (bf16[2048,128]{1,0:T(8,128)(2,1)}, bf16[2048,128]{1,0:T(8,128)(2,1)}, bf16[128,2048]{1,0:T(8,128)(2,1)}) custom-call(s32[2]{0:T(128)S(1)} %pad_add_fusion.ids, bf16[256,2048]{1,0:T(8,128)(2,1)S(1)} %bitcast.25, bf16[256,2048]{1,0:T(8,128)(2,1)S(1)} %collective-permute-done.other, bf16[256,2048]{1,0:T(8,128)(2,1)S(1)} %collective-permute-done.1.far, ...), custom_call_target="tpu_custom_call" | custom-call | flops 1000000000 | bytes 4587528 | tf_op jit(solution)/shard_map/pallas_call | solution.py:36
  167.6 1.6 shard_map.187
  169.1 1.0 convert_reduce_fusion
  (44 shorter events, 3.1 us)
Async XLA Ops:
  0.7 1.0 copy-start.2
  1.8 1.0 copy-start.3
  2.8 0.7 copy-start.12
  3.5 0.7 copy-start.13
  6.3 13.9 %copy-start.4 = (bf16[1,2048,128]{2,1,0:T(8,128)(2,1)S(1)}, bf16[1,2048,128]{2,1,0:T(8,128)(2,1)}, u32[]{:S(2)}) copy-start(bf16[1,2048,128]{2,1,0:T(8,128)(2,1)} %param.17) | copy-start | bytes 1572868
  6.3 13.9 %copy-start.5 = (bf16[1,2048,128]{2,1,0:T(8,128)(2,1)S(1)}, bf16[1,2048,128]{2,1,0:T(8,128)(2,1)}, u32[]{:S(2)}) copy-start(bf16[1,2048,128]{2,1,0:T(8,128)(2,1)} %param.18) | copy-start | bytes 1572868
  6.3 13.9 %copy-start.6 = (bf16[1,128,2048]{2,1,0:T(8,128)(2,1)S(1)}, bf16[1,128,2048]{2,1,0:T(8,128)(2,1)}, u32[]{:S(2)}) copy-start(bf16[1,128,2048]{2,1,0:T(8,128)(2,1)} %param.19) | copy-start | bytes 1572868
  6.3 40.0 %all-to-all-start = ((bf16[32,8,2048]{2,1,0:T(8,128)(2,1)}), bf16[32,8,2048]{2,1,0:T(8,128)(2,1)S(1)}, u32[]{:S(2)}, u32[]{:S(2)}) async-start(bf16[32,8,2048]{2,1,0:T(8,128)(2,1)} %bitcast.4), calls=%async_computation | async-start | bytes 2097152 | tf_op jit(solution)/shard_map/all_to_all | solution.py:306
  22.1 37.2 %collective-permute-start.3 = (bf16[3,2048,128]{2,1,0:T(8,128)(2,1)}, bf16[3,2048,128]{2,1,0:T(8,128)(2,1)}, u32[]{:S(2)}, u32[]{:S(2)}) collective-permute-start(bf16[3,2048,128]{2,1,0:T(8,128)(2,1)} %shard_map.181.own), channel_id=1, source_target_pairs={{0,2},{2,0},{4,6},{6,4},{8,10},{10,8},{12,14},{14,12},{1,3},{3,1},... | collective-permute-start | bytes 4718600 | tf_op jit(solution)/shard_map/ppermute | solution.py:56
  46.4 12.9 %collective-permute-start = (bf16[256,2048]{1,0:T(8,128)(2,1)S(1)}, bf16[256,2048]{1,0:T(8,128)(2,1)S(1)}, u32[]{:S(2)}, u32[]{:S(2)}) collective-permute-start(bf16[256,2048]{1,0:T(8,128)(2,1)S(1)} %bitcast.22), channel_id=1, source_target_pairs={{0,1},{1,0},{2,3},{3,2},{4,5},{5,4},{6,7},{7,6},{8,9},{9,8},{10,11... | collective-permute-start | bytes 3145736 | tf_op jit(solution)/shard_map/ppermute | solution.py:51
  64.3 7.9 %copy-start.8 = (bf16[3,256,128]{2,1,0:T(8,128)(2,1)}, bf16[3,256,128]{2,1,0:T(8,128)(2,1)S(1)}, u32[]{:S(2)}) copy-start(bf16[3,256,128]{2,1,0:T(8,128)(2,1)S(1)} %get-tuple-element.33) | copy-start | bytes 589828
  64.3 6.9 %collective-permute-start.4 = (bf16[256,1024]{1,0:T(8,128)(2,1)S(1)}, bf16[256,1024]{1,0:T(8,128)(2,1)S(1)}, u32[]{:S(2)}, u32[]{:S(2)}) collective-permute-start(bf16[256,1024]{1,0:T(8,128)(2,1)S(1)} %get-tuple-element.29), channel_id=1, source_target_pairs={{0,1},{1,0},{2,3},{3,2},{4,5},{5,4},{6,7},{7,6},{8,9},{9,8},{10,11... | collective-permute-start | bytes 1572872 | tf_op jit(solution)/shard_map/ppermute | solution.py:51
  68.0 29.5 %collective-permute-start.1 = (bf16[256,2048]{1,0:T(8,128)(2,1)S(1)}, bf16[256,2048]{1,0:T(8,128)(2,1)S(1)}, u32[]{:S(2)}, u32[]{:S(2)}) collective-permute-start(bf16[256,2048]{1,0:T(8,128)(2,1)S(1)} %bitcast.24), channel_id=1, source_target_pairs={{0,2},{2,0},{4,6},{6,4},{8,10},{10,8},{12,14},{14,12},{1,3},{3,1},... | collective-permute-start | bytes 3145736 | tf_op jit(solution)/shard_map/ppermute | solution.py:56
  71.2 29.4 %copy-start.18 = (f32[64]{0:T(128)S(1)}, f32[64]{0:T(128)}, u32[]{:S(2)}) copy-start(f32[64]{0:T(128)} %param.25) | copy-start | bytes 772
  71.2 44.1 %copy-start.9 = (bf16[64,128]{1,0:T(8,128)(2,1)S(1)}, bf16[64,128]{1,0:T(8,128)(2,1)}, u32[]{:S(2)}) copy-start(bf16[64,128]{1,0:T(8,128)(2,1)} %conv.3) | copy-start | bytes 49156
  72.2 43.1 %all-to-all-start.1 = ((bf16[256,8,128]{2,1,0:T(8,128)(2,1)}), bf16[256,8,128]{2,1,0:T(8,128)(2,1)}, u32[]{:S(2)}, u32[]{:S(2)}) async-start(bf16[256,8,128]{2,1,0:T(8,128)(2,1)} %bitcast.34), calls=%async_computation.1 | async-start | bytes 1048576 | tf_op jit(solution)/shard_map/all_to_all | solution.py:330
  97.5 65.6 %collective-permute-start.2 = (bf16[256,2048]{1,0:T(8,128)(2,1)S(1)}, bf16[256,2048]{1,0:T(8,128)(2,1)}, u32[]{:S(2)}, u32[]{:S(2)}) collective-permute-start(bf16[256,2048]{1,0:T(8,128)(2,1)S(1)} %collective-permute-done.1.far), channel_id=1, source_target_pairs={{0,1},{1,0},{2,3},{3,2},{4,5},{5,4},{6,7},{7,6},{8,9},{9,8},{10,11... | collective-permute-start | bytes 3145736 | tf_op jit(solution)/shard_map/ppermute | solution.py:51
  115.3 20.8 %copy-start.7 = (bf16[2048,64]{0,1:T(8,128)(2,1)S(1)}, bf16[2048,64]{0,1:T(8,128)(2,1)}, u32[]{:S(2)}) copy-start(bf16[2048,64]{0,1:T(8,128)(2,1)} %param.20) | copy-start | bytes 786436
  137.6 12.3 %copy-start.14 = (f32[64,128]{1,0:T(8,128)}, f32[64,128]{1,0:T(8,128)S(1)}, u32[]{:S(2)}) copy-start(f32[64,128]{1,0:T(8,128)S(1)} %get-tuple-element.42.xhat) | copy-start | bytes 98308
  137.6 12.3 %copy-start.16 = (f32[64,128]{1,0:T(8,128)}, f32[64,128]{1,0:T(8,128)S(1)}, u32[]{:S(2)}) copy-start(f32[64,128]{1,0:T(8,128)S(1)} %get-tuple-element.43.centred) | copy-start | bytes 98308
  149.9 19.2 %all-to-all-start.2 = ((bf16[32,32,128]{2,1,0:T(8,128)(2,1)}), bf16[32,32,128]{2,1,0:T(8,128)(2,1)}, u32[]{:S(2)}, u32[]{:S(2)}) async-start(bf16[32,32,128]{2,1,0:T(8,128)(2,1)} %get-tuple-element.40), calls=%async_computation.2 | async-start | bytes 524288 | tf_op jit(solution)/shard_map/all_to_all | solution.py:384
  154.5 8.5 %collective-permute-start.5 = (bf16[3,256,128]{2,1,0:T(8,128)(2,1)}, bf16[3,256,128]{2,1,0:T(8,128)(2,1)S(1)}, u32[]{:S(2)}, u32[]{:S(2)}) collective-permute-start(bf16[3,256,128]{2,1,0:T(8,128)(2,1)} %copy-done.8), channel_id=1, source_target_pairs={{0,2},{2,0},{4,6},{6,4},{8,10},{10,8},{12,14},{14,12},{1,3},{3,1},... | collective-permute-start | bytes 589832 | tf_op jit(solution)/shard_map/ppermute | solution.py:56
  158.0 0.8 copy-start
  158.9 0.8 copy-start.15
  159.6 0.8 copy-start.17
  160.4 7.1 %copy-start.1 = (f32[31,64]{0,1:T(8,128)S(1)}, f32[31,64]{0,1:T(8,128)}, u32[]{:S(2)}) copy-start(f32[31,64]{0,1:T(8,128)} %copy.21) | copy-start | bytes 23812
  160.4 7.1 %copy-start.10 = (bf16[64,128]{1,0:T(8,128)(2,1)S(1)}, bf16[64,128]{1,0:T(8,128)(2,1)}, u32[]{:S(2)}) copy-start(bf16[64,128]{1,0:T(8,128)(2,1)} %gate.1) | copy-start | bytes 49156
  160.4 7.1 %copy-start.11 = (bf16[64,128]{1,0:T(8,128)(2,1)S(1)}, bf16[64,128]{1,0:T(8,128)(2,1)}, u32[]{:S(2)}) copy-start(bf16[64,128]{1,0:T(8,128)(2,1)} %value.1) | copy-start | bytes 49156
  160.5 7.1 %collective-permute-start.6 = (f32[64,128]{1,0:T(8,128)S(1)}, f32[64,128]{1,0:T(8,128)S(1)}, u32[]{:S(2)}, u32[]{:S(2)}) collective-permute-start(f32[64,128]{1,0:T(8,128)S(1)} %shard_map.186.conv), channel_id=1, source_target_pairs={{16,0},{32,16},{48,32},{64,48},{80,64},{96,80},{112,96},{128,112},... | collective-permute-start | bytes 98312 | tf_op jit(solution)/shard_map/ppermute | solution.py:388

commit v3 on v2

--- a/solution.py
+++ b/solution.py
@@ -166,7 +166,7 @@
     return high, middle, x - high - middle
 
 
-def finish(capacity, share, chips, data, slots, cot, conv, out):
+def finish(capacity, share, chips, ids, data, slots, cot, conv, out):
     rows, count = data.shape[0], slots.shape[1]
     row = lax.broadcasted_iota(jnp.int32, (rows, count), 0)
     expert = row // (chips * share)
@@ -174,7 +174,8 @@
     key = expert * capacity + (chip % 2) * share + row % share
     hit = (key == slots[0:1, :]) | (key == slots[1:2, :])
     total = dot(jnp.where(hit, 1.0, 0.0).astype(bf16), data[...], TN)
-    out[0:count, :] = (cot[...].astype(f32) + total).astype(bf16)
+    at = pl.ds(pl.multiple_of(ids[2] * LANES, LANES), LANES)
+    out[0:count, :] = (cot[:, at].astype(f32) + total).astype(bf16)
     wide = conv[...].astype(f32)
     at = lax.broadcasted_iota(jnp.int32, (16, count), 0)
     block = jnp.zeros((16, count), f32)
@@ -265,7 +266,6 @@
     chips = lax.axis_size("chip")
     core = lax.axis_index("core")
     chip = lax.axis_index("chip")
-    tp = 2 * chip + core
     tp_count = 2 * chips
     experts = w_gate.shape[0] * sp_count
     tokens, width = stream_in.shape
@@ -281,7 +281,7 @@
     channel_total = channels * tp_count
     positions = conv_result.shape[1]
 
-    ids = jnp.stack([core, chip % 2]).astype(jnp.int32)
+    ids = jnp.stack([core, chip % 2, 2 * chip + core]).astype(jnp.int32)
     w_own = local_kernel(
         functools.partial(pack_weights, chips),
         shaped((3, width, hid), bf16),
@@ -345,14 +345,15 @@
     )
     grad_gate, grad_up, grad_down = gate[None], up[None], down[None]
 
-    cot_cols = lax.dynamic_slice_in_dim(out_cot, tp * cols, cols, 1)
     payload = local_kernel(
         functools.partial(finish, capacity, share, chips),
         shaped((tokens + 16, cols), bf16),
+        ids,
         returned.reshape(experts * chips * share, cols),
         slots,
-        cot_cols,
+        out_cot,
         conv_result,
+        specs=[SMEM] + [VMEM] * 4,
     )
     got = lax.all_gather(payload, TP)
 

time: 173 us -> 174 us (level)
    unnamed x39 -> x41, local copies, waits for them, and re-layouts: 7.25 us -> 8.31 us
  transfers between devices with their start and end apart: 10 -> 10, of which waited for: 5 -> 5; matrix products, arithmetic and copies ran while one was open for 2% -> 1% of each run, Pallas kernels for 7% -> 7%
where the time goes in v3:
time: 174 us; the launch traced here: 172 us
  starting transfers between devices  59 us (34%)
  waiting for transfers between devices  51.3 us (29%)
  blocking collectives  31.2 us (18%)
  Pallas kernels  18.4 us (11%)
  local copies, waits for them, and re-layouts  8.48 us (5%)
  other arithmetic  2.65 us (2%)
    all_to_all x1, waiting for transfers between devices, body(): lax.all_to_all(sent.reshape(experts, share, width), 'sp', 0, 0, tiled=True)  21.1 us
    all_to_all x1, starting transfers between devices, body(): returned = lax.all_to_all(back, ('sp', 'chip'), 0, 0, tiled=True)  18.9 us
    all_gather x1, blocking collectives, body(): got = lax.all_gather(payload, TP)  18.8 us
    pallas_call x8, Pallas kernels, local_kernel(): pl.pallas_call(body, out_shape=outs, in_specs=[VMEM] * len(args) if specs...  18.4 us
    ppermute x3, waiting for transfers between devices, swap_chips(): return lax.ppermute(value, 'chip', [(k, k ^ 1) for k in range(count)])  15.6 us
    all_to_all x1, waiting for transfers between devices, body(): returned = lax.all_to_all(back, ('sp', 'chip'), 0, 0, tiled=True)  14.6 us
    all_to_all x1, starting transfers between devices, body(): lax.all_to_all(sent.reshape(experts, share, width), 'sp', 0, 0, tiled=True)  13.8 us
    all_to_all x1, blocking collectives, body(): sums = lax.all_to_all(sums, TP, 0, 0, tiled=True)  12.3 us
  transfers between devices with their start and end apart: 10, of which 5 were waited for; matrix products, arithmetic and copies ran while one was open for 1% of the time, Pallas kernels for 7%

profile of v3, /device:TPU:1, one launch (start us, length us, event | category | flops | bytes accessed | tf_op | source)
XLA Modules:
  0.0 171.9 jit_solution(17466610090176501189)
XLA Ops:
  0.7 1.0 copy-done.2
  1.8 1.0 copy-done.6
  4.2 2.2 %shard_map.180 = (bf16[256,2048]{1,0:T(8,128)(2,1)}, s32[2,128]{1,0:T(2,128)S(1)}) custom-call(s32[3]{0:T(128)S(1)} %pad_add_fusion.ids, s32[2,128]{1,0:T(2,128)S(1)} %bitcast.33, f32[2,128]{1,0:T(2,128)S(1)} %bitcast.34, bf16[128,2048]{1,0:T(8,128)(2,1)S(1)} %copy-done.2, bf16[128,2048]{1,0:T(8,128)(2,1)S(1)} %copy-done.6), custom_call_target="tpu_custom_call" | custom-call | flops 1000000000 | bytes 1050636 | tf_op jit(solution)/shard_map/pallas_call | solution.py:36
  6.3 13.8 %all-to-all-start = ((bf16[32,8,2048]{2,1,0:T(8,128)(2,1)}), bf16[32,8,2048]{2,1,0:T(8,128)(2,1)S(1)}, u32[]{:S(2)}, u32[]{:S(2)}) async-start(bf16[32,8,2048]{2,1,0:T(8,128)(2,1)} %bitcast.5), calls=%async_computation | async-start | bytes 2097152 | tf_op jit(solution)/shard_map/all_to_all | solution.py:306
  20.2 1.9 %shard_map.181.own = bf16[3,2048,128]{2,1,0:T(8,128)(2,1)} custom-call(s32[3]{0:T(128)S(1)} %pad_add_fusion.ids, bf16[2048,128]{1,0:T(8,128)(2,1)S(1)} %bitcast.29, bf16[2048,128]{1,0:T(8,128)(2,1)S(1)} %bitcast.30, bf16[128,2048]{1,0:T(8,128)(2,1)S(1)} %bitcast.31), custom_call_target="tpu_custom_call" | custom-call | flops 1000000000 | bytes 1572876 | tf_op jit(solution)/shard_map/pallas_call | solution.py:36
  22.1 3.2 %collective-permute-start.3 = (bf16[3,2048,128]{2,1,0:T(8,128)(2,1)}, bf16[3,2048,128]{2,1,0:T(8,128)(2,1)}, u32[]{:S(2)}, u32[]{:S(2)}) collective-permute-start(bf16[3,2048,128]{2,1,0:T(8,128)(2,1)} %shard_map.181.own), channel_id=1, source_target_pairs={{0,2},{2,0},{4,6},{6,4},{8,10},{10,8},{12,14},{14,12},{1,3},{3,1},... | collective-permute-start | bytes 4718600 | tf_op jit(solution)/shard_map/ppermute | solution.py:56
  25.3 21.1 %all-to-all-done = bf16[32,8,2048]{2,1,0:T(8,128)(2,1)S(1)} async-done(((bf16[32,8,2048]{2,1,0:T(8,128)(2,1)}), bf16[32,8,2048]{2,1,0:T(8,128)(2,1)S(1)}, u32[]{:S(2)}, u32[]{:S(2)}) %all-to-all-start) | async-done | bytes 1048608 | tf_op jit(solution)/shard_map/all_to_all | solution.py:306
  46.4 4.7 %collective-permute-start = (bf16[256,2048]{1,0:T(8,128)(2,1)S(1)}, bf16[256,2048]{1,0:T(8,128)(2,1)S(1)}, u32[]{:S(2)}, u32[]{:S(2)}) collective-permute-start(bf16[256,2048]{1,0:T(8,128)(2,1)S(1)} %bitcast.23), channel_id=1, source_target_pairs={{0,1},{1,0},{2,3},{3,2},{4,5},{5,4},{6,7},{7,6},{8,9},{9,8},{10,11... | collective-permute-start | bytes 3145736 | tf_op jit(solution)/shard_map/ppermute | solution.py:51
  51.1 8.2 %collective-permute-done.3.far = bf16[3,2048,128]{2,1,0:T(8,128)(2,1)} collective-permute-done((bf16[3,2048,128]{2,1,0:T(8,128)(2,1)}, bf16[3,2048,128]{2,1,0:T(8,128)(2,1)}, u32[]{:S(2)}, u32[]{:S(2)}) %collective-permute-start.3) | collective-permute-done | bytes 1572896 | tf_op jit(solution)/shard_map/ppermute | solution.py:56
  59.3 4.9 %shard_map.182 = (bf16[3,256,128]{2,1,0:T(8,128)(2,1)S(1)}, bf16[3,256,128]{2,1,0:T(8,128)(2,1)S(1)}, f32[256,1024]{1,0:T(8,128)S(1)}, bf16[256,1024]{1,0:T(8,128)(2,1)S(1)}) custom-call(bf16[256,2048]{1,0:T(8,128)(2,1)S(1)} %bitcast.24, bf16[256,2048]{1,0:T(8,128)(2,1)S(1)} %collective-permute-done.other, bf16[3,2048,128]{2,1,0:T(8,128)(2,1)} %shard_map.181.own, ...), custom_call_target="tpu_custom_call" | custom-call | flops 1000000000 | bytes 5242880 | tf_op jit(solution)/shard_map/pallas_call | solution.py:36
  64.3 3.7 %collective-permute-start.4 = (bf16[256,1024]{1,0:T(8,128)(2,1)S(1)}, bf16[256,1024]{1,0:T(8,128)(2,1)S(1)}, u32[]{:S(2)}, u32[]{:S(2)}) collective-permute-start(bf16[256,1024]{1,0:T(8,128)(2,1)S(1)} %get-tuple-element.29), channel_id=1, source_target_pairs={{0,1},{1,0},{2,3},{3,2},{4,5},{5,4},{6,7},{7,6},{8,9},{9,8},{10,11... | collective-permute-start | bytes 1572872 | tf_op jit(solution)/shard_map/ppermute | solution.py:51
  68.0 3.2 %collective-permute-start.1 = (bf16[256,2048]{1,0:T(8,128)(2,1)S(1)}, bf16[256,2048]{1,0:T(8,128)(2,1)S(1)}, u32[]{:S(2)}, u32[]{:S(2)}) collective-permute-start(bf16[256,2048]{1,0:T(8,128)(2,1)S(1)} %bitcast.25), channel_id=1, source_target_pairs={{0,2},{2,0},{4,6},{6,4},{8,10},{10,8},{12,14},{14,12},{1,3},{3,1},... | collective-permute-start | bytes 3145736 | tf_op jit(solution)/shard_map/ppermute | solution.py:56
  71.2 0.9 add_convert_fusion
  72.2 18.9 %all-to-all-start.1 = ((bf16[256,8,128]{2,1,0:T(8,128)(2,1)}), bf16[256,8,128]{2,1,0:T(8,128)(2,1)}, u32[]{:S(2)}, u32[]{:S(2)}) async-start(bf16[256,8,128]{2,1,0:T(8,128)(2,1)} %bitcast.35), calls=%async_computation.1 | async-start | bytes 1048576 | tf_op jit(solution)/shard_map/all_to_all | solution.py:330
  91.1 6.4 %collective-permute-done.1.far = bf16[256,2048]{1,0:T(8,128)(2,1)S(1)} collective-permute-done((bf16[256,2048]{1,0:T(8,128)(2,1)S(1)}, bf16[256,2048]{1,0:T(8,128)(2,1)S(1)}, u32[]{:S(2)}, u32[]{:S(2)}) %collective-permute-start.1) | collective-permute-done | bytes 1048608 | tf_op jit(solution)/shard_map/ppermute | solution.py:56
  97.5 3.1 %collective-permute-start.2 = (bf16[256,2048]{1,0:T(8,128)(2,1)S(1)}, bf16[256,2048]{1,0:T(8,128)(2,1)}, u32[]{:S(2)}, u32[]{:S(2)}) collective-permute-start(bf16[256,2048]{1,0:T(8,128)(2,1)S(1)} %collective-permute-done.1.far), channel_id=1, source_target_pairs={{0,1},{1,0},{2,3},{3,2},{4,5},{5,4},{6,7},{7,6},{8,9},{9,8},{10,11... | collective-permute-start | bytes 3145736 | tf_op jit(solution)/shard_map/ppermute | solution.py:51
  100.8 14.6 %all-to-all-done.1 = bf16[256,8,128]{2,1,0:T(8,128)(2,1)} async-done(((bf16[256,8,128]{2,1,0:T(8,128)(2,1)}), bf16[256,8,128]{2,1,0:T(8,128)(2,1)}, u32[]{:S(2)}, u32[]{:S(2)}) %all-to-all-start.1) | async-done | bytes 524320 | tf_op jit(solution)/shard_map/all_to_all | solution.py:330
  115.3 1.0 copy-done.7
  116.4 1.9 %shard_map.184 = bf16[144,128]{1,0:T(8,128)(2,1)S(1)} custom-call(s32[3]{0:T(128)S(1)} %pad_add_fusion.ids, bf16[2048,128]{1,0:T(8,128)(2,1)} %bitcast.16.data, s32[2,128]{1,0:T(2,128)S(1)} %get-tuple-element.38.slots, bf16[128,2048]{1,0:T(8,128)(2,1)S(1)} %copy-done.7, bf16[64,128]{1,0:T(8,128)(2,1)S(1)} %copy-done.10), custom_call_target="tpu_custom_call" | custom-call | flops 1000000000 | bytes 1065996 | tf_op jit(solution)/shard_map/pallas_call | solution.py:36
  118.3 18.8 %all-gather = bf16[2304,128]{1,0:T(8,128)(2,1)S(1)} all-gather(bf16[144,128]{1,0:T(8,128)(2,1)S(1)} %shard_map.184), channel_id=2, replica_groups=mesh['sp'=32,'chip'=8,'core'=2] {'chip','core'}, dimensions={0}, use_global_device_ids=true | all-gather | bytes 626688 | tf_op jit(solution)/shard_map/all_gather | solution.py:358
  137.1 1.5 shard_map.185
  138.6 12.3 %all_to_all.20.sums = f32[16,8,128]{2,1,0:T(8,128)} all-to-all(f32[16,8,128]{2,1,0:T(8,128)S(1)} %get-tuple-element.41), channel_id=1, replica_groups=mesh['sp'=32,'chip'=8,'core'=2] {'chip','core'}, dimensions={0} | all-to-all | bytes 131072 | tf_op jit(solution)/shard_map/all_to_all | solution.py:375
  151.0 4.6 %all-to-all-start.2 = ((bf16[32,32,128]{2,1,0:T(8,128)(2,1)}), bf16[32,32,128]{2,1,0:T(8,128)(2,1)}, u32[]{:S(2)}, u32[]{:S(2)}) async-start(bf16[32,32,128]{2,1,0:T(8,128)(2,1)} %get-tuple-element.40), calls=%async_computation.2 | async-start | bytes 524288 | tf_op jit(solution)/shard_map/all_to_all | solution.py:385
  155.6 2.1 %collective-permute-start.5 = (bf16[3,256,128]{2,1,0:T(8,128)(2,1)}, bf16[3,256,128]{2,1,0:T(8,128)(2,1)S(1)}, u32[]{:S(2)}, u32[]{:S(2)}) collective-permute-start(bf16[3,256,128]{2,1,0:T(8,128)(2,1)} %copy-done.9), channel_id=1, source_target_pairs={{0,2},{2,0},{4,6},{6,4},{8,10},{10,8},{12,14},{14,12},{1,3},{3,1},... | collective-permute-start | bytes 589832 | tf_op jit(solution)/shard_map/ppermute | solution.py:56
  157.7 1.4 copy.21
  159.1 0.8 copy-done
  160.7 0.8 copy-done.18
  161.5 1.6 collective-permute-start.6
  163.1 1.0 collective-permute-done.5.far_acts
  164.1 4.5 %shard_map.183 = (bf16[2048,128]{1,0:T(8,128)(2,1)}, bf16[2048,128]{1,0:T(8,128)(2,1)}, bf16[128,2048]{1,0:T(8,128)(2,1)}) custom-call(s32[3]{0:T(128)S(1)} %pad_add_fusion.ids, bf16[256,2048]{1,0:T(8,128)(2,1)S(1)} %bitcast.26, bf16[256,2048]{1,0:T(8,128)(2,1)S(1)} %collective-permute-done.other, bf16[256,2048]{1,0:T(8,128)(2,1)S(1)} %collective-permute-done.1.far, ...), custom_call_target="tpu_custom_call" | custom-call | flops 1000000000 | bytes 4587532 | tf_op jit(solution)/shard_map/pallas_call | solution.py:36
  168.6 1.6 shard_map.187
  170.2 1.0 convert_reduce_fusion
  (45 shorter events, 3.1 us)
Async XLA Ops:
  0.7 1.0 copy-start.2
  1.8 1.0 copy-start.6
  2.8 0.7 copy-start.13
  3.5 0.7 copy-start.14
  6.3 13.9 %copy-start.3 = (bf16[1,2048,128]{2,1,0:T(8,128)(2,1)S(1)}, bf16[1,2048,128]{2,1,0:T(8,128)(2,1)}, u32[]{:S(2)}) copy-start(bf16[1,2048,128]{2,1,0:T(8,128)(2,1)} %param.17) | copy-start | bytes 1572868
  6.3 13.9 %copy-start.4 = (bf16[1,2048,128]{2,1,0:T(8,128)(2,1)S(1)}, bf16[1,2048,128]{2,1,0:T(8,128)(2,1)}, u32[]{:S(2)}) copy-start(bf16[1,2048,128]{2,1,0:T(8,128)(2,1)} %param.18) | copy-start | bytes 1572868
  6.3 13.9 %copy-start.5 = (bf16[1,128,2048]{2,1,0:T(8,128)(2,1)S(1)}, bf16[1,128,2048]{2,1,0:T(8,128)(2,1)}, u32[]{:S(2)}) copy-start(bf16[1,128,2048]{2,1,0:T(8,128)(2,1)} %param.19) | copy-start | bytes 1572868
  6.3 40.0 %all-to-all-start = ((bf16[32,8,2048]{2,1,0:T(8,128)(2,1)}), bf16[32,8,2048]{2,1,0:T(8,128)(2,1)S(1)}, u32[]{:S(2)}, u32[]{:S(2)}) async-start(bf16[32,8,2048]{2,1,0:T(8,128)(2,1)} %bitcast.5), calls=%async_computation | async-start | bytes 2097152 | tf_op jit(solution)/shard_map/all_to_all | solution.py:306
  22.1 37.2 %collective-permute-start.3 = (bf16[3,2048,128]{2,1,0:T(8,128)(2,1)}, bf16[3,2048,128]{2,1,0:T(8,128)(2,1)}, u32[]{:S(2)}, u32[]{:S(2)}) collective-permute-start(bf16[3,2048,128]{2,1,0:T(8,128)(2,1)} %shard_map.181.own), channel_id=1, source_target_pairs={{0,2},{2,0},{4,6},{6,4},{8,10},{10,8},{12,14},{14,12},{1,3},{3,1},... | collective-permute-start | bytes 4718600 | tf_op jit(solution)/shard_map/ppermute | solution.py:56
  46.4 12.9 %collective-permute-start = (bf16[256,2048]{1,0:T(8,128)(2,1)S(1)}, bf16[256,2048]{1,0:T(8,128)(2,1)S(1)}, u32[]{:S(2)}, u32[]{:S(2)}) collective-permute-start(bf16[256,2048]{1,0:T(8,128)(2,1)S(1)} %bitcast.23), channel_id=1, source_target_pairs={{0,1},{1,0},{2,3},{3,2},{4,5},{5,4},{6,7},{7,6},{8,9},{9,8},{10,11... | collective-permute-start | bytes 3145736 | tf_op jit(solution)/shard_map/ppermute | solution.py:51
  64.2 8.0 %copy-start.9 = (bf16[3,256,128]{2,1,0:T(8,128)(2,1)}, bf16[3,256,128]{2,1,0:T(8,128)(2,1)S(1)}, u32[]{:S(2)}) copy-start(bf16[3,256,128]{2,1,0:T(8,128)(2,1)S(1)} %get-tuple-element.33) | copy-start | bytes 589828
  64.3 7.0 %collective-permute-start.4 = (bf16[256,1024]{1,0:T(8,128)(2,1)S(1)}, bf16[256,1024]{1,0:T(8,128)(2,1)S(1)}, u32[]{:S(2)}, u32[]{:S(2)}) collective-permute-start(bf16[256,1024]{1,0:T(8,128)(2,1)S(1)} %get-tuple-element.29), channel_id=1, source_target_pairs={{0,1},{1,0},{2,3},{3,2},{4,5},{5,4},{6,7},{7,6},{8,9},{9,8},{10,11... | collective-permute-start | bytes 1572872 | tf_op jit(solution)/shard_map/ppermute | solution.py:51
  68.0 29.5 %collective-permute-start.1 = (bf16[256,2048]{1,0:T(8,128)(2,1)S(1)}, bf16[256,2048]{1,0:T(8,128)(2,1)S(1)}, u32[]{:S(2)}, u32[]{:S(2)}) collective-permute-start(bf16[256,2048]{1,0:T(8,128)(2,1)S(1)} %bitcast.25), channel_id=1, source_target_pairs={{0,2},{2,0},{4,6},{6,4},{8,10},{10,8},{12,14},{14,12},{1,3},{3,1},... | collective-permute-start | bytes 3145736 | tf_op jit(solution)/shard_map/ppermute | solution.py:56
  71.2 29.4 %copy-start.19 = (f32[64]{0:T(128)S(1)}, f32[64]{0:T(128)}, u32[]{:S(2)}) copy-start(f32[64]{0:T(128)} %param.25) | copy-start | bytes 772
  71.2 44.1 %copy-start.10 = (bf16[64,128]{1,0:T(8,128)(2,1)S(1)}, bf16[64,128]{1,0:T(8,128)(2,1)}, u32[]{:S(2)}) copy-start(bf16[64,128]{1,0:T(8,128)(2,1)} %conv.3) | copy-start | bytes 49156
  72.2 43.1 %all-to-all-start.1 = ((bf16[256,8,128]{2,1,0:T(8,128)(2,1)}), bf16[256,8,128]{2,1,0:T(8,128)(2,1)}, u32[]{:S(2)}, u32[]{:S(2)}) async-start(bf16[256,8,128]{2,1,0:T(8,128)(2,1)} %bitcast.35), calls=%async_computation.1 | async-start | bytes 1048576 | tf_op jit(solution)/shard_map/all_to_all | solution.py:330
  97.5 66.6 %collective-permute-start.2 = (bf16[256,2048]{1,0:T(8,128)(2,1)S(1)}, bf16[256,2048]{1,0:T(8,128)(2,1)}, u32[]{:S(2)}, u32[]{:S(2)}) collective-permute-start(bf16[256,2048]{1,0:T(8,128)(2,1)S(1)} %collective-permute-done.1.far), channel_id=1, source_target_pairs={{0,1},{1,0},{2,3},{3,2},{4,5},{5,4},{6,7},{7,6},{8,9},{9,8},{10,11... | collective-permute-start | bytes 3145736 | tf_op jit(solution)/shard_map/ppermute | solution.py:51
  115.3 1.0 copy-start.7
  116.4 20.8 %copy-start.8 = (bf16[2048,64]{0,1:T(8,128)(2,1)S(1)}, bf16[2048,64]{0,1:T(8,128)(2,1)}, u32[]{:S(2)}) copy-start(bf16[2048,64]{0,1:T(8,128)(2,1)} %param.20) | copy-start | bytes 786436
  138.6 12.4 %copy-start.15 = (f32[64,128]{1,0:T(8,128)}, f32[64,128]{1,0:T(8,128)S(1)}, u32[]{:S(2)}) copy-start(f32[64,128]{1,0:T(8,128)S(1)} %get-tuple-element.42.xhat) | copy-start | bytes 98308
  138.6 12.4 %copy-start.17 = (f32[64,128]{1,0:T(8,128)}, f32[64,128]{1,0:T(8,128)S(1)}, u32[]{:S(2)}) copy-start(f32[64,128]{1,0:T(8,128)S(1)} %get-tuple-element.43.centred) | copy-start | bytes 98308
  151.0 19.2 %all-to-all-start.2 = ((bf16[32,32,128]{2,1,0:T(8,128)(2,1)}), bf16[32,32,128]{2,1,0:T(8,128)(2,1)}, u32[]{:S(2)}, u32[]{:S(2)}) async-start(bf16[32,32,128]{2,1,0:T(8,128)(2,1)} %get-tuple-element.40), calls=%async_computation.2 | async-start | bytes 524288 | tf_op jit(solution)/shard_map/all_to_all | solution.py:385
  155.6 8.5 %collective-permute-start.5 = (bf16[3,256,128]{2,1,0:T(8,128)(2,1)}, bf16[3,256,128]{2,1,0:T(8,128)(2,1)S(1)}, u32[]{:S(2)}, u32[]{:S(2)}) collective-permute-start(bf16[3,256,128]{2,1,0:T(8,128)(2,1)} %copy-done.9), channel_id=1, source_target_pairs={{0,2},{2,0},{4,6},{6,4},{8,10},{10,8},{12,14},{14,12},{1,3},{3,1},... | collective-permute-start | bytes 589832 | tf_op jit(solution)/shard_map/ppermute | solution.py:56
  159.1 0.8 copy-start
  159.9 0.8 copy-start.16
  160.7 0.8 copy-start.18
  161.5 7.1 %copy-start.1 = (f32[31,64]{0,1:T(8,128)S(1)}, f32[31,64]{0,1:T(8,128)}, u32[]{:S(2)}) copy-start(f32[31,64]{0,1:T(8,128)} %copy.21) | copy-start | bytes 23812
  161.5 7.1 %copy-start.11 = (bf16[64,128]{1,0:T(8,128)(2,1)S(1)}, bf16[64,128]{1,0:T(8,128)(2,1)}, u32[]{:S(2)}) copy-start(bf16[64,128]{1,0:T(8,128)(2,1)} %gate.1) | copy-start | bytes 49156
  161.5 7.1 %copy-start.12 = (bf16[64,128]{1,0:T(8,128)(2,1)S(1)}, bf16[64,128]{1,0:T(8,128)(2,1)}, u32[]{:S(2)}) copy-start(bf16[64,128]{1,0:T(8,128)(2,1)} %value.1) | copy-start | bytes 49156
  161.5 7.1 %collective-permute-start.6 = (f32[64,128]{1,0:T(8,128)S(1)}, f32[64,128]{1,0:T(8,128)S(1)}, u32[]{:S(2)}, u32[]{:S(2)}) collective-permute-start(f32[64,128]{1,0:T(8,128)S(1)} %shard_map.186.conv), channel_id=1, source_target_pairs={{16,0},{32,16},{48,32},{64,48},{80,64},{96,80},{112,96},{128,112},... | collective-permute-start | bytes 98312 | tf_op jit(solution)/shard_map/ppermute | solution.py:389

commit v4 on v3

--- a/solution.py
+++ b/solution.py
@@ -20,6 +20,7 @@
 TP = ("chip", "core")
 VMEM = pl.BlockSpec(memory_space=pltpu.VMEM)
 SMEM = pl.BlockSpec(memory_space=pltpu.SMEM)
+HBM = pl.BlockSpec(memory_space=pltpu.HBM)
 
 
 def dot(a, b, dims):
@@ -31,7 +32,7 @@
 TN = ((0,), (0,))
 
 
-def local_kernel(body, outs, *args, specs=None, flops=10**9):
+def local_kernel(body, outs, *args, specs=None, scratch=(), grant=16, flops=10**9):
     size = sum(a.size * a.dtype.itemsize for a in args)
     return pl.pallas_call(
         body,
@@ -39,7 +40,8 @@
         in_specs=[VMEM] * len(args) if specs is None else specs,
         out_specs=jax.tree.map(lambda _: VMEM, outs),
         cost_estimate=pl.CostEstimate(flops=flops, bytes_accessed=size, transcendentals=0),
-        compiler_params=pltpu.CompilerParams(vmem_limit_bytes=40 * 2**20),
+        compiler_params=pltpu.CompilerParams(vmem_limit_bytes=grant * 2**20),
+        scratch_shapes=scratch,
     )(*args)
 
 
@@ -56,16 +58,20 @@
     return lax.ppermute(value, "chip", [(k, k ^ 1) for k in range(count)])
 
 
-def pack_weights(chips, ids, gate, up, down, out):
+def pack_weights(chips, ids, gate, up, down, out, sems):
     half = chips * LANES
+    copies = []
     for turn in range(2):
         which = ids[0] if turn == 0 else 1 - ids[0]
         for i in range(chips):
             at = pl.ds(pl.multiple_of((2 * i + which) * LANES, LANES), LANES)
             here = slice(turn * half + i * LANES, turn * half + (i + 1) * LANES)
-            out[0, here, :] = gate[at, :]
-            out[1, here, :] = up[at, :]
-            out[2, here, :] = down[:, at]
+            for n, block in enumerate((gate.at[0, at, :], up.at[0, at, :], down.at[0, :, at])):
+                sem = sems.at[len(copies)]
+                copies.append(pltpu.make_async_copy(block, out.at[n, here, :], sem))
+                copies[-1].start()
+    for copy in copies:
+        copy.wait()
 
 
 def prepare(experts, capacity, share, chips, ids, routes, weights, stream, cot, out, slots):
@@ -166,17 +172,23 @@
     return high, middle, x - high - middle
 
 
-def finish(capacity, share, chips, ids, data, slots, cot, conv, out):
+def finish(capacity, share, chips, ids, data, slots, cot, conv, out, cot_here, conv_here, sems):
     rows, count = data.shape[0], slots.shape[1]
+    columns = pl.ds(pl.multiple_of(ids[2] * LANES, LANES), LANES)
+    cot_copy = pltpu.make_async_copy(cot.at[:, columns], cot_here, sems.at[0])
+    conv_copy = pltpu.make_async_copy(conv, conv_here, sems.at[1])
+    cot_copy.start()
+    conv_copy.start()
     row = lax.broadcasted_iota(jnp.int32, (rows, count), 0)
     expert = row // (chips * share)
     chip = (row // share) % chips
     key = expert * capacity + (chip % 2) * share + row % share
     hit = (key == slots[0:1, :]) | (key == slots[1:2, :])
     total = dot(jnp.where(hit, 1.0, 0.0).astype(bf16), data[...], TN)
-    at = pl.ds(pl.multiple_of(ids[2] * LANES, LANES), LANES)
-    out[0:count, :] = (cot[:, at].astype(f32) + total).astype(bf16)
-    wide = conv[...].astype(f32)
+    cot_copy.wait()
+    out[0:count, :] = (cot_here[...].astype(f32) + total).astype(bf16)
+    conv_copy.wait()
+    wide = conv_here[...].astype(f32)
     at = lax.broadcasted_iota(jnp.int32, (16, count), 0)
     block = jnp.zeros((16, count), f32)
     sums = jnp.sum(wide, axis=0, keepdims=True), jnp.sum(wide * wide, axis=0, keepdims=True)
@@ -185,7 +197,7 @@
     out[count : count + 16, :] = block.astype(bf16)
 
 
-def tail(total_channels, got, proj_t, conv, gain, xhat, centred, inverse, sums, stream, packed):
+def tail(total_channels, got, proj_t, conv, gain, kept, sums, stream, packed):
     pieces, count = got.shape[0], stream.shape[0]
     channels = proj_t.shape[0]
     lane = lax.broadcasted_iota(jnp.int32, (32, 2 * channels), 1)
@@ -211,9 +223,9 @@
             second = outer[64 * u + 32 : 64 * u + 64]
             packed[2 * j + u] = jnp.where(lane < channels, first, second).astype(bf16)
     grown = hidden_grad * sig * (1.0 + normed * (1.0 - sig)) * gain[...]
-    xhat[...] = grown
-    centred[...] = removed
-    inverse[...] = scale
+    kept[0:channels] = grown
+    kept[channels : 2 * channels] = removed
+    kept[2 * channels :] = jnp.broadcast_to(scale, (8, count))
     at = lax.broadcasted_iota(jnp.int32, (8, count), 0)
     one = jnp.sum(grown, axis=0, keepdims=True)
     two = jnp.sum(grown * removed, axis=0, keepdims=True)
@@ -222,12 +234,15 @@
         sums[j] = block
 
 
-def normalise(total_channels, sums, xhat, centred, inverse, conv):
+def normalise(total_channels, sums, kept, conv):
+    channels = conv.shape[0]
     block = jnp.zeros(sums.shape[1:], f32)
     for j in range(sums.shape[0]):
         block = block + sums[j]
     block = block / total_channels
-    conv[...] = inverse[...] * (xhat[...] - block[0:1] - centred[...] * block[1:2])
+    xhat, centred = kept[0:channels], kept[channels : 2 * channels]
+    inverse = kept[2 * channels : 2 * channels + 1]
+    conv[...] = inverse * (xhat - block[0:1] - centred * block[1:2])
 
 
 def convolve(conv, rim, taps, gate, value, grad_value, grad_gate_in):
@@ -286,10 +301,12 @@
         functools.partial(pack_weights, chips),
         shaped((3, width, hid), bf16),
         ids,
-        w_gate[0],
-        w_up[0],
-        w_down[0],
-        specs=[SMEM, VMEM, VMEM, VMEM],
+        w_gate,
+        w_up,
+        w_down,
+        specs=[SMEM] + [HBM] * 3,
+        scratch=[pltpu.SemaphoreType.DMA((3 * tp_count,))],
+        grant=60,
     )
     w_far = swap_chips(w_own)
 
@@ -353,16 +370,20 @@
         slots,
         out_cot,
         conv_result,
-        specs=[SMEM] + [VMEM] * 4,
+        specs=[SMEM, VMEM, VMEM, HBM, HBM],
+        scratch=[
+            pltpu.VMEM((tokens, cols), bf16),
+            pltpu.VMEM((channels, positions), bf16),
+            pltpu.SemaphoreType.DMA((2,)),
+        ],
+        grant=60,
     )
     got = lax.all_gather(payload, TP)
 
-    xhat, centred, inverse, sums, grad_stream, packed = local_kernel(
+    kept, sums, grad_stream, packed = local_kernel(
         functools.partial(tail, channel_total),
         (
-            shaped((channels, positions), f32),
-            shaped((channels, positions), f32),
-            shaped((1, positions), f32),
+            shaped((2 * channels + 8, positions), f32),
             shaped((tp_count, 8, positions), f32),
             shaped((tokens, width), bf16),
             shaped((sp_count, 32, 2 * channels), bf16),
@@ -377,9 +398,7 @@
         functools.partial(normalise, channel_total),
         shaped((channels, positions), f32),
         sums,
-        xhat,
-        centred,
-        inverse,
+        kept,
     )
 
     packed = lax.all_to_all(packed, "sp", 0, 0, tiled=True)

time: 174 us -> 176 us (1.011)
    ppermute x3, waiting for transfers between devices: 15.6 us -> 18.6 us  [swap_chips(): return lax.ppermute(value, 'chip', [(k, k ^ 1) for k in range(count)])]
    unnamed x41 -> x39, local copies, waits for them, and re-layouts: 8.31 us -> 7.89 us
  transfers between devices with their start and end apart: 10 -> 10, of which waited for: 5 -> 5; matrix products, arithmetic and copies ran while one was open for 1% -> 1% of each run, Pallas kernels for 7% -> 8%
where the time goes in v4:
time: 176 us; the launch traced here: 174 us
  starting transfers between devices  58.9 us (33%)
  waiting for transfers between devices  52.6 us (30%)
  blocking collectives  31.4 us (18%)
  Pallas kernels  19.9 us (11%)
  local copies, waits for them, and re-layouts  8.06 us (5%)
  other arithmetic  2.64 us (2%)
    pallas_call x8, Pallas kernels, local_kernel(): pl.pallas_call(body, out_shape=outs, in_specs=[VMEM] * len(args) if specs...  19.9 us
    all_to_all x1, waiting for transfers between devices, body(): lax.all_to_all(sent.reshape(experts, share, width), 'sp', 0, 0, tiled=True)  19.4 us
    all_gather x1, blocking collectives, body(): got = lax.all_gather(payload, TP)  19.1 us
    all_to_all x1, starting transfers between devices, body(): returned = lax.all_to_all(back, ('sp', 'chip'), 0, 0, tiled=True)  18.9 us
    ppermute x3, waiting for transfers between devices, swap_chips(): return lax.ppermute(value, 'chip', [(k, k ^ 1) for k in range(count)])  18.6 us
    all_to_all x1, waiting for transfers between devices, body(): returned = lax.all_to_all(back, ('sp', 'chip'), 0, 0, tiled=True)  14.6 us
    all_to_all x1, starting transfers between devices, body(): lax.all_to_all(sent.reshape(experts, share, width), 'sp', 0, 0, tiled=True)  13.7 us
    all_to_all x1, blocking collectives, body(): sums = lax.all_to_all(sums, TP, 0, 0, tiled=True)  12.3 us
  transfers between devices with their start and end apart: 10, of which 5 were waited for; matrix products, arithmetic and copies ran while one was open for 1% of the time, Pallas kernels for 8%

profile of v4, /device:TPU:1, one launch (start us, length us, event | category | flops | bytes accessed | tf_op | source)
XLA Modules:
  0.0 174.4 jit_solution(2969968349545347219)
XLA Ops:
  0.7 1.0 copy-done.5
  1.8 1.0 copy-done.6
  4.2 2.2 %shard_map.180 = (bf16[256,2048]{1,0:T(8,128)(2,1)}, s32[2,128]{1,0:T(2,128)S(1)}) custom-call(s32[3]{0:T(128)S(1)} %pad_add_fusion.ids, s32[2,128]{1,0:T(2,128)S(1)} %bitcast.27, f32[2,128]{1,0:T(2,128)S(1)} %bitcast.28, bf16[128,2048]{1,0:T(8,128)(2,1)S(1)} %copy-done.5, bf16[128,2048]{1,0:T(8,128)(2,1)S(1)} %copy-done.6), custom_call_target="tpu_custom_call" | custom-call | flops 1000000000 | bytes 1050636 | tf_op jit(solution)/shard_map/pallas_call | solution.py:37
  6.9 13.7 %all-to-all-start = ((bf16[32,8,2048]{2,1,0:T(8,128)(2,1)}), bf16[32,8,2048]{2,1,0:T(8,128)(2,1)S(1)}, u32[]{:S(2)}, u32[]{:S(2)}) async-start(bf16[32,8,2048]{2,1,0:T(8,128)(2,1)} %bitcast.5), calls=%async_computation | async-start | bytes 2097152 | tf_op jit(solution)/shard_map/all_to_all | solution.py:323
  20.6 3.6 %shard_map.181.own = bf16[3,2048,128]{2,1,0:T(8,128)(2,1)} custom-call(s32[3]{0:T(128)} %copy-done.3, bf16[1,2048,128]{2,1,0:T(8,128)(2,1)} %gate.2, bf16[1,2048,128]{2,1,0:T(8,128)(2,1)} %up.1, bf16[1,128,2048]{2,1,0:T(8,128)(2,1)} %down.1), custom_call_target="tpu_custom_call" | custom-call | flops 1000000000 | bytes 1572876 | tf_op jit(solution)/shard_map/pallas_call | solution.py:37
  24.2 3.2 %collective-permute-start.3 = (bf16[3,2048,128]{2,1,0:T(8,128)(2,1)}, bf16[3,2048,128]{2,1,0:T(8,128)(2,1)}, u32[]{:S(2)}, u32[]{:S(2)}) collective-permute-start(bf16[3,2048,128]{2,1,0:T(8,128)(2,1)} %shard_map.181.own), channel_id=1, source_target_pairs={{0,2},{2,0},{4,6},{6,4},{8,10},{10,8},{12,14},{14,12},{1,3},{3,1},... | collective-permute-start | bytes 4718600 | tf_op jit(solution)/shard_map/ppermute | solution.py:58
  27.5 19.4 %all-to-all-done = bf16[32,8,2048]{2,1,0:T(8,128)(2,1)S(1)} async-done(((bf16[32,8,2048]{2,1,0:T(8,128)(2,1)}), bf16[32,8,2048]{2,1,0:T(8,128)(2,1)S(1)}, u32[]{:S(2)}, u32[]{:S(2)}) %all-to-all-start) | async-done | bytes 1048608 | tf_op jit(solution)/shard_map/all_to_all | solution.py:323
  46.8 4.7 %collective-permute-start = (bf16[256,2048]{1,0:T(8,128)(2,1)S(1)}, bf16[256,2048]{1,0:T(8,128)(2,1)S(1)}, u32[]{:S(2)}, u32[]{:S(2)}) collective-permute-start(bf16[256,2048]{1,0:T(8,128)(2,1)S(1)} %bitcast.20), channel_id=1, source_target_pairs={{0,1},{1,0},{2,3},{3,2},{4,5},{5,4},{6,7},{7,6},{8,9},{9,8},{10,11... | collective-permute-start | bytes 3145736 | tf_op jit(solution)/shard_map/ppermute | solution.py:53
  51.5 9.9 %collective-permute-done.3.far = bf16[3,2048,128]{2,1,0:T(8,128)(2,1)} collective-permute-done((bf16[3,2048,128]{2,1,0:T(8,128)(2,1)}, bf16[3,2048,128]{2,1,0:T(8,128)(2,1)}, u32[]{:S(2)}, u32[]{:S(2)}) %collective-permute-start.3) | collective-permute-done | bytes 1572896 | tf_op jit(solution)/shard_map/ppermute | solution.py:58
  61.5 1.4 copy-done
  62.9 4.3 %shard_map.182 = (bf16[3,256,128]{2,1,0:T(8,128)(2,1)S(1)}, bf16[3,256,128]{2,1,0:T(8,128)(2,1)S(1)}, f32[256,1024]{1,0:T(8,128)S(1)}, bf16[256,1024]{1,0:T(8,128)(2,1)S(1)}) custom-call(bf16[256,2048]{1,0:T(8,128)(2,1)S(1)} %bitcast.21, bf16[256,2048]{1,0:T(8,128)(2,1)S(1)} %collective-permute-done.other, bf16[3,2048,128]{2,1,0:T(8,128)(2,1)S(1)} %copy-done, ...), custom_call_target="tpu_custom_call" | custom-call | flops 1000000000 | bytes 5242880 | tf_op jit(solution)/shard_map/pallas_call | solution.py:37
  67.2 3.7 %collective-permute-start.4 = (bf16[256,1024]{1,0:T(8,128)(2,1)S(1)}, bf16[256,1024]{1,0:T(8,128)(2,1)S(1)}, u32[]{:S(2)}, u32[]{:S(2)}) collective-permute-start(bf16[256,1024]{1,0:T(8,128)(2,1)S(1)} %get-tuple-element.27), channel_id=1, source_target_pairs={{0,1},{1,0},{2,3},{3,2},{4,5},{5,4},{6,7},{7,6},{8,9},{9,8},{10,11... | collective-permute-start | bytes 1572872 | tf_op jit(solution)/shard_map/ppermute | solution.py:53
  70.9 3.2 %collective-permute-start.1 = (bf16[256,2048]{1,0:T(8,128)(2,1)S(1)}, bf16[256,2048]{1,0:T(8,128)(2,1)S(1)}, u32[]{:S(2)}, u32[]{:S(2)}) collective-permute-start(bf16[256,2048]{1,0:T(8,128)(2,1)S(1)} %bitcast.22), channel_id=1, source_target_pairs={{0,2},{2,0},{4,6},{6,4},{8,10},{10,8},{12,14},{14,12},{1,3},{3,1},... | collective-permute-start | bytes 3145736 | tf_op jit(solution)/shard_map/ppermute | solution.py:58
  74.2 0.9 add_convert_fusion
  75.1 18.9 %all-to-all-start.1 = ((bf16[256,8,128]{2,1,0:T(8,128)(2,1)}), bf16[256,8,128]{2,1,0:T(8,128)(2,1)}, u32[]{:S(2)}, u32[]{:S(2)}) async-start(bf16[256,8,128]{2,1,0:T(8,128)(2,1)} %bitcast.29), calls=%async_computation.1 | async-start | bytes 1048576 | tf_op jit(solution)/shard_map/all_to_all | solution.py:347
  94.0 6.4 %collective-permute-done.1.far = bf16[256,2048]{1,0:T(8,128)(2,1)S(1)} collective-permute-done((bf16[256,2048]{1,0:T(8,128)(2,1)S(1)}, bf16[256,2048]{1,0:T(8,128)(2,1)S(1)}, u32[]{:S(2)}, u32[]{:S(2)}) %collective-permute-start.1) | collective-permute-done | bytes 1048608 | tf_op jit(solution)/shard_map/ppermute | solution.py:58
  100.5 3.1 %collective-permute-start.2 = (bf16[256,2048]{1,0:T(8,128)(2,1)S(1)}, bf16[256,2048]{1,0:T(8,128)(2,1)}, u32[]{:S(2)}, u32[]{:S(2)}) collective-permute-start(bf16[256,2048]{1,0:T(8,128)(2,1)S(1)} %collective-permute-done.1.far), channel_id=1, source_target_pairs={{0,1},{1,0},{2,3},{3,2},{4,5},{5,4},{6,7},{7,6},{8,9},{9,8},{10,11... | collective-permute-start | bytes 3145736 | tf_op jit(solution)/shard_map/ppermute | solution.py:53
  103.7 14.6 %all-to-all-done.1 = bf16[256,8,128]{2,1,0:T(8,128)(2,1)} async-done(((bf16[256,8,128]{2,1,0:T(8,128)(2,1)}), bf16[256,8,128]{2,1,0:T(8,128)(2,1)}, u32[]{:S(2)}, u32[]{:S(2)}) %all-to-all-start.1) | async-done | bytes 524320 | tf_op jit(solution)/shard_map/all_to_all | solution.py:347
  118.3 2.6 %shard_map.184 = bf16[144,128]{1,0:T(8,128)(2,1)} custom-call(s32[3]{0:T(128)} %copy-done.3, bf16[2048,128]{1,0:T(8,128)(2,1)} %bitcast.13.data, s32[2,128]{1,0:T(2,128)} %copy-done.16, bf16[128,2048]{1,0:T(8,128)(2,1)} %cot.3, bf16[64,128]{1,0:T(8,128)(2,1)} %conv.3), custom_call_target="tpu_custom_call" | custom-call | flops 1000000000 | bytes 1065996 | tf_op jit(solution)/shard_map/pallas_call | solution.py:37
  120.9 19.1 %all-gather = bf16[2304,128]{1,0:T(8,128)(2,1)S(1)} all-gather(bf16[144,128]{1,0:T(8,128)(2,1)} %shard_map.184), channel_id=2, replica_groups=mesh['sp'=32,'chip'=8,'core'=2] {'chip','core'}, dimensions={0}, use_global_device_ids=true | all-gather | bytes 626688 | tf_op jit(solution)/shard_map/all_gather | solution.py:381
  140.0 1.5 shard_map.185
  141.5 12.3 %all_to_all.20.sums = f32[16,8,128]{2,1,0:T(8,128)} all-to-all(f32[16,8,128]{2,1,0:T(8,128)S(1)} %get-tuple-element.39), channel_id=1, replica_groups=mesh['sp'=32,'chip'=8,'core'=2] {'chip','core'}, dimensions={0} | all-to-all | bytes 131072 | tf_op jit(solution)/shard_map/all_to_all | solution.py:396
  153.8 4.6 %all-to-all-start.2 = ((bf16[32,32,128]{2,1,0:T(8,128)(2,1)}), bf16[32,32,128]{2,1,0:T(8,128)(2,1)}, u32[]{:S(2)}, u32[]{:S(2)}) async-start(bf16[32,32,128]{2,1,0:T(8,128)(2,1)} %get-tuple-element.38), calls=%async_computation.2 | async-start | bytes 524288 | tf_op jit(solution)/shard_map/all_to_all | solution.py:404
  158.4 2.1 %collective-permute-start.5 = (bf16[3,256,128]{2,1,0:T(8,128)(2,1)}, bf16[3,256,128]{2,1,0:T(8,128)(2,1)S(1)}, u32[]{:S(2)}, u32[]{:S(2)}) collective-permute-start(bf16[3,256,128]{2,1,0:T(8,128)(2,1)} %copy-done.8), channel_id=1, source_target_pairs={{0,2},{2,0},{4,6},{6,4},{8,10},{10,8},{12,14},{14,12},{1,3},{3,1},... | collective-permute-start | bytes 589832 | tf_op jit(solution)/shard_map/ppermute | solution.py:58
  160.5 0.7 copy.21
  161.2 0.8 copy-done.1
  162.1 0.9 copy-done.15
  163.0 1.6 collective-permute-start.6
  164.6 2.3 %collective-permute-done.5.far_acts = bf16[3,256,128]{2,1,0:T(8,128)(2,1)S(1)} collective-permute-done((bf16[3,256,128]{2,1,0:T(8,128)(2,1)}, bf16[3,256,128]{2,1,0:T(8,128)(2,1)S(1)}, u32[]{:S(2)}, u32[]{:S(2)}) %collective-permute-start.5) | collective-permute-done | bytes 196640 | tf_op jit(solution)/shard_map/ppermute | solution.py:58
  167.0 4.2 %shard_map.183 = (bf16[2048,128]{1,0:T(8,128)(2,1)}, bf16[2048,128]{1,0:T(8,128)(2,1)}, bf16[128,2048]{1,0:T(8,128)(2,1)}) custom-call(s32[3]{0:T(128)S(1)} %copy-done.4, bf16[256,2048]{1,0:T(8,128)(2,1)S(1)} %bitcast.23, bf16[256,2048]{1,0:T(8,128)(2,1)S(1)} %collective-permute-done.other, bf16[256,2048]{1,0:T(8,128)(2,1)S(1)} %collective-permute-done.1.far, ...), custom_call_target="tpu_custom_call" | custom-call | flops 1000000000 | bytes 4587532 | tf_op jit(solution)/shard_map/pallas_call | solution.py:37
  171.2 1.6 shard_map.187
  172.7 1.0 convert_reduce_fusion
  (43 shorter events, 2.9 us)
Async XLA Ops:
  0.7 5.6 %copy-start.3 = (s32[3]{0:T(128)}, s32[3]{0:T(128)S(1)}, u32[]{:S(2)}) copy-start(s32[3]{0:T(128)S(1)} %pad_add_fusion.ids) | copy-start | bytes 40
  0.7 1.0 copy-start.5
  1.8 1.0 copy-start.6
  2.8 0.7 copy-start.12
  3.5 0.7 copy-start.13
  6.4 0.6 copy-start.16
  6.9 39.9 %all-to-all-start = ((bf16[32,8,2048]{2,1,0:T(8,128)(2,1)}), bf16[32,8,2048]{2,1,0:T(8,128)(2,1)S(1)}, u32[]{:S(2)}, u32[]{:S(2)}) async-start(bf16[32,8,2048]{2,1,0:T(8,128)(2,1)} %bitcast.5), calls=%async_computation | async-start | bytes 2097152 | tf_op jit(solution)/shard_map/all_to_all | solution.py:323
  24.2 37.2 %collective-permute-start.3 = (bf16[3,2048,128]{2,1,0:T(8,128)(2,1)}, bf16[3,2048,128]{2,1,0:T(8,128)(2,1)}, u32[]{:S(2)}, u32[]{:S(2)}) collective-permute-start(bf16[3,2048,128]{2,1,0:T(8,128)(2,1)} %shard_map.181.own), channel_id=1, source_target_pairs={{0,2},{2,0},{4,6},{6,4},{8,10},{10,8},{12,14},{14,12},{1,3},{3,1},... | collective-permute-start | bytes 4718600 | tf_op jit(solution)/shard_map/ppermute | solution.py:58
  46.8 14.6 %collective-permute-start = (bf16[256,2048]{1,0:T(8,128)(2,1)S(1)}, bf16[256,2048]{1,0:T(8,128)(2,1)S(1)}, u32[]{:S(2)}, u32[]{:S(2)}) collective-permute-start(bf16[256,2048]{1,0:T(8,128)(2,1)S(1)} %bitcast.20), channel_id=1, source_target_pairs={{0,1},{1,0},{2,3},{3,2},{4,5},{5,4},{6,7},{7,6},{8,9},{9,8},{10,11... | collective-permute-start | bytes 3145736 | tf_op jit(solution)/shard_map/ppermute | solution.py:53
  61.4 1.4 copy-start
  67.2 7.9 %copy-start.8 = (bf16[3,256,128]{2,1,0:T(8,128)(2,1)}, bf16[3,256,128]{2,1,0:T(8,128)(2,1)S(1)}, u32[]{:S(2)}) copy-start(bf16[3,256,128]{2,1,0:T(8,128)(2,1)S(1)} %get-tuple-element.31) | copy-start | bytes 589828
  67.2 7.0 %collective-permute-start.4 = (bf16[256,1024]{1,0:T(8,128)(2,1)S(1)}, bf16[256,1024]{1,0:T(8,128)(2,1)S(1)}, u32[]{:S(2)}, u32[]{:S(2)}) collective-permute-start(bf16[256,1024]{1,0:T(8,128)(2,1)S(1)} %get-tuple-element.27), channel_id=1, source_target_pairs={{0,1},{1,0},{2,3},{3,2},{4,5},{5,4},{6,7},{7,6},{8,9},{9,8},{10,11... | collective-permute-start | bytes 1572872 | tf_op jit(solution)/shard_map/ppermute | solution.py:53
  70.9 29.5 %collective-permute-start.1 = (bf16[256,2048]{1,0:T(8,128)(2,1)S(1)}, bf16[256,2048]{1,0:T(8,128)(2,1)S(1)}, u32[]{:S(2)}, u32[]{:S(2)}) collective-permute-start(bf16[256,2048]{1,0:T(8,128)(2,1)S(1)} %bitcast.22), channel_id=1, source_target_pairs={{0,2},{2,0},{4,6},{6,4},{8,10},{10,8},{12,14},{14,12},{1,3},{3,1},... | collective-permute-start | bytes 3145736 | tf_op jit(solution)/shard_map/ppermute | solution.py:58
  74.2 29.4 %copy-start.18 = (f32[64]{0:T(128)S(1)}, f32[64]{0:T(128)}, u32[]{:S(2)}) copy-start(f32[64]{0:T(128)} %param.25) | copy-start | bytes 772
  75.1 43.2 %all-to-all-start.1 = ((bf16[256,8,128]{2,1,0:T(8,128)(2,1)}), bf16[256,8,128]{2,1,0:T(8,128)(2,1)}, u32[]{:S(2)}, u32[]{:S(2)}) async-start(bf16[256,8,128]{2,1,0:T(8,128)(2,1)} %bitcast.29), calls=%async_computation.1 | async-start | bytes 1048576 | tf_op jit(solution)/shard_map/all_to_all | solution.py:347
  100.5 66.5 %collective-permute-start.2 = (bf16[256,2048]{1,0:T(8,128)(2,1)S(1)}, bf16[256,2048]{1,0:T(8,128)(2,1)}, u32[]{:S(2)}, u32[]{:S(2)}) collective-permute-start(bf16[256,2048]{1,0:T(8,128)(2,1)S(1)} %collective-permute-done.1.far), channel_id=1, source_target_pairs={{0,1},{1,0},{2,3},{3,2},{4,5},{5,4},{6,7},{7,6},{8,9},{9,8},{10,11... | collective-permute-start | bytes 3145736 | tf_op jit(solution)/shard_map/ppermute | solution.py:53
  118.3 21.7 %copy-start.7 = (bf16[2048,64]{0,1:T(8,128)(2,1)S(1)}, bf16[2048,64]{0,1:T(8,128)(2,1)}, u32[]{:S(2)}) copy-start(bf16[2048,64]{0,1:T(8,128)(2,1)} %param.20) | copy-start | bytes 786436
  118.3 21.7 %copy-start.9 = (bf16[64,128]{1,0:T(8,128)(2,1)S(1)}, bf16[64,128]{1,0:T(8,128)(2,1)}, u32[]{:S(2)}) copy-start(bf16[64,128]{1,0:T(8,128)(2,1)} %conv.3) | copy-start | bytes 49156
  140.0 20.5 %copy-start.17 = (f32[31,64]{1,0:T(8,128)S(1)}, f32[31,64]{1,0:T(8,128)}, u32[]{:S(2)}) copy-start(f32[31,64]{1,0:T(8,128)} %param.23) | copy-start | bytes 23812
  141.5 12.3 %copy-start.14 = (f32[136,128]{1,0:T(8,128)}, f32[136,128]{1,0:T(8,128)S(1)}, u32[]{:S(2)}) copy-start(f32[136,128]{1,0:T(8,128)S(1)} %get-tuple-element.40.kept) | copy-start | bytes 208900
  153.8 18.9 %all-to-all-start.2 = ((bf16[32,32,128]{2,1,0:T(8,128)(2,1)}), bf16[32,32,128]{2,1,0:T(8,128)(2,1)}, u32[]{:S(2)}, u32[]{:S(2)}) async-start(bf16[32,32,128]{2,1,0:T(8,128)(2,1)} %get-tuple-element.38), calls=%async_computation.2 | async-start | bytes 524288 | tf_op jit(solution)/shard_map/all_to_all | solution.py:404
  158.4 8.5 %collective-permute-start.5 = (bf16[3,256,128]{2,1,0:T(8,128)(2,1)}, bf16[3,256,128]{2,1,0:T(8,128)(2,1)S(1)}, u32[]{:S(2)}, u32[]{:S(2)}) collective-permute-start(bf16[3,256,128]{2,1,0:T(8,128)(2,1)} %copy-done.8), channel_id=1, source_target_pairs={{0,2},{2,0},{4,6},{6,4},{8,10},{10,8},{12,14},{14,12},{1,3},{3,1},... | collective-permute-start | bytes 589832 | tf_op jit(solution)/shard_map/ppermute | solution.py:58
  161.2 0.8 copy-start.1
  162.1 0.9 copy-start.15
  163.0 4.0 %copy-start.4 = (s32[3]{0:T(128)S(1)}, s32[3]{0:T(128)}, u32[]{:S(2)}) copy-start(s32[3]{0:T(128)} %copy-done.3) | copy-start | bytes 40
  163.0 8.2 %copy-start.2 = (f32[31,64]{0,1:T(8,128)S(1)}, f32[31,64]{0,1:T(8,128)}, u32[]{:S(2)}) copy-start(f32[31,64]{0,1:T(8,128)} %copy.21) | copy-start | bytes 23812
  163.0 8.1 %copy-start.10 = (bf16[64,128]{1,0:T(8,128)(2,1)S(1)}, bf16[64,128]{1,0:T(8,128)(2,1)}, u32[]{:S(2)}) copy-start(bf16[64,128]{1,0:T(8,128)(2,1)} %gate.3) | copy-start | bytes 49156
  163.0 8.1 %copy-start.11 = (bf16[64,128]{1,0:T(8,128)(2,1)S(1)}, bf16[64,128]{1,0:T(8,128)(2,1)}, u32[]{:S(2)}) copy-start(bf16[64,128]{1,0:T(8,128)(2,1)} %value.1) | copy-start | bytes 49156
  163.0 8.1 %collective-permute-start.6 = (f32[64,128]{1,0:T(8,128)S(1)}, f32[64,128]{1,0:T(8,128)S(1)}, u32[]{:S(2)}, u32[]{:S(2)}) collective-permute-start(f32[64,128]{1,0:T(8,128)S(1)} %shard_map.186.conv), channel_id=1, source_target_pairs={{16,0},{32,16},{48,32},{64,48},{80,64},{96,80},{112,96},{128,112},... | collective-permute-start | bytes 98312 | tf_op jit(solution)/shard_map/ppermute | solution.py:408

commit v5 on v4

--- a/solution.py
+++ b/solution.py
@@ -56,22 +56,6 @@
 def swap_chips(value):
     count = lax.axis_size("chip")
     return lax.ppermute(value, "chip", [(k, k ^ 1) for k in range(count)])
-
-
-def pack_weights(chips, ids, gate, up, down, out, sems):
-    half = chips * LANES
-    copies = []
-    for turn in range(2):
-        which = ids[0] if turn == 0 else 1 - ids[0]
-        for i in range(chips):
-            at = pl.ds(pl.multiple_of((2 * i + which) * LANES, LANES), LANES)
-            here = slice(turn * half + i * LANES, turn * half + (i + 1) * LANES)
-            for n, block in enumerate((gate.at[0, at, :], up.at[0, at, :], down.at[0, :, at])):
-                sem = sems.at[len(copies)]
-                copies.append(pltpu.make_async_copy(block, out.at[n, here, :], sem))
-                copies[-1].start()
-    for copy in copies:
-        copy.wait()
 
 
 def prepare(experts, capacity, share, chips, ids, routes, weights, stream, cot, out, slots):
@@ -109,22 +93,24 @@
         out[:, half + i * LANES : half + (i + 1) * LANES] = (scale * got).astype(bf16)
 
 
-def experts_step(mine, other, own, far, own_acts, far_acts, back_mine, back_other):
+def experts_step(ids, mine, other, *refs):
+    weights, (own_acts, far_acts, back_mine, back_other) = refs[:6], refs[6:]
     half = mine.shape[1] // 2
-    for w, acts in ((own, own_acts), (far, far_acts)):
-
-        def product(n, at):
-            return dot(mine[:, at : at + half], w[n, :half], NN) + dot(
-                other[:, at : at + half], w[n, half:], NN
-            )
-
-        pre_gate, pre_up = product(0, 0), product(1, 0)
-        grad_act = 0.0
-        for i in range(half // LANES):
-            here, there = i * LANES, half + i * LANES
-            block = slice(there, there + LANES)
-            grad_act = grad_act + dot(mine[:, block], w[2, here : here + LANES], NT)
-            grad_act = grad_act + dot(other[:, block], w[2, there : there + LANES], NT)
+    core = ids[0]
+
+    def block(i, which):
+        return pl.ds(pl.multiple_of((2 * i + which) * LANES, LANES), LANES)
+
+    for (gate, up, down), acts in ((weights[:3], own_acts), (weights[3:], far_acts)):
+        pre_gate = pre_up = grad_act = 0.0
+        for rows, which in ((mine, core), (other, 1 - core)):
+            for i in range(half // LANES):
+                at = block(i, which)
+                row = rows[:, i * LANES : (i + 1) * LANES]
+                pre_gate = pre_gate + dot(row, gate[0, at, :], NN)
+                pre_up = pre_up + dot(row, up[0, at, :], NN)
+                cot = rows[:, half + i * LANES : half + (i + 1) * LANES]
+                grad_act = grad_act + dot(cot, down[0, :, at], NT)
         glu = jnp.minimum(pre_gate, clamp_limit)
         lin = jnp.clip(pre_up, -clamp_limit, clamp_limit)
         sig = jax.nn.sigmoid(alpha_gate * glu)
@@ -137,15 +123,14 @@
             jnp.abs(pre_up) < clamp_limit, grad_act * glu * sig, 0.0
         ).astype(bf16)
 
-    def back(at):
-        total = 0.0
-        for w, acts in ((own, own_acts), (far, far_acts)):
-            total = total + dot(acts[0], w[0, at : at + half], NT)
-            total = total + dot(acts[1], w[1, at : at + half], NT)
-        return total
-
-    back_other[...] = back(half).astype(bf16)
-    back_mine[...] = back(0)
+    for out, which in ((back_other, 1 - core), (back_mine, core)):
+        for i in range(half // LANES):
+            at = block(i, which)
+            total = 0.0
+            for (gate, up, _), acts in ((weights[:3], own_acts), (weights[3:], far_acts)):
+                total = total + dot(acts[0], gate[0, at, :], NT)
+                total = total + dot(acts[1], up[0, at, :], NT)
+            out[:, i * LANES : (i + 1) * LANES] = total.astype(out.dtype)
 
 
 def weight_grads(chips, ids, mine, other, far, far_other, own_acts, far_acts, gate, up, down):
@@ -297,18 +282,11 @@
     positions = conv_result.shape[1]
 
     ids = jnp.stack([core, chip % 2, 2 * chip + core]).astype(jnp.int32)
-    w_own = local_kernel(
-        functools.partial(pack_weights, chips),
-        shaped((3, width, hid), bf16),
-        ids,
-        w_gate,
-        w_up,
-        w_down,
-        specs=[SMEM] + [HBM] * 3,
-        scratch=[pltpu.SemaphoreType.DMA((3 * tp_count,))],
-        grant=60,
-    )
-    w_far = swap_chips(w_own)
+    gate_far = swap_chips(w_gate)
+    up_far = swap_chips(w_up)
+    down_far = swap_chips(w_down)
+
+    gain = channel_norm_gain[:, None]
 
     sent, slots = local_kernel(
         functools.partial(prepare, experts, capacity, share, chips),
@@ -334,10 +312,16 @@
             shaped((rows, half), f32),
             shaped((rows, half), bf16),
         ),
+        ids,
         mine,
         other,
-        w_own,
-        w_far,
+        w_gate,
+        w_up,
+        w_down,
+        gate_far,
+        up_far,
+        down_far,
+        specs=[SMEM] + [VMEM] * 8,
     )
     from_core = swap_cores(back_other)
     back = (back_mine + from_core.astype(f32)).astype(bf16)
@@ -391,7 +375,7 @@
         got,
         w_proj.T,
         conv_result,
-        channel_norm_gain[:, None],
+        gain,
     )
     sums = lax.all_to_all(sums, TP, 0, 0, tiled=True)
     grad_conv = local_kernel(

time: 176 us -> 199 us (1.13)
  blocking collectives: 31.4 us -> 71.4 us
  starting transfers between devices: 58.9 us -> 48.7 us
  Pallas kernels: 19.9 us -> 15.7 us
  local copies, waits for them, and re-layouts: 8.06 us -> 6 us
    all_to_all x0 -> x1, blocking collectives: none -> 39.8 us  [body(): lax.all_to_all(sent.reshape(experts, share, width), 'sp', 0, 0, tiled=True)]
    ppermute x3 -> x5, waiting for transfers between devices: 18.6 us -> 41.7 us  [swap_chips(): return lax.ppermute(value, 'chip', [(k, k ^ 1) for k in range(count)])]
    all_to_all x1 -> x0, waiting for transfers between devices: 19.4 us -> none  [body(): lax.all_to_all(sent.reshape(experts, share, width), 'sp', 0, 0, tiled=True)]
    all_to_all x1 -> x0, starting transfers between devices: 13.7 us -> none  [body(): lax.all_to_all(sent.reshape(experts, share, width), 'sp', 0, 0, tiled=True)]
    ppermute x3 -> x5, starting transfers between devices: 8.52 us -> 13.8 us  [swap_chips(): return lax.ppermute(value, 'chip', [(k, k ^ 1) for k in range(count)])]
    pallas_call x8 -> x7, Pallas kernels: 19.9 us -> 15.7 us  [local_kernel(): pl.pallas_call(body, out_shape=outs, in_specs=[VMEM] * len(args) if specs...]
    all_to_all x1, starting transfers between devices: 18.9 us -> 15 us  [body(): returned = lax.all_to_all(back, ('sp', 'chip'), 0, 0, tiled=True)]
    all_to_all x1, waiting for transfers between devices: 14.6 us -> 10.9 us  [body(): returned = lax.all_to_all(back, ('sp', 'chip'), 0, 0, tiled=True)]
  transfers between devices with their start and end apart: 10 -> 11, of which waited for: 5 -> 6; matrix products, arithmetic and copies ran while one was open for 1% -> 1% of each run, Pallas kernels for 8% -> 5%
where the time goes in v5:
time: 199 us; the launch traced here: 198 us
  blocking collectives  71.4 us (36%)
  waiting for transfers between devices  52.7 us (26%)
  starting transfers between devices  48.7 us (24%)
  Pallas kernels  15.7 us (8%)
  local copies, waits for them, and re-layouts  6 us (3%)
  other arithmetic  2.65 us (1%)
    ppermute x5, waiting for transfers between devices, swap_chips(): return lax.ppermute(value, 'chip', [(k, k ^ 1) for k in range(count)])  41.7 us
    all_to_all x1, blocking collectives, body(): lax.all_to_all(sent.reshape(experts, share, width), 'sp', 0, 0, tiled=True)  39.8 us
    all_gather x1, blocking collectives, body(): got = lax.all_gather(payload, TP)  19.2 us
    pallas_call x7, Pallas kernels, local_kernel(): pl.pallas_call(body, out_shape=outs, in_specs=[VMEM] * len(args) if specs...  15.7 us
    all_to_all x1, starting transfers between devices, body(): returned = lax.all_to_all(back, ('sp', 'chip'), 0, 0, tiled=True)  15 us
    ppermute x5, starting transfers between devices, swap_chips(): return lax.ppermute(value, 'chip', [(k, k ^ 1) for k in range(count)])  13.8 us
    all_to_all x1, blocking collectives, body(): sums = lax.all_to_all(sums, TP, 0, 0, tiled=True)  12.4 us
    all_to_all x1, waiting for transfers between devices, body(): returned = lax.all_to_all(back, ('sp', 'chip'), 0, 0, tiled=True)  10.9 us
  transfers between devices with their start and end apart: 11, of which 6 were waited for; matrix products, arithmetic and copies ran while one was open for 1% of the time, Pallas kernels for 5%

profile of v5, /device:TPU:1, one launch (start us, length us, event | category | flops | bytes accessed | tf_op | source)
XLA Modules:
  0.0 197.9 jit_solution(13304802631144460351)
XLA Ops:
  1.4 1.0 copy-done.7
  2.5 1.0 copy-done.8
  3.5 1.2 shard_map.180
  5.3 39.8 %all_to_all.20 = bf16[32,8,2048]{2,1,0:T(8,128)(2,1)S(1)} all-to-all(bf16[32,8,2048]{2,1,0:T(8,128)(2,1)S(1)} %bitcast.24), channel_id=1, replica_groups=mesh['sp'=32,'chip'=8,'core'=2] {'sp'}, dimensions={0} | all-to-all | bytes 2097152 | tf_op jit(solution)/shard_map/all_to_all | solution.py:301
  45.1 4.7 %collective-permute-start = (bf16[256,2048]{1,0:T(8,128)(2,1)S(1)}, bf16[256,2048]{1,0:T(8,128)(2,1)S(1)}, u32[]{:S(2)}, u32[]{:S(2)}) collective-permute-start(bf16[256,2048]{1,0:T(8,128)(2,1)S(1)} %bitcast.20), channel_id=1, source_target_pairs={{0,1},{1,0},{2,3},{3,2},{4,5},{5,4},{6,7},{7,6},{8,9},{9,8},{10,11... | collective-permute-start | bytes 3145736 | tf_op jit(solution)/shard_map/ppermute | solution.py:53
  49.8 3.2 %collective-permute-start.3 = (bf16[1,2048,128]{2,1,0:T(8,128)(2,1)S(1)}, bf16[1,2048,128]{2,1,0:T(8,128)(2,1)S(1)}, u32[]{:S(2)}, u32[]{:S(2)}) collective-permute-start(bf16[1,2048,128]{2,1,0:T(8,128)(2,1)S(1)} %copy-done), channel_id=1, source_target_pairs={{0,2},{2,0},{4,6},{6,4},{8,10},{10,8},{12,14},{14,12},{1,3},{3,1},... | collective-permute-start | bytes 1572872 | tf_op jit(solution)/shard_map/ppermute | solution.py:58
  53.1 2.1 %collective-permute-start.4 = (bf16[1,2048,128]{2,1,0:T(8,128)(2,1)S(1)}, bf16[1,2048,128]{2,1,0:T(8,128)(2,1)S(1)}, u32[]{:S(2)}, u32[]{:S(2)}) collective-permute-start(bf16[1,2048,128]{2,1,0:T(8,128)(2,1)S(1)} %copy-done.1), channel_id=1, source_target_pairs={{0,2},{2,0},{4,6},{6,4},{8,10},{10,8},{12,14},{14,12},{1,3},{3,1},... | collective-permute-start | bytes 1572872 | tf_op jit(solution)/shard_map/ppermute | solution.py:58
  55.2 3.2 %collective-permute-start.5 = (bf16[1,128,2048]{2,1,0:T(8,128)(2,1)S(1)}, bf16[1,128,2048]{2,1,0:T(8,128)(2,1)S(1)}, u32[]{:S(2)}, u32[]{:S(2)}) collective-permute-start(bf16[1,128,2048]{2,1,0:T(8,128)(2,1)S(1)} %copy-done.2), channel_id=1, source_target_pairs={{0,2},{2,0},{4,6},{6,4},{8,10},{10,8},{12,14},{14,12},{1,3},{3,1},... | collective-permute-start | bytes 1572872 | tf_op jit(solution)/shard_map/ppermute | solution.py:58
  58.4 6.8 %collective-permute-done.3.refs_3_ = bf16[1,2048,128]{2,1,0:T(8,128)(2,1)S(1)} collective-permute-done((bf16[1,2048,128]{2,1,0:T(8,128)(2,1)S(1)}, bf16[1,2048,128]{2,1,0:T(8,128)(2,1)S(1)}, u32[]{:S(2)}, u32[]{:S(2)}) %collective-permute-start.3) | collective-permute-done | bytes 524320 | tf_op jit(solution)/shard_map/ppermute | solution.py:58
  65.2 11.2 %collective-permute-done.4.refs_4_ = bf16[1,2048,128]{2,1,0:T(8,128)(2,1)S(1)} collective-permute-done((bf16[1,2048,128]{2,1,0:T(8,128)(2,1)S(1)}, bf16[1,2048,128]{2,1,0:T(8,128)(2,1)S(1)}, u32[]{:S(2)}, u32[]{:S(2)}) %collective-permute-start.4) | collective-permute-done | bytes 524320 | tf_op jit(solution)/shard_map/ppermute | solution.py:58
  76.4 11.2 %collective-permute-done.5.refs_5_ = bf16[1,128,2048]{2,1,0:T(8,128)(2,1)S(1)} collective-permute-done((bf16[1,128,2048]{2,1,0:T(8,128)(2,1)S(1)}, bf16[1,128,2048]{2,1,0:T(8,128)(2,1)S(1)}, u32[]{:S(2)}, u32[]{:S(2)}) %collective-permute-start.5) | collective-permute-done | bytes 524320 | tf_op jit(solution)/shard_map/ppermute | solution.py:58
  87.7 4.7 %shard_map.181 = (bf16[3,256,128]{2,1,0:T(8,128)(2,1)S(1)}, bf16[3,256,128]{2,1,0:T(8,128)(2,1)S(1)}, f32[256,1024]{1,0:T(8,128)S(1)}, bf16[256,1024]{1,0:T(8,128)(2,1)S(1)}) custom-call(s32[3]{0:T(128)S(1)} %pad_add_fusion.ids, bf16[256,2048]{1,0:T(8,128)(2,1)S(1)} %bitcast.21, bf16[256,2048]{1,0:T(8,128)(2,1)S(1)} %collective-permute-done.other, ...), custom_call_target="tpu_custom_call" | custom-call | flops 1000000000 | bytes 5242892 | tf_op jit(solution)/shard_map/pallas_call | solution.py:37
  92.4 2.8 %collective-permute-start.6 = (bf16[256,1024]{1,0:T(8,128)(2,1)S(1)}, bf16[256,1024]{1,0:T(8,128)(2,1)S(1)}, u32[]{:S(2)}, u32[]{:S(2)}) collective-permute-start(bf16[256,1024]{1,0:T(8,128)(2,1)S(1)} %get-tuple-element.27), channel_id=1, source_target_pairs={{0,1},{1,0},{2,3},{3,2},{4,5},{5,4},{6,7},{7,6},{8,9},{9,8},{10,11... | collective-permute-start | bytes 1572872 | tf_op jit(solution)/shard_map/ppermute | solution.py:53
  95.2 3.2 %collective-permute-start.1 = (bf16[256,2048]{1,0:T(8,128)(2,1)S(1)}, bf16[256,2048]{1,0:T(8,128)(2,1)S(1)}, u32[]{:S(2)}, u32[]{:S(2)}) collective-permute-start(bf16[256,2048]{1,0:T(8,128)(2,1)S(1)} %bitcast.22), channel_id=1, source_target_pairs={{0,2},{2,0},{4,6},{6,4},{8,10},{10,8},{12,14},{14,12},{1,3},{3,1},... | collective-permute-start | bytes 3145736 | tf_op jit(solution)/shard_map/ppermute | solution.py:58
  98.4 0.9 add_convert_fusion
  99.3 15.0 %all-to-all-start.1 = ((bf16[256,8,128]{2,1,0:T(8,128)(2,1)}), bf16[256,8,128]{2,1,0:T(8,128)(2,1)}, u32[]{:S(2)}, u32[]{:S(2)}) async-start(bf16[256,8,128]{2,1,0:T(8,128)(2,1)} %bitcast.30), calls=%async_computation.1 | async-start | bytes 1048576 | tf_op jit(solution)/shard_map/all_to_all | solution.py:331
  114.3 10.4 %collective-permute-done.1.far = bf16[256,2048]{1,0:T(8,128)(2,1)S(1)} collective-permute-done((bf16[256,2048]{1,0:T(8,128)(2,1)S(1)}, bf16[256,2048]{1,0:T(8,128)(2,1)S(1)}, u32[]{:S(2)}, u32[]{:S(2)}) %collective-permute-start.1) | collective-permute-done | bytes 1048608 | tf_op jit(solution)/shard_map/ppermute | solution.py:58
  124.7 3.1 %collective-permute-start.2 = (bf16[256,2048]{1,0:T(8,128)(2,1)S(1)}, bf16[256,2048]{1,0:T(8,128)(2,1)}, u32[]{:S(2)}, u32[]{:S(2)}) collective-permute-start(bf16[256,2048]{1,0:T(8,128)(2,1)S(1)} %collective-permute-done.1.far), channel_id=1, source_target_pairs={{0,1},{1,0},{2,3},{3,2},{4,5},{5,4},{6,7},{7,6},{8,9},{9,8},{10,11... | collective-permute-start | bytes 3145736 | tf_op jit(solution)/shard_map/ppermute | solution.py:53
  127.9 10.9 %all-to-all-done.1 = bf16[256,8,128]{2,1,0:T(8,128)(2,1)} async-done(((bf16[256,8,128]{2,1,0:T(8,128)(2,1)}), bf16[256,8,128]{2,1,0:T(8,128)(2,1)}, u32[]{:S(2)}, u32[]{:S(2)}) %all-to-all-start.1) | async-done | bytes 524320 | tf_op jit(solution)/shard_map/all_to_all | solution.py:331
  138.9 2.5 %shard_map.183 = bf16[144,128]{1,0:T(8,128)(2,1)} custom-call(s32[3]{0:T(128)} %copy-done.5, bf16[2048,128]{1,0:T(8,128)(2,1)} %bitcast.13.data, s32[2,128]{1,0:T(2,128)} %copy-done.18, bf16[128,2048]{1,0:T(8,128)(2,1)} %cot.3, bf16[64,128]{1,0:T(8,128)(2,1)} %conv.3), custom_call_target="tpu_custom_call" | custom-call | flops 1000000000 | bytes 1065996 | tf_op jit(solution)/shard_map/pallas_call | solution.py:37
  141.4 19.2 %all-gather = bf16[2304,128]{1,0:T(8,128)(2,1)S(1)} all-gather(bf16[144,128]{1,0:T(8,128)(2,1)} %shard_map.183), channel_id=2, replica_groups=mesh['sp'=32,'chip'=8,'core'=2] {'chip','core'}, dimensions={0}, use_global_device_ids=true | all-gather | bytes 626688 | tf_op jit(solution)/shard_map/all_gather | solution.py:365
  160.6 1.5 shard_map.184
  162.1 12.4 %all_to_all.21.sums = f32[16,8,128]{2,1,0:T(8,128)} all-to-all(f32[16,8,128]{2,1,0:T(8,128)S(1)} %get-tuple-element.39), channel_id=1, replica_groups=mesh['sp'=32,'chip'=8,'core'=2] {'chip','core'}, dimensions={0} | all-to-all | bytes 131072 | tf_op jit(solution)/shard_map/all_to_all | solution.py:380
  174.5 7.7 %all-to-all-start.2 = ((bf16[32,32,128]{2,1,0:T(8,128)(2,1)}), bf16[32,32,128]{2,1,0:T(8,128)(2,1)}, u32[]{:S(2)}, u32[]{:S(2)}) async-start(bf16[32,32,128]{2,1,0:T(8,128)(2,1)} %get-tuple-element.38), calls=%async_computation.2 | async-start | bytes 524288 | tf_op jit(solution)/shard_map/all_to_all | solution.py:388
  182.2 2.1 %collective-permute-start.7 = (bf16[3,256,128]{2,1,0:T(8,128)(2,1)}, bf16[3,256,128]{2,1,0:T(8,128)(2,1)S(1)}, u32[]{:S(2)}, u32[]{:S(2)}) collective-permute-start(bf16[3,256,128]{2,1,0:T(8,128)(2,1)} %copy-done.10), channel_id=1, source_target_pairs={{0,2},{2,0},{4,6},{6,4},{8,10},{10,8},{12,14},{14,12},{1,3},{3,1},... | collective-permute-start | bytes 589832 | tf_op jit(solution)/shard_map/ppermute | solution.py:58
  185.0 0.8 copy-done.3
  185.8 0.9 copy-done.17
  186.8 1.6 collective-permute-start.8
  188.4 2.0 %collective-permute-done.7.far_acts = bf16[3,256,128]{2,1,0:T(8,128)(2,1)S(1)} collective-permute-done((bf16[3,256,128]{2,1,0:T(8,128)(2,1)}, bf16[3,256,128]{2,1,0:T(8,128)(2,1)S(1)}, u32[]{:S(2)}, u32[]{:S(2)}) %collective-permute-start.7) | collective-permute-done | bytes 196640 | tf_op jit(solution)/shard_map/ppermute | solution.py:58
  190.4 4.2 %shard_map.182 = (bf16[2048,128]{1,0:T(8,128)(2,1)}, bf16[2048,128]{1,0:T(8,128)(2,1)}, bf16[128,2048]{1,0:T(8,128)(2,1)}) custom-call(s32[3]{0:T(128)S(1)} %copy-done.6, bf16[256,2048]{1,0:T(8,128)(2,1)S(1)} %bitcast.23, bf16[256,2048]{1,0:T(8,128)(2,1)S(1)} %collective-permute-done.other, bf16[256,2048]{1,0:T(8,128)(2,1)S(1)} %collective-permute-done.1.far, ...), custom_call_target="tpu_custom_call" | custom-call | flops 1000000000 | bytes 4587532 | tf_op jit(solution)/shard_map/pallas_call | solution.py:37
  194.7 1.6 shard_map.186
  196.2 1.0 convert_reduce_fusion
  (49 shorter events, 2.9 us)
Async XLA Ops:
  0.7 86.9 %copy-start.5 = (s32[3]{0:T(128)}, s32[3]{0:T(128)S(1)}, u32[]{:S(2)}) copy-start(s32[3]{0:T(128)S(1)} %pad_add_fusion.ids) | copy-start | bytes 40
  0.7 0.7 copy-start.15
  0.7 0.7 copy-start.14
  1.4 1.0 copy-start.7
  2.5 1.0 copy-start.8
  4.7 0.6 copy-start.18
  5.3 44.6 %copy-start = (bf16[1,2048,128]{2,1,0:T(8,128)(2,1)S(1)}, bf16[1,2048,128]{2,1,0:T(8,128)(2,1)}, u32[]{:S(2)}) copy-start(bf16[1,2048,128]{2,1,0:T(8,128)(2,1)} %refs_0_.1) | copy-start | bytes 1572868
  5.3 47.8 %copy-start.1 = (bf16[1,2048,128]{2,1,0:T(8,128)(2,1)S(1)}, bf16[1,2048,128]{2,1,0:T(8,128)(2,1)}, u32[]{:S(2)}) copy-start(bf16[1,2048,128]{2,1,0:T(8,128)(2,1)} %refs_1_.1) | copy-start | bytes 1572868
  5.3 49.9 %copy-start.2 = (bf16[1,128,2048]{2,1,0:T(8,128)(2,1)S(1)}, bf16[1,128,2048]{2,1,0:T(8,128)(2,1)}, u32[]{:S(2)}) copy-start(bf16[1,128,2048]{2,1,0:T(8,128)(2,1)} %refs_2_.1) | copy-start | bytes 1572868
  45.1 42.6 %collective-permute-start = (bf16[256,2048]{1,0:T(8,128)(2,1)S(1)}, bf16[256,2048]{1,0:T(8,128)(2,1)S(1)}, u32[]{:S(2)}, u32[]{:S(2)}) collective-permute-start(bf16[256,2048]{1,0:T(8,128)(2,1)S(1)} %bitcast.20), channel_id=1, source_target_pairs={{0,1},{1,0},{2,3},{3,2},{4,5},{5,4},{6,7},{7,6},{8,9},{9,8},{10,11... | collective-permute-start | bytes 3145736 | tf_op jit(solution)/shard_map/ppermute | solution.py:53
  49.8 15.4 %collective-permute-start.3 = (bf16[1,2048,128]{2,1,0:T(8,128)(2,1)S(1)}, bf16[1,2048,128]{2,1,0:T(8,128)(2,1)S(1)}, u32[]{:S(2)}, u32[]{:S(2)}) collective-permute-start(bf16[1,2048,128]{2,1,0:T(8,128)(2,1)S(1)} %copy-done), channel_id=1, source_target_pairs={{0,2},{2,0},{4,6},{6,4},{8,10},{10,8},{12,14},{14,12},{1,3},{3,1},... | collective-permute-start | bytes 1572872 | tf_op jit(solution)/shard_map/ppermute | solution.py:58
  53.1 23.4 %collective-permute-start.4 = (bf16[1,2048,128]{2,1,0:T(8,128)(2,1)S(1)}, bf16[1,2048,128]{2,1,0:T(8,128)(2,1)S(1)}, u32[]{:S(2)}, u32[]{:S(2)}) collective-permute-start(bf16[1,2048,128]{2,1,0:T(8,128)(2,1)S(1)} %copy-done.1), channel_id=1, source_target_pairs={{0,2},{2,0},{4,6},{6,4},{8,10},{10,8},{12,14},{14,12},{1,3},{3,1},... | collective-permute-start | bytes 1572872 | tf_op jit(solution)/shard_map/ppermute | solution.py:58
  55.2 32.5 %collective-permute-start.5 = (bf16[1,128,2048]{2,1,0:T(8,128)(2,1)S(1)}, bf16[1,128,2048]{2,1,0:T(8,128)(2,1)S(1)}, u32[]{:S(2)}, u32[]{:S(2)}) collective-permute-start(bf16[1,128,2048]{2,1,0:T(8,128)(2,1)S(1)} %copy-done.2), channel_id=1, source_target_pairs={{0,2},{2,0},{4,6},{6,4},{8,10},{10,8},{12,14},{14,12},{1,3},{3,1},... | collective-permute-start | bytes 1572872 | tf_op jit(solution)/shard_map/ppermute | solution.py:58
  92.4 7.0 %copy-start.10 = (bf16[3,256,128]{2,1,0:T(8,128)(2,1)}, bf16[3,256,128]{2,1,0:T(8,128)(2,1)S(1)}, u32[]{:S(2)}) copy-start(bf16[3,256,128]{2,1,0:T(8,128)(2,1)S(1)} %get-tuple-element.31) | copy-start | bytes 589828
  92.4 6.0 %collective-permute-start.6 = (bf16[256,1024]{1,0:T(8,128)(2,1)S(1)}, bf16[256,1024]{1,0:T(8,128)(2,1)S(1)}, u32[]{:S(2)}, u32[]{:S(2)}) collective-permute-start(bf16[256,1024]{1,0:T(8,128)(2,1)S(1)} %get-tuple-element.27), channel_id=1, source_target_pairs={{0,1},{1,0},{2,3},{3,2},{4,5},{5,4},{6,7},{7,6},{8,9},{9,8},{10,11... | collective-permute-start | bytes 1572872 | tf_op jit(solution)/shard_map/ppermute | solution.py:53
  95.2 29.5 %collective-permute-start.1 = (bf16[256,2048]{1,0:T(8,128)(2,1)S(1)}, bf16[256,2048]{1,0:T(8,128)(2,1)S(1)}, u32[]{:S(2)}, u32[]{:S(2)}) collective-permute-start(bf16[256,2048]{1,0:T(8,128)(2,1)S(1)} %bitcast.22), channel_id=1, source_target_pairs={{0,2},{2,0},{4,6},{6,4},{8,10},{10,8},{12,14},{14,12},{1,3},{3,1},... | collective-permute-start | bytes 3145736 | tf_op jit(solution)/shard_map/ppermute | solution.py:58
  99.3 39.5 %all-to-all-start.1 = ((bf16[256,8,128]{2,1,0:T(8,128)(2,1)}), bf16[256,8,128]{2,1,0:T(8,128)(2,1)}, u32[]{:S(2)}, u32[]{:S(2)}) async-start(bf16[256,8,128]{2,1,0:T(8,128)(2,1)} %bitcast.30), calls=%async_computation.1 | async-start | bytes 1048576 | tf_op jit(solution)/shard_map/all_to_all | solution.py:331
  114.3 13.5 %copy-start.20 = (f32[64]{0:T(128)S(1)}, f32[64]{0:T(128)}, u32[]{:S(2)}) copy-start(f32[64]{0:T(128)} %param.25) | copy-start | bytes 772
  124.7 65.8 %collective-permute-start.2 = (bf16[256,2048]{1,0:T(8,128)(2,1)S(1)}, bf16[256,2048]{1,0:T(8,128)(2,1)}, u32[]{:S(2)}, u32[]{:S(2)}) collective-permute-start(bf16[256,2048]{1,0:T(8,128)(2,1)S(1)} %collective-permute-done.1.far), channel_id=1, source_target_pairs={{0,1},{1,0},{2,3},{3,2},{4,5},{5,4},{6,7},{7,6},{8,9},{9,8},{10,11... | collective-permute-start | bytes 3145736 | tf_op jit(solution)/shard_map/ppermute | solution.py:53
  141.4 19.2 %copy-start.9 = (bf16[2048,64]{0,1:T(8,128)(2,1)S(1)}, bf16[2048,64]{0,1:T(8,128)(2,1)}, u32[]{:S(2)}) copy-start(bf16[2048,64]{0,1:T(8,128)(2,1)} %param.20) | copy-start | bytes 786436
  141.4 19.2 %copy-start.11 = (bf16[64,128]{1,0:T(8,128)(2,1)S(1)}, bf16[64,128]{1,0:T(8,128)(2,1)}, u32[]{:S(2)}) copy-start(bf16[64,128]{1,0:T(8,128)(2,1)} %conv.3) | copy-start | bytes 49156
  162.1 12.4 %copy-start.16 = (f32[136,128]{1,0:T(8,128)}, f32[136,128]{1,0:T(8,128)S(1)}, u32[]{:S(2)}) copy-start(f32[136,128]{1,0:T(8,128)S(1)} %get-tuple-element.40.kept) | copy-start | bytes 208900
  174.5 9.8 %copy-start.19 = (f32[31,64]{1,0:T(8,128)S(1)}, f32[31,64]{1,0:T(8,128)}, u32[]{:S(2)}) copy-start(f32[31,64]{1,0:T(8,128)} %param.23) | copy-start | bytes 23812
  174.5 21.7 %all-to-all-start.2 = ((bf16[32,32,128]{2,1,0:T(8,128)(2,1)}), bf16[32,32,128]{2,1,0:T(8,128)(2,1)}, u32[]{:S(2)}, u32[]{:S(2)}) async-start(bf16[32,32,128]{2,1,0:T(8,128)(2,1)} %get-tuple-element.38), calls=%async_computation.2 | async-start | bytes 524288 | tf_op jit(solution)/shard_map/all_to_all | solution.py:388
  182.2 8.3 %collective-permute-start.7 = (bf16[3,256,128]{2,1,0:T(8,128)(2,1)}, bf16[3,256,128]{2,1,0:T(8,128)(2,1)S(1)}, u32[]{:S(2)}, u32[]{:S(2)}) collective-permute-start(bf16[3,256,128]{2,1,0:T(8,128)(2,1)} %copy-done.10), channel_id=1, source_target_pairs={{0,2},{2,0},{4,6},{6,4},{8,10},{10,8},{12,14},{14,12},{1,3},{3,1},... | collective-permute-start | bytes 589832 | tf_op jit(solution)/shard_map/ppermute | solution.py:58
  185.0 0.8 copy-start.3
  185.8 0.9 copy-start.17
  186.7 3.7 %copy-start.6 = (s32[3]{0:T(128)S(1)}, s32[3]{0:T(128)}, u32[]{:S(2)}) copy-start(s32[3]{0:T(128)} %copy-done.5) | copy-start | bytes 40
  186.8 7.9 %copy-start.4 = (f32[31,64]{0,1:T(8,128)S(1)}, f32[31,64]{0,1:T(8,128)}, u32[]{:S(2)}) copy-start(f32[31,64]{0,1:T(8,128)} %copy.21) | copy-start | bytes 23812
  186.8 7.9 %copy-start.12 = (bf16[64,128]{1,0:T(8,128)(2,1)S(1)}, bf16[64,128]{1,0:T(8,128)(2,1)}, u32[]{:S(2)}) copy-start(bf16[64,128]{1,0:T(8,128)(2,1)} %gate.1) | copy-start | bytes 49156
  186.8 7.9 %copy-start.13 = (bf16[64,128]{1,0:T(8,128)(2,1)S(1)}, bf16[64,128]{1,0:T(8,128)(2,1)}, u32[]{:S(2)}) copy-start(bf16[64,128]{1,0:T(8,128)(2,1)} %value.1) | copy-start | bytes 49156
  186.8 7.8 %collective-permute-start.8 = (f32[64,128]{1,0:T(8,128)S(1)}, f32[64,128]{1,0:T(8,128)S(1)}, u32[]{:S(2)}, u32[]{:S(2)}) collective-permute-start(f32[64,128]{1,0:T(8,128)S(1)} %shard_map.185.conv), channel_id=1, source_target_pairs={{16,0},{32,16},{48,32},{64,48},{80,64},{96,80},{112,96},{128,112},... | collective-permute-start | bytes 98312 | tf_op jit(solution)/shard_map/ppermute | solution.py:392
